TPU v7x, 128 devices: a whole 4x4x4 slice. The times are simulated.
128 devices in a mesh: ra: 16 (over z, x), cb: 8 (over y, core).
Axes of the slice: x: 4, y: 4, z: 4, core: 2. Of those that a mesh axis runs over, the one named last changes fastest.
Arguments:
- inputs: bfloat16 [1536, 4096], P(None, 'ra'), may hold values from -12 to 12
- gate_weight: bfloat16 [2, 4096, 11264], P(None, 'ra', 'cb'), may hold values from -0.09375 to 0.09375
- up_weight: bfloat16 [2, 4096, 11264], P(None, 'ra', 'cb'), may hold values from -0.09375 to 0.09375
- down_weight: bfloat16 [2, 11264, 4096], P(None, 'cb', 'ra'), may hold values from -0.0546875 to 0.0546875
- norm_gain: float32 [2, 4096], P(None, 'ra'), may hold values from 0.05 to 8
- norm_shift: float32 [2, 4096], P(None, 'ra'), may hold values from -1.5 to 1.5
Outputs:
- outputs: bfloat16 [1536, 4096], P(None, 'ra')
All inputs are finite; a program needn't handle non-finite values.
Results may differ from a plain program's by a relative error of at most 0.04.
Values may be sent and summed in bfloat16 or wider, within the bound.
No kernel may reach another device: no remote copies, remote signals or barrier semaphores. Data moves between devices by JAX's collectives and lax.ppermute only.
A program may use at most 64 MiB of HBM per device.

v0:
```python
import jax
import jax.numpy as jnp
from jax import lax
from jax.experimental import pallas as pl
from jax.experimental.pallas import tpu as pltpu
from jax.sharding import Mesh
from jax.sharding import PartitionSpec as P

RESIDUAL = 0.5
EPSILON = 1e-05
WIDTH = 4096.0
BF16 = jnp.bfloat16
F32 = jnp.float32
ANY = pl.BlockSpec(memory_space=pl.ANY)
SMEM = pl.BlockSpec(memory_space=pltpu.SMEM)
VMEM = pl.BlockSpec(memory_space=pltpu.VMEM)


def exchange(parts, axes):
    return lax.all_to_all(parts, axes, 0, 0, tiled=True)


def share(block, axes, peers):
    return exchange(jnp.broadcast_to(block[None], (peers, *block.shape)), axes)


def shift(block, axis, step):
    return lax.ppermute(block, axis, [(i, (i + step) % 4) for i in range(4)])


def swap_core(block):
    return lax.ppermute(block, "c", [(0, 1), (1, 0)])


def share4(block, axis):
    return exchange4([block] * 4, axis)


def exchange4(parts, axis):
    got = [parts[0]]
    for step in (1, 2, 3):
        got.append(shift(parts[step], axis, step))
    return got


def behind(own, k):
    return lax.rem(own + 4 - k, 4)


def dot_nt(a, b):
    return lax.dot_general(a, b, (((1,), (1,)), ((), ())), preferred_element_type=F32)


def sds(*shape):
    return jax.ShapeDtypeStruct(shape, BF16)


def run_copies(copies, sems):
    started = []
    for i, (src, dst) in enumerate(copies):
        copy = pltpu.make_async_copy(src, dst, sems.at[i])
        copy.start()
        started.append(copy)
    return started


def turn_kernel(gate_ref, up_ref, down_ref, out):
    rows = out.shape[2]
    for g, ref in enumerate((gate_ref, up_ref)):
        turned = ref[0].T
        for p in range(16):
            out[p, g] = turned[p * rows : p * rows + rows]
    for p in range(16):
        out[p, 2] = down_ref[0, p * rows : p * rows + rows]


def turn(layer, gate, up, down):
    rows = gate.shape[2] // 16
    pick = lambda i: (layer, 0, 0)
    return pl.pallas_call(
        turn_kernel,
        out_shape=sds(16, 3, rows, 256),
        in_specs=[
            pl.BlockSpec((1, *gate.shape[1:]), pick),
            pl.BlockSpec((1, *up.shape[1:]), pick),
            pl.BlockSpec((1, *down.shape[1:]), pick),
        ],
        out_specs=VMEM,
        grid=(1,),
    )(gate, up, down)


def pack_kernel(place_ref, gate_ref, up_ref, down_ref, *rest):
    outs, turned = rest[:-1], rest[-1]
    own = place_ref[1]
    cols = gate_ref.shape[2]
    for g, ref in enumerate((gate_ref, up_ref)):
        for at in range(0, cols, 128):
            turned[g, at : at + 128, :] = ref[0, :, at : at + 128].T
    rows = cols // 4
    for k in range(4):
        at = pl.ds(pl.multiple_of(lax.rem(own + k, 4) * rows, 16), rows)
        outs[k][0:2] = turned[:, at, :]
        outs[4 + k][...] = down_ref[0, at, :]


def pack(place, layer, gate, up, down):
    rows = gate.shape[2] // 4
    out_shape = [sds(2, rows, 256)] * 4 + [sds(rows, 256)] * 4
    pick = lambda i: (layer, 0, 0)
    return pl.pallas_call(
        pack_kernel,
        out_shape=out_shape,
        in_specs=[
            SMEM,
            pl.BlockSpec((1, *gate.shape[1:]), pick),
            pl.BlockSpec((1, *up.shape[1:]), pick),
            pl.BlockSpec((1, *down.shape[1:]), pick),
        ],
        out_specs=[VMEM] * len(out_shape),
        grid=(1,),
        scratch_shapes=[pltpu.VMEM((2, gate.shape[2], 256), BF16)],
    )(place, gate, up, down)


def gate_up_kernel(place_ref, *refs):
    rows, mine, theirs, outs = refs[:4], refs[4:8], refs[8:12], refs[12:16]
    stream, weights, sems = refs[16:]
    z, y = place_ref[0], place_ref[2]
    half = mine[0].shape[1]
    copies = []
    for m in range(4):
        lanes = slice(m * 256, m * 256 + 256)
        for s, piece in enumerate((mine[m], theirs[m])):
            for g in range(2):
                at = (2 * g + s) * half
                copies.append((piece.at[g], weights.at[at : at + half, lanes]))
    for j in range(4):
        for m in range(4):
            copies.append((rows[j].at[m], stream.at[behind(y, j), :, m * 256 : m * 256 + 256]))
    for copy in run_copies(copies, sems):
        copy.wait()
    for k in range(4):
        outs[k][...] = dot_nt(stream[lax.rem(z + k, 4)], weights[...]).astype(BF16)


def gate_up(place, rows, mine, theirs):
    n, half = rows[0].shape[1], mine[0].shape[1]
    return pl.pallas_call(
        gate_up_kernel,
        out_shape=[sds(n, 4 * half)] * 4,
        in_specs=[SMEM] + [ANY] * 12,
        out_specs=[VMEM] * 4,
        scratch_shapes=[
            pltpu.VMEM((4, n, 1024), BF16),
            pltpu.VMEM((4 * half, 1024), BF16),
            pltpu.SemaphoreType.DMA((32,)),
        ],
    )(place, *rows, *mine, *theirs)


def down_kernel(place_ref, *refs):
    hidden, mine, theirs, out = refs[:4], refs[4:8], refs[8:12], refs[12]
    rows, weights, sems = refs[13:]
    z, x = place_ref[0], place_ref[1]
    half = mine[0].shape[0]
    copies = []
    for m in range(4):
        lanes = pl.ds(pl.multiple_of(behind(x, m) * 256, 256), 256)
        copies.append((mine[m], weights.at[:half, lanes]))
        copies.append((theirs[m], weights.at[half:, lanes]))
    for k in range(4):
        copies.append((hidden[k], rows.at[behind(z, k)]))
    for copy in run_copies(copies, sems):
        copy.wait()
    n = rows.shape[1]
    for b in range(4):
        out[b * n : b * n + n, :] = jnp.dot(rows[b], weights[...], preferred_element_type=F32).astype(BF16)


def down(place, hidden, mine, theirs):
    n, cols = hidden[0].shape
    return pl.pallas_call(
        down_kernel,
        out_shape=sds(4 * n, 1024),
        in_specs=[SMEM] + [ANY] * 12,
        out_specs=VMEM,
        scratch_shapes=[
            pltpu.VMEM((4, n, cols), BF16),
            pltpu.VMEM((cols, 1024), BF16),
            pltpu.SemaphoreType.DMA((12,)),
        ],
    )(place, *hidden, *mine, *theirs)


def block_kernel(place_ref, rows_ref, *refs):
    pieces, out, own_out = refs[:10], refs[10], refs[11]
    stream, w_gu, w_down, row_sems, sems = refs[12:]
    z, x = place_ref[0], place_ref[1]
    n = rows_ref.shape[1]
    cols = pieces[0].shape[3]
    copies = []
    for i in range(16):
        copies.append((rows_ref.at[i], stream.at[i % 4 * n : i % 4 * n + n, i // 4 * 1024 : i // 4 * 1024 + 1024]))
    row_copies = run_copies(copies, row_sems)
    spans = [(q, slice(0, 4)) for q in range(3)] + [(3, slice(0, 2)), (3, slice(2, 4))]
    copies = []
    for i, piece in enumerate(pieces):
        slot, span = spans[i % 5]
        for g in range(2):
            copies.append((piece.at[:, :, g], w_gu.at[span, :, g, slot + 4 * (i // 5)]))
    for i, piece in enumerate(pieces):
        slot, span = spans[i % 5]
        copies.append((piece.at[:, :, 2], w_down.at[span, :, slot + 4 * (i // 5)]))
    weight_copies = run_copies(copies, sems)
    for copy in row_copies:
        copy.wait()
    for copy in weight_copies[:20]:
        copy.wait()
    at = z * 4 + x
    own_out[...] = stream[:, pl.ds(pl.multiple_of(at * 256, 256), 256)]
    total = [None, None]
    for i in range(16):
        block = stream[:, i * 256 : i * 256 + 256]
        for g in range(2):
            part = dot_nt(block, w_gu[i // 4, i % 4, g].reshape(8 * cols, 256))
            total[g] = part if total[g] is None else total[g] + part
    hidden = (total[0] * jax.nn.sigmoid(total[0]) * total[1]).astype(BF16)
    for copy in weight_copies[20:]:
        copy.wait()
    for i in range(16):
        part = jnp.dot(hidden, w_down[i // 4, i % 4].reshape(8 * cols, 256), preferred_element_type=F32)
        out[i] = part.astype(BF16)


def block_layer(place, rows, pieces):
    n = rows.shape[1]
    cols = pieces[0].shape[3]
    return pl.pallas_call(
        block_kernel,
        out_shape=[sds(16, 4 * n, 256), sds(4 * n, 256)],
        in_specs=[SMEM] + [ANY] * 11,
        out_specs=[VMEM] * 2,
        scratch_shapes=[
            pltpu.VMEM((4 * n, 4096), BF16),
            pltpu.VMEM((4, 4, 2, 8, cols, 256), BF16),
            pltpu.VMEM((4, 4, 8, cols, 256), BF16),
            pltpu.SemaphoreType.DMA((16,)),
            pltpu.SemaphoreType.DMA((30,)),
        ],
    )(place, rows, *pieces)


def normed(mixed, row_sum, row_squares, gain, shift_row):
    mean = row_sum / WIDTH
    var = row_squares / WIDTH - mean * mean
    out = (mixed - mean[:, None]) * lax.rsqrt(var + EPSILON)[:, None]
    return (out * gain + shift_row).astype(BF16)


def row_stats(mixed):
    return jnp.stack((mixed.sum(axis=1), (mixed * mixed).sum(axis=1)))


def in_order(pieces, own):
    back = jnp.concatenate((pieces[:1], pieces[3:4], pieces[2:3], pieces[1:2]))
    return lax.dynamic_slice_in_dim(jnp.concatenate((back, back[:3])), (4 - own) % 4, 4, 0)


def thirds(values):
    high = lax.reduce_precision(values, 8, 7)
    middle = lax.reduce_precision(values - high, 8, 7)
    low = values - high - middle
    return jnp.concatenate((high, middle, low)).astype(BF16)


def per_device(inputs, gate_weight, up_weight, down_weight, norm_gain, norm_shift):
    z, x, y, c = (lax.axis_index(a) for a in ("z", "x", "y", "c"))
    place = jnp.stack((z, x, y, c)).astype(jnp.int32)
    half = inputs.shape[0] // 2
    quarter = half // 4
    block = half // 16
    cols = gate_weight.shape[2] // 2

    mine = lax.dynamic_slice_in_dim(inputs, c * half + y * quarter, quarter, 0)
    affine = thirds(jnp.stack((norm_gain[0], norm_shift[0])))
    mine = jnp.concatenate((mine, affine, jnp.zeros((2, 256), BF16)))
    mine = jnp.stack(share4(mine, "x"))
    rows = share4(mine[:, :quarter], "y")

    packed = pack(place, 0, gate_weight, up_weight, down_weight)
    gu0 = exchange4(packed[:4], "x")
    down0 = exchange4(packed[4:], "x")
    gu0_core = [swap_core(w) for w in gu0]
    down0_core = [swap_core(w) for w in down0]

    w1 = turn(1, gate_weight, up_weight, down_weight)
    w1 = exchange(w1, ("z", "x")).reshape(4, 4, *w1.shape[1:])
    near = shift(w1, "y", 1)
    far = shift(w1, "y", 3)
    across = [shift(near[:2], "y", 1)]
    across.append(shift(far[2:], "y", 3))
    w1 = [w1, near, far, *across]
    w1_core = []
    for w in w1:
        w1_core.append(swap_core(w))

    sums = gate_up(place, rows, gu0, gu0_core)
    sums = exchange4(sums, "z")
    summed = sum(piece.astype(F32) for piece in sums)
    hidden = (jax.nn.silu(summed[:, :cols]) * summed[:, cols:]).astype(BF16)
    hidden = share4(hidden, "z")
    partial = down(place, hidden, down0, down0_core)
    branch = exchange(partial.reshape(16, block, 1024), ("y", "x"))
    branch = branch.astype(F32).sum(axis=0)
    own = lax.dynamic_slice_in_dim(rows[0], x * block, block, 1)
    own = in_order(own, x).transpose(1, 0, 2).reshape(block, 1024)
    affine = in_order(mine[:, quarter : quarter + 6].astype(F32), x)
    affine = (affine[:, :2] + affine[:, 2:4]) + affine[:, 4:]
    affine = affine.transpose(1, 0, 2).reshape(2, 1024)
    mixed = RESIDUAL * own.astype(F32) + branch
    stats = share(row_stats(mixed), "z", 4).sum(axis=0)
    out = normed(mixed, stats[0], stats[1], affine[0], affine[1])
    stream = share(out, ("z", "x"), 16)

    parts, own = block_layer(place, stream, w1 + w1_core)
    branch = exchange(parts, ("z", "x")).astype(F32).sum(axis=0)
    mixed = RESIDUAL * own.astype(F32) + branch
    stats = share(row_stats(mixed), ("z", "x"), 16).sum(axis=0)
    out = normed(mixed, stats[0], stats[1], norm_gain[1], norm_shift[1])
    ours = share(out, "y", 4).reshape(half, 256)
    theirs = swap_core(ours)
    return jnp.where(c == 0, jnp.concatenate((ours, theirs)), jnp.concatenate((theirs, ours)))


def solution(mesh):
    finer = Mesh(mesh.devices.reshape(4, 4, 4, 2), ("z", "x", "y", "c"))
    ra, cb = ("z", "x"), ("y", "c")
    in_specs = (
        P(None, ra),
        P(None, ra, cb),
        P(None, ra, cb),
        P(None, cb, ra),
        P(None, ra),
        P(None, ra),
    )


    return jax.shard_map(
        per_device, mesh=finer, in_specs=in_specs, out_specs=P(None, ra), check_vma=False
    )
```

profile of v0, /device:TPU:1, one launch (start us, length us, event | category | flops | bytes accessed | tf_op | source)
XLA Modules:
  0.0 283.6 jit_solution(8774627420248065948)
XLA Ops:
  1.2 3.4 %collective-permute-start.2 = (bf16[200,256]{1,0:T(8,128)(2,1)S(1)}, bf16[200,256]{1,0:T(8,128)(2,1)S(1)}, u32[]{:S(2)}, u32[]{:S(2)}) collective-permute-start(bf16[200,256]{1,0:T(8,128)(2,1)S(1)} %concatenate.26), channel_id=1, source_target_pairs={{0,24},{8,0},{16,8},{24,16},{1,25},{9,1},{17,9},{25,17},{2,26},{10... | collective-permute-start | bytes 307208 | tf_op jit(solution)/shard_map/ppermute | solution.py:28
  6.3 3.3 %shard_map.64 = (bf16[2,352,256]{2,1,0:T(8,128)(2,1)}, bf16[2,352,256]{2,1,0:T(8,128)(2,1)}, bf16[2,352,256]{2,1,0:T(8,128)(2,1)}, bf16[2,352,256]{2,1,0:T(8,128...) custom-call(s32[4]{0:T(128)} %pad_add_fusion.place_ref, ...), custom_call_target="tpu_custom_call" | custom-call | tf_op jit(solution)/shard_map/pallas_call | solution.py:111
  13.8 2.8 collective-permute-start.5
  19.7 2.9 %collective-permute-start.4 = (bf16[4,192,256]{2,1,0:T(8,128)(2,1)S(1)}, bf16[4,192,256]{2,1,0:T(8,128)(2,1)}, u32[]{:S(2)}, u32[]{:S(2)}) collective-permute-start(bf16[4,192,256]{2,1,0:T(8,128)(2,1)S(1)} %slice.114.refs_0_), channel_id=1, source_target_pairs={{0,4},{2,6},{4,0},{6,2},{1,5},{3,7},{5,1},{7,3},{8,12},{10,14},{12... | collective-permute-start | bytes 1179656 | tf_op jit(solution)/shard_map/ppermute | solution.py:28
  22.6 5.4 %collective-permute-done.7.refs_6_ = bf16[2,352,256]{2,1,0:T(8,128)(2,1)} collective-permute-done((bf16[2,352,256]{2,1,0:T(8,128)(2,1)}, bf16[2,352,256]{2,1,0:T(8,128)(2,1)}, u32[]{:S(2)}, u32[]{:S(2)}) %collective-permute-start.7) | collective-permute-done | bytes 360480 | tf_op jit(solution)/shard_map/ppermute | solution.py:28
  29.3 2.7 collective-permute-start.10
  34.3 3.3 %shard_map.67 = bf16[16,3,88,256]{3,2,1,0:T(8,128)(2,1)} custom-call(bf16[2,256,1408]{2,1,0:T(8,128)(2,1)} %gate_ref.3, bf16[2,256,1408]{2,1,0:T(8,128)(2,1)} %up_ref.3, bf16[2,1408,256]{2,1,0:T(8,128)(2,1)} %down_ref.3), custom_call_target="tpu_custom_call" | custom-call | tf_op jit(solution)/shard_map/pallas_call | solution.py:80
  37.7 6.1 %all-to-all-start.3 = ((bf16[16,3,88,256]{3,2,1,0:T(8,128)(2,1)}), bf16[16,3,88,256]{3,2,1,0:T(8,128)(2,1)S(1)}, u32[]{:S(2)}, u32[]{:S(2)}) async-start(bf16[16,3,88,256]{3,2,1,0:T(8,128)(2,1)} %shard_map.67), calls=%async_computation.3 | async-start | bytes 4325376 | tf_op jit(solution)/shard_map/all_to_all | solution.py:20
  46.5 2.4 collective-permute-start.20
  48.9 8.0 %shard_map.65 = (bf16[192,1408]{1,0:T(8,128)(2,1)}, bf16[192,1408]{1,0:T(8,128)(2,1)}, bf16[192,1408]{1,0:T(8,128)(2,1)}, bf16[192,1408]{1,0:T(8,128)(2,1)}) custom-call(s32[4]{0:T(128)} %pad_add_fusion.place_ref, bf16[4,192,256]{2,1,0:T(8,128)(2,1)} %copy-done.2, bf16[4,192,256]{2,1,0:T(8,128)(2,1)} %collective-permute-done.3.refs_1_, ...), custom_call_target="tpu_custom_call" | custom-call | tf_op jit(solution)/shard_map/pallas_call | solution.py:149
  58.1 2.4 collective-permute-start.14
  61.7 14.5 %collective-permute-done.19.refs_5_ = bf16[352,256]{1,0:T(8,128)(2,1)} collective-permute-done((bf16[352,256]{1,0:T(8,128)(2,1)}, bf16[352,256]{1,0:T(8,128)(2,1)}, u32[]{:S(2)}, u32[]{:S(2)}) %collective-permute-start.19) | collective-permute-done | bytes 180256 | tf_op jit(solution)/shard_map/ppermute | solution.py:28
  76.2 4.5 %collective-permute-start.21 = (bf16[352,256]{1,0:T(8,128)(2,1)S(1)}, bf16[352,256]{1,0:T(8,128)(2,1)}, u32[]{:S(2)}, u32[]{:S(2)}) collective-permute-start(bf16[352,256]{1,0:T(8,128)(2,1)S(1)} %copy-done.18), channel_id=1, source_target_pairs={{0,24},{8,0},{16,8},{24,16},{1,25},{9,1},{17,9},{25,17},{2,26},{10... | collective-permute-start | bytes 540680 | tf_op jit(solution)/shard_map/ppermute | solution.py:28
  80.7 3.6 %collective-permute-done.20.refs_6_ = bf16[352,256]{1,0:T(8,128)(2,1)} collective-permute-done((bf16[352,256]{1,0:T(8,128)(2,1)}, bf16[352,256]{1,0:T(8,128)(2,1)}, u32[]{:S(2)}, u32[]{:S(2)}) %collective-permute-start.20) | collective-permute-done | bytes 180256 | tf_op jit(solution)/shard_map/ppermute | solution.py:28
  88.0 6.9 %collective-permute-done.14 = bf16[192,1408]{1,0:T(8,128)(2,1)S(1)} collective-permute-done((bf16[192,1408]{1,0:T(8,128)(2,1)}, bf16[192,1408]{1,0:T(8,128)(2,1)S(1)}, u32[]{:S(2)}, u32[]{:S(2)}) %collective-permute-start.14) | collective-permute-done | bytes 540704 | tf_op jit(solution)/shard_map/ppermute | solution.py:28
  100.3 3.5 %collective-permute-start.27 = (bf16[4,4,3,88,256]{4,3,2,1,0:T(8,128)(2,1)S(1)}, bf16[4,4,3,88,256]{4,3,2,1,0:T(8,128)(2,1)}, u32[]{:S(2)}, u32[]{:S(2)}) collective-permute-start(bf16[4,4,3,88,256]{4,3,2,1,0:T(8,128)(2,1)S(1)} %bitcast.49), channel_id=1, source_target_pairs={{0,6},{2,0},{4,2},{6,4},{1,7},{3,1},{5,3},{7,5},{8,14},{10,8},{12,... | collective-permute-start | bytes 6488072 | tf_op jit(solution)/shard_map/ppermute | solution.py:28
  107.5 7.4 %collective-permute-done.16.refs_1_ = bf16[192,704]{1,0:T(8,128)(2,1)} collective-permute-done((bf16[192,704]{1,0:T(8,128)(2,1)S(1)}, bf16[192,704]{1,0:T(8,128)(2,1)}, u32[]{:S(2)}, u32[]{:S(2)}) %collective-permute-start.16) | collective-permute-done | bytes 270368 | tf_op jit(solution)/shard_map/ppermute | solution.py:28
  114.9 5.1 %shard_map.66 = bf16[768,1024]{1,0:T(8,128)(2,1)} custom-call(s32[4]{0:T(128)} %pad_add_fusion.place_ref, bf16[192,704]{1,0:T(8,128)(2,1)} %copy-done.3, bf16[192,704]{1,0:T(8,128)(2,1)} %collective-permute-done.16.refs_1_, bf16[192,704]{1,0:T(8,128)(2,1)} %collective-permute-done.17.refs_2_, bf16[192,704]{1,0:T(8,128)(2,1)} %copy-done.10, ...), custom_call_target="tpu_custom_call" | custom-call | tf_op jit(solution)/shard_map/pallas_call | solution.py:183
  120.1 8.0 %all-to-all-start = ((bf16[16,48,1024]{2,1,0:T(8,128)(2,1)}), bf16[16,48,1024]{2,1,0:T(8,128)(2,1)}, u32[]{:S(2)}, u32[]{:S(2)}) async-start(bf16[16,48,1024]{2,1,0:T(8,128)(2,1)} %bitcast.53), calls=%async_computation | async-start | bytes 3145728 | tf_op jit(solution)/shard_map/all_to_all | solution.py:20
  134.3 33.6 %all-to-all-done = bf16[16,48,1024]{2,1,0:T(8,128)(2,1)} async-done(((bf16[16,48,1024]{2,1,0:T(8,128)(2,1)}), bf16[16,48,1024]{2,1,0:T(8,128)(2,1)}, u32[]{:S(2)}, u32[]{:S(2)}) %all-to-all-start) | async-done | bytes 1572896 | tf_op jit(solution)/shard_map/all_to_all | solution.py:20
  170.4 4.8 %all-to-all-start.1 = ((f32[4,2,48]{2,1,0:T(2,128)}), f32[4,2,48]{2,1,0:T(2,128)S(1)}, u32[]{:S(2)}, u32[]{:S(2)}) async-start(f32[4,2,48]{2,1,0:T(2,128)} %broadcast_in_dim.11), calls=%async_computation.1 | async-start | bytes 8192 | tf_op jit(solution)/shard_map/all_to_all | solution.py:20
  181.3 3.9 %collective-permute-start.32 = (bf16[4,4,3,88,256]{4,3,2,1,0:T(8,128)(2,1)}, bf16[4,4,3,88,256]{4,3,2,1,0:T(8,128)(2,1)}, u32[]{:S(2)}, u32[]{:S(2)}) collective-permute-start(bf16[4,4,3,88,256]{4,3,2,1,0:T(8,128)(2,1)} %collective-permute-done.27.refs_2_), channel_id=1, source_target_pairs={{0,1},{1,0},{2,3},{3,2},{4,5},{5,4},{6,7},{7,6},{8,9},{9,8},{10,11... | collective-permute-start | bytes 6488072 | tf_op jit(solution)/shard_map/ppermute | solution.py:32
  186.7 7.0 %all-to-all-start.2 = ((bf16[16,48,1024]{2,1,0:T(8,128)(2,1)}), bf16[16,48,1024]{2,1,0:T(8,128)(2,1)}, u32[]{:S(2)}, u32[]{:S(2)}) async-start(bf16[16,48,1024]{2,1,0:T(8,128)(2,1)} %broadcast_in_dim.12), calls=%async_computation.2 | async-start | bytes 3145728 | tf_op jit(solution)/shard_map/all_to_all | solution.py:20
  193.8 6.6 %collective-permute-done.29.refs_4_ = bf16[2,4,3,88,256]{4,3,2,1,0:T(8,128)(2,1)} collective-permute-done((bf16[2,4,3,88,256]{4,3,2,1,0:T(8,128)(2,1)}, bf16[2,4,3,88,256]{4,3,2,1,0:T(8,128)(2,1)}, u32[]{:S(2)}, u32[]{:S(2)}) %collective-permute-start.29) | collective-permute-done | bytes 1081376 | tf_op jit(solution)/shard_map/ppermute | solution.py:28
  200.4 3.7 %collective-permute-start.34 = (bf16[2,4,3,88,256]{4,3,2,1,0:T(8,128)(2,1)}, bf16[2,4,3,88,256]{4,3,2,1,0:T(8,128)(2,1)}, u32[]{:S(2)}, u32[]{:S(2)}) collective-permute-start(bf16[2,4,3,88,256]{4,3,2,1,0:T(8,128)(2,1)} %collective-permute-done.29.refs_4_), channel_id=1, source_target_pairs={{0,1},{1,0},{2,3},{3,2},{4,5},{5,4},{6,7},{7,6},{8,9},{9,8},{10,11... | collective-permute-start | bytes 3244040 | tf_op jit(solution)/shard_map/ppermute | solution.py:32
  205.8 3.1 %collective-permute-start.33 = (bf16[2,4,3,88,256]{4,3,2,1,0:T(8,128)(2,1)}, bf16[2,4,3,88,256]{4,3,2,1,0:T(8,128)(2,1)}, u32[]{:S(2)}, u32[]{:S(2)}) collective-permute-start(bf16[2,4,3,88,256]{4,3,2,1,0:T(8,128)(2,1)} %collective-permute-done.28.refs_3_), channel_id=1, source_target_pairs={{0,1},{1,0},{2,3},{3,2},{4,5},{5,4},{6,7},{7,6},{8,9},{9,8},{10,11... | collective-permute-start | bytes 3244040 | tf_op jit(solution)/shard_map/ppermute | solution.py:32
  209.0 8.5 %all-to-all-done.2.rows_ref = bf16[16,48,1024]{2,1,0:T(8,128)(2,1)} async-done(((bf16[16,48,1024]{2,1,0:T(8,128)(2,1)}), bf16[16,48,1024]{2,1,0:T(8,128)(2,1)}, u32[]{:S(2)}, u32[]{:S(2)}) %all-to-all-start.2) | async-done | bytes 1572896 | tf_op jit(solution)/shard_map/all_to_all | solution.py:20
  217.4 13.8 %shard_map.68 = (bf16[16,192,256]{2,1,0:T(8,128)(2,1)}, bf16[192,256]{1,0:T(8,128)(2,1)}) custom-call(s32[4]{0:T(128)} %pad_add_fusion.place_ref, bf16[16,48,1024]{2,1,0:T(8,128)(2,1)} %all-to-all-done.2.rows_ref, bf16[4,4,3,88,256]{4,3,2,1,0:T(8,128)(2,1)} %bitcast.52, bf16[4,4,3,88,256]{4,3,2,1,0:T(8,128)(2,1)} %collective-permute-done.26.refs_1_, ...), custom_call_target="tpu_custom_call" | custom-call | tf_op jit(solution)/shard_map/pallas_call | solution.py:239
  231.3 25.8 %all_to_all.35 = bf16[16,192,256]{2,1,0:T(8,128)(2,1)S(1)} all-to-all(bf16[16,192,256]{2,1,0:T(8,128)(2,1)} %get-tuple-element.32), channel_id=1, replica_groups=mesh['z'=4,'x'=4,'y'=4,'c'=2] {'z','x'}, dimensions={0} | all-to-all | bytes 3145728 | tf_op jit(solution)/shard_map/all_to_all | solution.py:20
  258.2 9.4 %all_to_all.36 = f32[16,2,192]{2,1,0:T(2,128)S(1)} all-to-all(f32[16,2,192]{2,1,0:T(2,128)S(1)} %broadcast_in_dim.13), channel_id=1, replica_groups=mesh['z'=4,'x'=4,'y'=4,'c'=2] {'z','x'}, dimensions={0} | all-to-all | bytes 49152 | tf_op jit(solution)/shard_map/all_to_all | solution.py:20
  267.9 8.6 %all_to_all.37 = bf16[4,192,256]{2,1,0:T(8,128)(2,1)S(1)} all-to-all(bf16[4,192,256]{2,1,0:T(8,128)(2,1)S(1)} %broadcast_in_dim.14), channel_id=1, replica_groups=mesh['z'=4,'x'=4,'y'=4,'c'=2] {'y'}, dimensions={0} | all-to-all | bytes 786432 | tf_op jit(solution)/shard_map/all_to_all | solution.py:20
  276.5 4.6 %collective-permute-start.35 = (bf16[768,256]{1,0:T(8,128)(2,1)S(1)}, bf16[768,256]{1,0:T(8,128)(2,1)S(1)}, u32[]{:S(2)}, u32[]{:S(2)}) collective-permute-start(bf16[768,256]{1,0:T(8,128)(2,1)S(1)} %bitcast.55), channel_id=1, source_target_pairs={{0,1},{1,0},{2,3},{3,2},{4,5},{5,4},{6,7},{7,6},{8,9},{9,8},{10,11... | collective-permute-start | bytes 1179656 | tf_op jit(solution)/shard_map/ppermute | solution.py:32
  (144 shorter events, 53.5 us)
Async XLA Ops:
  1.2 11.7 %collective-permute-start.2 = (bf16[200,256]{1,0:T(8,128)(2,1)S(1)}, bf16[200,256]{1,0:T(8,128)(2,1)S(1)}, u32[]{:S(2)}, u32[]{:S(2)}) collective-permute-start(bf16[200,256]{1,0:T(8,128)(2,1)S(1)} %concatenate.26), channel_id=1, source_target_pairs={{0,24},{8,0},{16,8},{24,16},{1,25},{9,1},{17,9},{25,17},{2,26},{10... | collective-permute-start | bytes 307208 | tf_op jit(solution)/shard_map/ppermute | solution.py:28
  11.2 16.8 %collective-permute-start.7 = (bf16[2,352,256]{2,1,0:T(8,128)(2,1)}, bf16[2,352,256]{2,1,0:T(8,128)(2,1)}, u32[]{:S(2)}, u32[]{:S(2)}) collective-permute-start(bf16[2,352,256]{2,1,0:T(8,128)(2,1)} %get-tuple-element.21), channel_id=1, source_target_pairs={{0,16},{8,24},{16,0},{24,8},{1,17},{9,25},{17,1},{25,9},{2,18},{10... | collective-permute-start | bytes 1081352 | tf_op jit(solution)/shard_map/ppermute | solution.py:28
  13.8 18.3 %collective-permute-start.5 = (bf16[4,192,256]{2,1,0:T(8,128)(2,1)S(1)}, bf16[4,192,256]{2,1,0:T(8,128)(2,1)S(1)}, u32[]{:S(2)}, u32[]{:S(2)}) collective-permute-start(bf16[4,192,256]{2,1,0:T(8,128)(2,1)S(1)} %slice.114.refs_0_), channel_id=1, source_target_pairs={{0,6},{2,0},{4,2},{6,4},{1,7},{3,1},{5,3},{7,5},{8,14},{10,8},{12,... | collective-permute-start | bytes 1179656 | tf_op jit(solution)/shard_map/ppermute | solution.py:28
  16.6 12.7 %collective-permute-start.8 = (bf16[2,352,256]{2,1,0:T(8,128)(2,1)S(1)}, bf16[2,352,256]{2,1,0:T(8,128)(2,1)}, u32[]{:S(2)}, u32[]{:S(2)}) collective-permute-start(bf16[2,352,256]{2,1,0:T(8,128)(2,1)S(1)} %copy-done.17), channel_id=1, source_target_pairs={{0,24},{8,0},{16,8},{24,16},{1,25},{9,1},{17,9},{25,17},{2,26},{10... | collective-permute-start | bytes 1081352 | tf_op jit(solution)/shard_map/ppermute | solution.py:28
  17.3 14.6 %collective-permute-start.9 = (bf16[2,352,256]{2,1,0:T(8,128)(2,1)S(1)}, bf16[2,352,256]{2,1,0:T(8,128)(2,1)S(1)}, u32[]{:S(2)}, u32[]{:S(2)}) collective-permute-start(bf16[2,352,256]{2,1,0:T(8,128)(2,1)S(1)} %copy-done.8), channel_id=1, source_target_pairs={{0,1},{1,0},{2,3},{3,2},{4,5},{5,4},{6,7},{7,6},{8,9},{9,8},{10,11... | collective-permute-start | bytes 1081352 | tf_op jit(solution)/shard_map/ppermute | solution.py:32
  19.7 25.4 %collective-permute-start.4 = (bf16[4,192,256]{2,1,0:T(8,128)(2,1)S(1)}, bf16[4,192,256]{2,1,0:T(8,128)(2,1)}, u32[]{:S(2)}, u32[]{:S(2)}) collective-permute-start(bf16[4,192,256]{2,1,0:T(8,128)(2,1)S(1)} %slice.114.refs_0_), channel_id=1, source_target_pairs={{0,4},{2,6},{4,0},{6,2},{1,5},{3,7},{5,1},{7,3},{8,12},{10,14},{12... | collective-permute-start | bytes 1179656 | tf_op jit(solution)/shard_map/ppermute | solution.py:28
  28.0 18.5 %collective-permute-start.3 = (bf16[4,192,256]{2,1,0:T(8,128)(2,1)S(1)}, bf16[4,192,256]{2,1,0:T(8,128)(2,1)}, u32[]{:S(2)}, u32[]{:S(2)}) collective-permute-start(bf16[4,192,256]{2,1,0:T(8,128)(2,1)S(1)} %slice.114.refs_0_), channel_id=1, source_target_pairs={{0,2},{2,4},{4,6},{6,0},{1,3},{3,5},{5,7},{7,1},{8,10},{10,12},{12... | collective-permute-start | bytes 1179656 | tf_op jit(solution)/shard_map/ppermute | solution.py:28
  29.3 19.6 %collective-permute-start.10 = (bf16[2,352,256]{2,1,0:T(8,128)(2,1)}, bf16[2,352,256]{2,1,0:T(8,128)(2,1)}, u32[]{:S(2)}, u32[]{:S(2)}) collective-permute-start(bf16[2,352,256]{2,1,0:T(8,128)(2,1)} %collective-permute-done.6.refs_5_), channel_id=1, source_target_pairs={{0,1},{1,0},{2,3},{3,2},{4,5},{5,4},{6,7},{7,6},{8,9},{9,8},{10,11... | collective-permute-start | bytes 1081352 | tf_op jit(solution)/shard_map/ppermute | solution.py:32
  31.9 16.9 %collective-permute-start.11 = (bf16[2,352,256]{2,1,0:T(8,128)(2,1)}, bf16[2,352,256]{2,1,0:T(8,128)(2,1)}, u32[]{:S(2)}, u32[]{:S(2)}) collective-permute-start(bf16[2,352,256]{2,1,0:T(8,128)(2,1)} %collective-permute-done.7.refs_6_), channel_id=1, source_target_pairs={{0,1},{1,0},{2,3},{3,2},{4,5},{5,4},{6,7},{7,6},{8,9},{9,8},{10,11... | collective-permute-start | bytes 1081352 | tf_op jit(solution)/shard_map/ppermute | solution.py:32
  32.0 16.8 %collective-permute-start.12 = (bf16[2,352,256]{2,1,0:T(8,128)(2,1)}, bf16[2,352,256]{2,1,0:T(8,128)(2,1)}, u32[]{:S(2)}, u32[]{:S(2)}) collective-permute-start(bf16[2,352,256]{2,1,0:T(8,128)(2,1)} %collective-permute-done.8.refs_7_), channel_id=1, source_target_pairs={{0,1},{1,0},{2,3},{3,2},{4,5},{5,4},{6,7},{7,6},{8,9},{9,8},{10,11... | collective-permute-start | bytes 1081352 | tf_op jit(solution)/shard_map/ppermute | solution.py:32
  37.7 62.6 %all-to-all-start.3 = ((bf16[16,3,88,256]{3,2,1,0:T(8,128)(2,1)}), bf16[16,3,88,256]{3,2,1,0:T(8,128)(2,1)S(1)}, u32[]{:S(2)}, u32[]{:S(2)}) async-start(bf16[16,3,88,256]{3,2,1,0:T(8,128)(2,1)} %shard_map.67), calls=%async_computation.3 | async-start | bytes 4325376 | tf_op jit(solution)/shard_map/all_to_all | solution.py:20
  45.1 31.1 %collective-permute-start.19 = (bf16[352,256]{1,0:T(8,128)(2,1)}, bf16[352,256]{1,0:T(8,128)(2,1)}, u32[]{:S(2)}, u32[]{:S(2)}) collective-permute-start(bf16[352,256]{1,0:T(8,128)(2,1)} %get-tuple-element.28), channel_id=1, source_target_pairs={{0,8},{8,16},{16,24},{24,0},{1,9},{9,17},{17,25},{25,1},{2,10},{10... | collective-permute-start | bytes 540680 | tf_op jit(solution)/shard_map/ppermute | solution.py:28
  46.5 37.8 %collective-permute-start.20 = (bf16[352,256]{1,0:T(8,128)(2,1)}, bf16[352,256]{1,0:T(8,128)(2,1)}, u32[]{:S(2)}, u32[]{:S(2)}) collective-permute-start(bf16[352,256]{1,0:T(8,128)(2,1)} %get-tuple-element.29), channel_id=1, source_target_pairs={{0,16},{8,24},{16,0},{24,8},{1,17},{9,25},{17,1},{25,9},{2,18},{10... | collective-permute-start | bytes 540680 | tf_op jit(solution)/shard_map/ppermute | solution.py:28
  56.9 31.1 %collective-permute-start.13 = (bf16[192,1408]{1,0:T(8,128)(2,1)}, bf16[192,1408]{1,0:T(8,128)(2,1)S(1)}, u32[]{:S(2)}, u32[]{:S(2)}) collective-permute-start(bf16[192,1408]{1,0:T(8,128)(2,1)} %get-tuple-element.24), channel_id=1, source_target_pairs={{0,32},{32,64},{64,96},{96,0},{1,33},{33,65},{65,97},{97,1},{2,34}... | collective-permute-start | bytes 1622024 | tf_op jit(solution)/shard_map/ppermute | solution.py:28
  58.1 36.7 %collective-permute-start.14 = (bf16[192,1408]{1,0:T(8,128)(2,1)}, bf16[192,1408]{1,0:T(8,128)(2,1)S(1)}, u32[]{:S(2)}, u32[]{:S(2)}) collective-permute-start(bf16[192,1408]{1,0:T(8,128)(2,1)} %get-tuple-element.25), channel_id=1, source_target_pairs={{0,64},{32,96},{64,0},{96,32},{1,65},{33,97},{65,1},{97,33},{2,66}... | collective-permute-start | bytes 1622024 | tf_op jit(solution)/shard_map/ppermute | solution.py:28
  60.5 34.8 %collective-permute-start.15 = (bf16[192,1408]{1,0:T(8,128)(2,1)}, bf16[192,1408]{1,0:T(8,128)(2,1)S(1)}, u32[]{:S(2)}, u32[]{:S(2)}) collective-permute-start(bf16[192,1408]{1,0:T(8,128)(2,1)} %get-tuple-element.26), channel_id=1, source_target_pairs={{0,96},{32,0},{64,32},{96,64},{1,97},{33,1},{65,33},{97,65},{2,98}... | collective-permute-start | bytes 1622024 | tf_op jit(solution)/shard_map/ppermute | solution.py:28
  84.3 13.7 %collective-permute-start.22 = (bf16[352,256]{1,0:T(8,128)(2,1)}, bf16[352,256]{1,0:T(8,128)(2,1)S(1)}, u32[]{:S(2)}, u32[]{:S(2)}) collective-permute-start(bf16[352,256]{1,0:T(8,128)(2,1)} %get-tuple-element.27.refs_4_), channel_id=1, source_target_pairs={{0,1},{1,0},{2,3},{3,2},{4,5},{5,4},{6,7},{7,6},{8,9},{9,8},{10,11... | collective-permute-start | bytes 540680 | tf_op jit(solution)/shard_map/ppermute | solution.py:32
  86.8 12.1 %collective-permute-start.23 = (bf16[352,256]{1,0:T(8,128)(2,1)}, bf16[352,256]{1,0:T(8,128)(2,1)S(1)}, u32[]{:S(2)}, u32[]{:S(2)}) collective-permute-start(bf16[352,256]{1,0:T(8,128)(2,1)} %collective-permute-done.19.refs_5_), channel_id=1, source_target_pairs={{0,1},{1,0},{2,3},{3,2},{4,5},{5,4},{6,7},{7,6},{8,9},{9,8},{10,11... | collective-permute-start | bytes 540680 | tf_op jit(solution)/shard_map/ppermute | solution.py:32
  88.0 12.3 %collective-permute-start.24 = (bf16[352,256]{1,0:T(8,128)(2,1)}, bf16[352,256]{1,0:T(8,128)(2,1)}, u32[]{:S(2)}, u32[]{:S(2)}) collective-permute-start(bf16[352,256]{1,0:T(8,128)(2,1)} %collective-permute-done.20.refs_6_), channel_id=1, source_target_pairs={{0,1},{1,0},{2,3},{3,2},{4,5},{5,4},{6,7},{7,6},{8,9},{9,8},{10,11... | collective-permute-start | bytes 540680 | tf_op jit(solution)/shard_map/ppermute | solution.py:32
  98.8 16.1 %collective-permute-start.16 = (bf16[192,704]{1,0:T(8,128)(2,1)S(1)}, bf16[192,704]{1,0:T(8,128)(2,1)}, u32[]{:S(2)}, u32[]{:S(2)}) collective-permute-start(bf16[192,704]{1,0:T(8,128)(2,1)S(1)} %fusion.refs_0_), channel_id=1, source_target_pairs={{0,32},{32,64},{64,96},{96,0},{1,33},{33,65},{65,97},{97,1},{2,34}... | collective-permute-start | bytes 811016 | tf_op jit(solution)/shard_map/ppermute | solution.py:28
  100.3 74.9 %collective-permute-start.27 = (bf16[4,4,3,88,256]{4,3,2,1,0:T(8,128)(2,1)S(1)}, bf16[4,4,3,88,256]{4,3,2,1,0:T(8,128)(2,1)}, u32[]{:S(2)}, u32[]{:S(2)}) collective-permute-start(bf16[4,4,3,88,256]{4,3,2,1,0:T(8,128)(2,1)S(1)} %bitcast.49), channel_id=1, source_target_pairs={{0,6},{2,0},{4,2},{6,4},{1,7},{3,1},{5,3},{7,5},{8,14},{10,8},{12,... | collective-permute-start | bytes 6488072 | tf_op jit(solution)/shard_map/ppermute | solution.py:28
  103.8 75.0 %collective-permute-start.26 = (bf16[4,4,3,88,256]{4,3,2,1,0:T(8,128)(2,1)S(1)}, bf16[4,4,3,88,256]{4,3,2,1,0:T(8,128)(2,1)}, u32[]{:S(2)}, u32[]{:S(2)}) collective-permute-start(bf16[4,4,3,88,256]{4,3,2,1,0:T(8,128)(2,1)S(1)} %bitcast.50), channel_id=1, source_target_pairs={{0,2},{2,4},{4,6},{6,0},{1,3},{3,5},{5,7},{7,1},{8,10},{10,12},{12... | collective-permute-start | bytes 6488072 | tf_op jit(solution)/shard_map/ppermute | solution.py:28
  120.1 47.8 %all-to-all-start = ((bf16[16,48,1024]{2,1,0:T(8,128)(2,1)}), bf16[16,48,1024]{2,1,0:T(8,128)(2,1)}, u32[]{:S(2)}, u32[]{:S(2)}) async-start(bf16[16,48,1024]{2,1,0:T(8,128)(2,1)} %bitcast.53), calls=%async_computation | async-start | bytes 3145728 | tf_op jit(solution)/shard_map/all_to_all | solution.py:20
  133.4 75.6 %collective-permute-start.30 = (bf16[4,4,3,88,256]{4,3,2,1,0:T(8,128)(2,1)S(1)}, bf16[4,4,3,88,256]{4,3,2,1,0:T(8,128)(2,1)}, u32[]{:S(2)}, u32[]{:S(2)}) collective-permute-start(bf16[4,4,3,88,256]{4,3,2,1,0:T(8,128)(2,1)S(1)} %bitcast.51), channel_id=1, source_target_pairs={{0,1},{1,0},{2,3},{3,2},{4,5},{5,4},{6,7},{7,6},{8,9},{9,8},{10,11... | collective-permute-start | bytes 6488072 | tf_op jit(solution)/shard_map/ppermute | solution.py:32
  170.4 14.9 %all-to-all-start.1 = ((f32[4,2,48]{2,1,0:T(2,128)}), f32[4,2,48]{2,1,0:T(2,128)S(1)}, u32[]{:S(2)}, u32[]{:S(2)}) async-start(f32[4,2,48]{2,1,0:T(2,128)} %broadcast_in_dim.11), calls=%async_computation.1 | async-start | bytes 8192 | tf_op jit(solution)/shard_map/all_to_all | solution.py:20
  177.5 22.9 %collective-permute-start.29 = (bf16[2,4,3,88,256]{4,3,2,1,0:T(8,128)(2,1)}, bf16[2,4,3,88,256]{4,3,2,1,0:T(8,128)(2,1)}, u32[]{:S(2)}, u32[]{:S(2)}) collective-permute-start(bf16[2,4,3,88,256]{4,3,2,1,0:T(8,128)(2,1)} %slice.124), channel_id=1, source_target_pairs={{0,6},{2,0},{4,2},{6,4},{1,7},{3,1},{5,3},{7,5},{8,14},{10,8},{12,... | collective-permute-start | bytes 3244040 | tf_op jit(solution)/shard_map/ppermute | solution.py:28
  181.2 24.7 %collective-permute-start.28 = (bf16[2,4,3,88,256]{4,3,2,1,0:T(8,128)(2,1)}, bf16[2,4,3,88,256]{4,3,2,1,0:T(8,128)(2,1)}, u32[]{:S(2)}, u32[]{:S(2)}) collective-permute-start(bf16[2,4,3,88,256]{4,3,2,1,0:T(8,128)(2,1)} %slice.123), channel_id=1, source_target_pairs={{0,2},{2,4},{4,6},{6,0},{1,3},{3,5},{5,7},{7,1},{8,10},{10,12},{12... | collective-permute-start | bytes 3244040 | tf_op jit(solution)/shard_map/ppermute | solution.py:28
  181.3 36.1 %collective-permute-start.32 = (bf16[4,4,3,88,256]{4,3,2,1,0:T(8,128)(2,1)}, bf16[4,4,3,88,256]{4,3,2,1,0:T(8,128)(2,1)}, u32[]{:S(2)}, u32[]{:S(2)}) collective-permute-start(bf16[4,4,3,88,256]{4,3,2,1,0:T(8,128)(2,1)} %collective-permute-done.27.refs_2_), channel_id=1, source_target_pairs={{0,1},{1,0},{2,3},{3,2},{4,5},{5,4},{6,7},{7,6},{8,9},{9,8},{10,11... | collective-permute-start | bytes 6488072 | tf_op jit(solution)/shard_map/ppermute | solution.py:32
  185.2 32.3 %collective-permute-start.31 = (bf16[4,4,3,88,256]{4,3,2,1,0:T(8,128)(2,1)}, bf16[4,4,3,88,256]{4,3,2,1,0:T(8,128)(2,1)}, u32[]{:S(2)}, u32[]{:S(2)}) collective-permute-start(bf16[4,4,3,88,256]{4,3,2,1,0:T(8,128)(2,1)} %collective-permute-done.26.refs_1_), channel_id=1, source_target_pairs={{0,1},{1,0},{2,3},{3,2},{4,5},{5,4},{6,7},{7,6},{8,9},{9,8},{10,11... | collective-permute-start | bytes 6488072 | tf_op jit(solution)/shard_map/ppermute | solution.py:32
  186.7 30.7 %all-to-all-start.2 = ((bf16[16,48,1024]{2,1,0:T(8,128)(2,1)}), bf16[16,48,1024]{2,1,0:T(8,128)(2,1)}, u32[]{:S(2)}, u32[]{:S(2)}) async-start(bf16[16,48,1024]{2,1,0:T(8,128)(2,1)} %broadcast_in_dim.12), calls=%async_computation.2 | async-start | bytes 3145728 | tf_op jit(solution)/shard_map/all_to_all | solution.py:20
  200.4 17.1 %collective-permute-start.34 = (bf16[2,4,3,88,256]{4,3,2,1,0:T(8,128)(2,1)}, bf16[2,4,3,88,256]{4,3,2,1,0:T(8,128)(2,1)}, u32[]{:S(2)}, u32[]{:S(2)}) collective-permute-start(bf16[2,4,3,88,256]{4,3,2,1,0:T(8,128)(2,1)} %collective-permute-done.29.refs_4_), channel_id=1, source_target_pairs={{0,1},{1,0},{2,3},{3,2},{4,5},{5,4},{6,7},{7,6},{8,9},{9,8},{10,11... | collective-permute-start | bytes 3244040 | tf_op jit(solution)/shard_map/ppermute | solution.py:32
  205.8 11.6 %collective-permute-start.33 = (bf16[2,4,3,88,256]{4,3,2,1,0:T(8,128)(2,1)}, bf16[2,4,3,88,256]{4,3,2,1,0:T(8,128)(2,1)}, u32[]{:S(2)}, u32[]{:S(2)}) collective-permute-start(bf16[2,4,3,88,256]{4,3,2,1,0:T(8,128)(2,1)} %collective-permute-done.28.refs_3_), channel_id=1, source_target_pairs={{0,1},{1,0},{2,3},{3,2},{4,5},{5,4},{6,7},{7,6},{8,9},{9,8},{10,11... | collective-permute-start | bytes 3244040 | tf_op jit(solution)/shard_map/ppermute | solution.py:32
  (27 other events, 247.8 us)
where the time goes:
time: 285 us; the launch traced here: 284 us
  waiting for transfers between devices  93.2 us (33%)
  starting transfers between devices  88.2 us (31%)
  blocking collectives  43.9 us (15%)
  Pallas kernels  33.6 us (12%)
  local copies, waits for them, and re-layouts  17.1 us (6%)
  other arithmetic  7.29 us (3%)
    ppermute x22, waiting for transfers between devices, shift(): return lax.ppermute(block, axis, [(i, (i + step) % 4) for i in range(4)])  49.7 us
    all_to_all x3, blocking collectives, exchange(): return lax.all_to_all(parts, axes, 0, 0, tiled=True)  43.9 us
    all_to_all x4, waiting for transfers between devices, exchange(): return lax.all_to_all(parts, axes, 0, 0, tiled=True)  42.1 us
    ppermute x22, starting transfers between devices, shift(): return lax.ppermute(block, axis, [(i, (i + step) % 4) for i in range(4)])  35.7 us
    ppermute x14, starting transfers between devices, swap_core(): return lax.ppermute(block, 'c', [(0, 1), (1, 0)])  26.6 us
    all_to_all x4, starting transfers between devices, exchange(): return lax.all_to_all(parts, axes, 0, 0, tiled=True)  26 us
    pallas_call x1, Pallas kernels, block_layer(): pl.pallas_call(block_kernel, out_shape=[sds(16, 4 * n, 256), sds(4 * n, 2...  13.8 us
    unnamed x50, local copies, waits for them, and re-layouts  8.84 us
  transfers between devices with their start and end apart: 40, of which 13 were waited for; matrix products, arithmetic and copies ran while one was open for 7% of the time, Pallas kernels for 7%

commit v1 on v0

v1 whole, which is shorter than its diff:
```python
import jax
import jax.numpy as jnp
from jax import lax
from jax.experimental import pallas as pl
from jax.experimental.pallas import tpu as pltpu
from jax.sharding import Mesh
from jax.sharding import PartitionSpec as P

RESIDUAL = 0.5
EPSILON = 1e-05
WIDTH = 4096.0
BF16 = jnp.bfloat16
F32 = jnp.float32
ANY = pl.BlockSpec(memory_space=pltpu.HBM)
SMEM = pl.BlockSpec(memory_space=pltpu.SMEM)
VMEM = pl.BlockSpec(memory_space=pltpu.VMEM)


def exchange(parts, axes):
    return lax.all_to_all(parts, axes, 0, 0, tiled=True)


def share(block, axes, peers):
    return exchange(jnp.broadcast_to(block[None], (peers, *block.shape)), axes)


def shift(block, axis, step):
    return lax.ppermute(block, axis, [(i, (i + step) % 4) for i in range(4)])


def in_vmem(value):
    return pltpu.with_memory_space_constraint(value, pltpu.VMEM)


def swap_core(block):
    return lax.ppermute(block, "c", [(0, 1), (1, 0)])


def share4(block, axis):
    return exchange4([block] * 4, axis)


def exchange4(parts, axis):
    got = [parts[0]]
    for step in (1, 2, 3):
        got.append(shift(parts[step], axis, step))
    return got


def behind(own, k):
    return lax.rem(own + 4 - k, 4)


def dot_nt(a, b):
    return lax.dot_general(a, b, (((1,), (1,)), ((), ())), preferred_element_type=F32)


def sds(*shape):
    return jax.ShapeDtypeStruct(shape, BF16)


def run_copies(copies, sems):
    started = []
    for i, (src, dst) in enumerate(copies):
        copy = pltpu.make_async_copy(src, dst, sems.at[i])
        copy.start()
        started.append(copy)
    return started


def turn_kernel(gate_ref, up_ref, down_ref, out):
    rows = out.shape[2]
    for g, ref in enumerate((gate_ref, up_ref)):
        turned = ref[0].T
        for p in range(4):
            out[p, g] = turned[p * rows : p * rows + rows]
    for p in range(4):
        out[p, 2] = down_ref[0, p * rows : p * rows + rows]


def turn(layer, gate, up, down):
    rows = gate.shape[2] // 4
    pick = lambda i: (layer, 0, 0)
    return pl.pallas_call(
        turn_kernel,
        out_shape=sds(4, 3, rows, 256),
        in_specs=[
            pl.BlockSpec((1, *gate.shape[1:]), pick),
            pl.BlockSpec((1, *up.shape[1:]), pick),
            pl.BlockSpec((1, *down.shape[1:]), pick),
        ],
        out_specs=VMEM,
        grid=(1,),
    )(gate, up, down)


def pack_kernel(place_ref, gate_ref, up_ref, down_ref, *rest):
    outs, turned = rest[:-1], rest[-1]
    own = place_ref[1]
    cols = gate_ref.shape[2]
    for g, ref in enumerate((gate_ref, up_ref)):
        for at in range(0, cols, 128):
            turned[g, at : at + 128, :] = ref[0, :, at : at + 128].T
    rows = cols // 4
    for k in range(4):
        at = pl.ds(pl.multiple_of(lax.rem(own + k, 4) * rows, 16), rows)
        outs[k][0:2] = turned[:, at, :]
        outs[4 + k][...] = down_ref[0, at, :]


def pack(place, layer, gate, up, down):
    rows = gate.shape[2] // 4
    out_shape = [sds(2, rows, 256)] * 4 + [sds(rows, 256)] * 4
    pick = lambda i: (layer, 0, 0)
    return pl.pallas_call(
        pack_kernel,
        out_shape=out_shape,
        in_specs=[
            SMEM,
            pl.BlockSpec((1, *gate.shape[1:]), pick),
            pl.BlockSpec((1, *up.shape[1:]), pick),
            pl.BlockSpec((1, *down.shape[1:]), pick),
        ],
        out_specs=[VMEM] * len(out_shape),
        grid=(1,),
        scratch_shapes=[pltpu.VMEM((2, gate.shape[2], 256), BF16)],
    )(place, gate, up, down)


def gate_up_kernel(place_ref, *refs):
    rows, mine, theirs, outs, own_out = refs[:4], refs[4:8], refs[8:12], refs[12:19], refs[19]
    stream, weights, partial, sems, out_sems = refs[20:]
    z, x, y = place_ref[0], place_ref[1], place_ref[2]
    n, half = rows[0].shape[1], mine[0].shape[1]
    block = own_out.shape[0]
    lanes = [pl.ds(pl.multiple_of(behind(x, m) * 256, 256), 256) for m in range(4)]
    copies = []
    for j in range(4):
        for m in range(4):
            copies.append((rows[j].at[m], stream.at[behind(y, j), :, lanes[m]]))
    for g in range(2):
        for m in range(4):
            for s, piece in enumerate((mine[m], theirs[m])):
                at = (2 * g + s) * half
                copies.append((piece.at[g], weights.at[at : at + half, lanes[m]]))
    started = run_copies(copies, sems)
    for copy in started[:24]:
        copy.wait()
    own_out[...] = stream[x, pl.ds(pl.multiple_of(y * block, 16), block), :]
    whole = stream[...].reshape(4 * n, 1024)
    for g in range(2):
        at = slice(2 * g * half, 2 * g * half + 2 * half)
        if g == 1:
            for copy in started[24:]:
                copy.wait()
        partial[:, :, at] = dot_nt(whole, weights[at]).astype(BF16).reshape(4, n, 2 * half)
    copies = [(partial.at[z], outs[0])]
    for k in range(1, 4):
        for h in range(2):
            src = partial.at[lax.rem(z + k, 4), h * n // 2 : h * n // 2 + n // 2]
            copies.append((src, outs[2 * k - 1 + h]))
    for copy in run_copies(copies, out_sems):
        copy.wait()


def gate_up(place, rows, mine, theirs):
    n, half = rows[0].shape[1], mine[0].shape[1]
    return pl.pallas_call(
        gate_up_kernel,
        out_shape=[sds(n, 4 * half)] + [sds(n // 2, 4 * half)] * 6 + [sds(n // 4, 1024)],
        in_specs=[SMEM] + [ANY] * 12,
        out_specs=[ANY] * 7 + [VMEM],
        scratch_shapes=[
            pltpu.VMEM((4, n, 1024), BF16),
            pltpu.VMEM((4 * half, 1024), BF16),
            pltpu.VMEM((4, n, 4 * half), BF16),
            pltpu.SemaphoreType.DMA((32,)),
            pltpu.SemaphoreType.DMA((7,)),
        ],
    )(place, *rows, *mine, *theirs)


def down_kernel(place_ref, *refs):
    hidden, mine, theirs, out = refs[:4], refs[4:8], refs[8:12], refs[12]
    rows, weights, sems = refs[13:]
    z, x = place_ref[0], place_ref[1]
    half = mine[0].shape[0]
    copies = []
    for m in range(4):
        lanes = pl.ds(pl.multiple_of(behind(x, m) * 256, 256), 256)
        copies.append((mine[m], weights.at[:half, lanes]))
        copies.append((theirs[m], weights.at[half:, lanes]))
    for k in range(4):
        copies.append((hidden[k], rows.at[behind(z, k)]))
    for copy in run_copies(copies, sems):
        copy.wait()
    n, cols = rows.shape[1:]
    out[...] = jnp.dot(rows[...].reshape(4 * n, cols), weights[...], preferred_element_type=F32).astype(BF16)


def down(place, hidden, mine, theirs):
    n, cols = hidden[0].shape
    return pl.pallas_call(
        down_kernel,
        out_shape=sds(4 * n, 1024),
        in_specs=[SMEM] + [ANY] * 12,
        out_specs=VMEM,
        scratch_shapes=[
            pltpu.VMEM((4, n, cols), BF16),
            pltpu.VMEM((cols, 1024), BF16),
            pltpu.SemaphoreType.DMA((12,)),
        ],
    )(place, *hidden, *mine, *theirs)


def parts_of(value):
    high = value.astype(BF16)
    rest = value - high.astype(F32)
    middle = rest.astype(BF16)
    return high, middle, (rest - middle.astype(F32)).astype(BF16)


def norm_kernel(branch, own, out, message, sems):
    mixed = RESIDUAL * own[...].astype(F32)
    for i in range(branch.shape[0]):
        mixed += branch[i].astype(F32)
    cols = mixed.shape[1]
    mean = mixed.sum(axis=1, keepdims=True) / cols
    mixed -= mean
    message[:, :cols] = mixed.astype(BF16)
    lane = lax.broadcasted_iota(jnp.int32, (mixed.shape[0], 128), 1)
    tail = jnp.zeros((mixed.shape[0], 128), F32)
    for i, part in enumerate(parts_of(mean) + parts_of((mixed * mixed).sum(axis=1, keepdims=True))):
        tail = jnp.where(lane == i, part.astype(F32), tail)
    message[:, cols:] = tail.astype(BF16)
    for copy in run_copies([(message, out.at[i]) for i in range(out.shape[0])], sems):
        copy.wait()


def norm_message(branch, own):
    n, cols = own.shape
    return pl.pallas_call(
        norm_kernel,
        out_shape=sds(16, n, cols + 128),
        in_specs=[VMEM] * 2,
        out_specs=ANY,
        scratch_shapes=[pltpu.VMEM((n, cols + 128), BF16), pltpu.SemaphoreType.DMA((16,))],
        compiler_params=pltpu.CompilerParams(vmem_limit_bytes=16 << 20),
    )(branch, own)


def block_kernel(place_ref, rows_ref, affine_ref, *refs):
    pieces, out, own_out = refs[:16], refs[16], refs[17]
    stream, tails, weights, row_sems, sems = refs[18:]
    z, x, y = place_ref[0], place_ref[1], place_ref[2]
    n, rows = rows_ref.shape[1], pieces[0].shape[2]
    copies = []
    for i in range(16):
        at = slice(i % 4 * n, i % 4 * n + n)
        copies.append((rows_ref.at[i, :, :1024], stream.at[at, i // 4 * 1024 : i // 4 * 1024 + 1024]))
        copies.append((rows_ref.at[i, :, 1024:], tails.at[i // 4, at]))
    row_copies = run_copies(copies, row_sems)

    def load(g):
        for i, piece in enumerate(pieces):
            at, step, first = i // 8 * rows, (0, 1, 3, 2)[i % 8 // 2], i % 2 * 2
            for q in range(2):
                lanes = pl.ds(pl.multiple_of((first + q) * 1024 + behind(x, step) * 256, 256), 256)
                pltpu.make_async_copy(piece.at[q, g], weights.at[g, at : at + rows, lanes], sems.at[g]).start()

    def loaded(g):
        pltpu.make_async_copy(weights.at[g], weights.at[g], sems.at[g]).wait()

    load(0)
    for copy in row_copies:
        copy.wait()
    means, squares = [], []
    for q in range(4):
        tail = tails[q].astype(F32)
        means.append(tail[:, 0:1] + tail[:, 1:2] + tail[:, 2:3])
        squares.append(tail[:, 3:4] + tail[:, 4:5] + tail[:, 5:6])
    mean = sum(means) / 4
    square = sum(squares) + sum((m - mean) * (m - mean) for m in means) * 1024
    scale = lax.rsqrt(square / WIDTH + EPSILON)
    for q in range(4):
        at = slice(q * 1024, q * 1024 + 1024)
        value = (stream[:, at].astype(F32) + (means[q] - mean)) * scale
        stream[:, at] = (value * affine_ref[0:1, at] + affine_ref[1:2, at]).astype(BF16)
    own_out[...] = stream[pl.ds(pl.multiple_of(y * n, 16), n), pl.ds(pl.multiple_of(z * 1024, 1024), 1024)]
    loaded(0)
    load(1)
    load(2)
    gate = dot_nt(stream[...], weights[0])
    gate = gate * jax.nn.sigmoid(gate)
    loaded(1)
    hidden = (gate * dot_nt(stream[...], weights[1])).astype(BF16)
    loaded(2)
    for q in range(4):
        part = jnp.dot(hidden, weights[2, :, q * 1024 : q * 1024 + 1024], preferred_element_type=F32)
        out[4 * q : 4 * q + 4] = part.astype(BF16).reshape(4, n, 1024)


def block_layer(place, rows, affine, pieces):
    n, half = rows.shape[1], pieces[0].shape[2]
    return pl.pallas_call(
        block_kernel,
        out_shape=[sds(16, n, 1024), sds(n, 1024)],
        in_specs=[SMEM, VMEM, VMEM] + [ANY] * 16,
        out_specs=[VMEM] * 2,
        scratch_shapes=[
            pltpu.VMEM((4 * n, 4096), BF16),
            pltpu.VMEM((4, 4 * n, 128), BF16),
            pltpu.VMEM((3, 2 * half, 4096), BF16),
            pltpu.SemaphoreType.DMA((32,)),
            pltpu.SemaphoreType.DMA((3,)),
        ],
        compiler_params=pltpu.CompilerParams(vmem_limit_bytes=40 << 20),
    )(place, rows, affine, *pieces)


def normed(mixed, row_sum, row_squares, gain, shift_row):
    mean = row_sum / WIDTH
    var = row_squares / WIDTH - mean * mean
    out = (mixed - mean[:, None]) * lax.rsqrt(var + EPSILON)[:, None]
    return (out * gain + shift_row).astype(BF16)


def row_stats(mixed):
    return jnp.stack((mixed.sum(axis=1), (mixed * mixed).sum(axis=1)))


def in_order(pieces, own):
    back = jnp.concatenate((pieces[:1], pieces[3:4], pieces[2:3], pieces[1:2]))
    return lax.dynamic_slice_in_dim(jnp.concatenate((back, back[:3])), (4 - own) % 4, 4, 0)


def thirds(values):
    high = lax.reduce_precision(values, 8, 7)
    middle = lax.reduce_precision(values - high, 8, 7)
    low = values - high - middle
    return jnp.concatenate((high, middle, low)).astype(BF16)


def per_device(inputs, gate_weight, up_weight, down_weight, norm_gain, norm_shift):
    z, x, y, c = (lax.axis_index(a) for a in ("z", "x", "y", "c"))
    place = jnp.stack((z, x, y, c)).astype(jnp.int32)
    half = inputs.shape[0] // 2
    quarter = half // 4
    block = half // 16
    cols = gate_weight.shape[2] // 2

    mine = lax.dynamic_slice_in_dim(inputs, c * half + y * quarter, quarter, 0)
    affine = thirds(jnp.concatenate((norm_gain, norm_shift)))
    mine = jnp.concatenate((mine, affine, jnp.zeros((4, 256), BF16)))
    mine = jnp.stack(share4(mine, "x"))
    rows = share4(mine[:, :quarter], "y")

    packed = pack(place, 0, gate_weight, up_weight, down_weight)
    gu0 = exchange4(packed[:4], "x")
    down0 = exchange4(packed[4:], "x")
    gu0_core = [swap_core(w) for w in gu0]
    down0_core = [swap_core(w) for w in down0]

    w1 = turn(1, gate_weight, up_weight, down_weight)
    w1 = exchange(w1, "z")
    w1 = [w1[:2], w1[2:]]
    near, far = [], []
    for h in range(2):
        near.append(shift(w1[h], "x", 1))
        far.append(shift(w1[h], "x", 3))
    across = [shift(near[0], "x", 1)]
    across.append(shift(far[1], "x", 3))
    w1 = [*w1, *near, *far, *across]
    w1_core = []
    for w in w1:
        w1_core.append(swap_core(w))

    sums, next_a, next_b, over_a, over_b, prev_a, prev_b, own = gate_up(place, rows, gu0, gu0_core)
    over_a = shift(over_a, "z", 1)
    over_b = shift(over_b, "z", 3)
    next_b = shift(next_b, "z", 1)
    prev_a = shift(prev_a, "z", 3)
    next_a = shift((next_a.astype(F32) + over_a.astype(F32)).astype(BF16), "z", 1)
    prev_b = shift((prev_b.astype(F32) + over_b.astype(F32)).astype(BF16), "z", 3)
    sums = sums.astype(F32)
    sums = jnp.concatenate(
        (
            sums[: quarter // 2] + (prev_a.astype(F32) + next_a.astype(F32)),
            sums[quarter // 2 :] + (next_b.astype(F32) + prev_b.astype(F32)),
        )
    )
    hidden = (jax.nn.silu(sums[:, :cols]) * sums[:, cols:]).astype(BF16)
    hidden = share4(hidden, "z")
    partial = down(place, hidden, down0, down0_core)
    branch = exchange(partial.reshape(16, block, 1024), ("x", "y"))
    affine = in_order(mine[:, quarter : quarter + 12].astype(F32), x)
    affine = (affine[:, :4] + affine[:, 4:8]) + affine[:, 8:]
    affine = affine.transpose(1, 0, 2).reshape(4, 1024)
    spread = in_order(jnp.stack(share4(affine[::2], "z")), z)
    spread = spread.transpose(1, 0, 2).reshape(2, 4096)
    message = norm_message(in_vmem(branch), own)
    stream = in_vmem(exchange(message, ("z", "y")))

    parts, own = block_layer(place, stream, spread, w1 + w1_core)
    branch = exchange(parts, ("z", "y")).astype(F32).sum(axis=0)
    mixed = RESIDUAL * own.astype(F32) + branch
    stats = share(row_stats(mixed), "z", 4).sum(axis=0)
    out = normed(mixed, stats[0], stats[1], affine[1], affine[3])
    parts = jnp.broadcast_to(out.reshape(block, 4, 1, 256).transpose(1, 2, 0, 3), (4, 4, block, 256))
    ours = exchange(parts.reshape(16, block, 256), ("x", "y")).reshape(half, 256)
    theirs = swap_core(ours)
    return jnp.where(c == 0, jnp.concatenate((ours, theirs)), jnp.concatenate((theirs, ours)))


def solution(mesh):
    finer = Mesh(mesh.devices.reshape(4, 4, 4, 2), ("z", "x", "y", "c"))
    ra, cb = ("z", "x"), ("y", "c")
    in_specs = (
        P(None, ra),
        P(None, ra, cb),
        P(None, ra, cb),
        P(None, cb, ra),
        P(None, ra),
        P(None, ra),
    )


    return jax.shard_map(per_device, mesh=finer, in_specs=in_specs, out_specs=P(None, ra), check_vma=False)
```

time: 285 us -> 282 us (0.989)
  blocking collectives: 43.9 us -> 12.3 us
  starting transfers between devices: 88.2 us -> 111 us
  waiting for transfers between devices: 93.2 us -> 101 us
    all_to_all x3 -> x1, blocking collectives: 43.9 us -> 12.3 us  [exchange(): return lax.all_to_all(parts, axes, 0, 0, tiled=True)]
    ppermute x22 -> x30, waiting for transfers between devices: 49.7 us -> 66.6 us  [shift(): return lax.ppermute(block, axis, [(i, (i + step) % 4) for i in range(4)])]
    all_to_all x4 -> x5, waiting for transfers between devices: 42.1 us -> 29 us  [exchange(): return lax.all_to_all(parts, axes, 0, 0, tiled=True)]
    ppermute x22 -> x30, starting transfers between devices: 35.7 us -> 47.7 us  [shift(): return lax.ppermute(block, axis, [(i, (i + step) % 4) for i in range(4)])]
    ppermute x14 -> x17, starting transfers between devices: 26.6 us -> 38.5 us  [swap_core(): return lax.ppermute(block, 'c', [(0, 1), (1, 0)])]
    ppermute x14 -> x17, waiting for transfers between devices: 1.38 us -> 5.67 us  [swap_core(): return lax.ppermute(block, 'c', [(0, 1), (1, 0)])]
    slice x4 -> x3, local copies, waits for them, and re-layouts: 5.44 us -> 2.26 us  [the longest x1 1.51 us: per_device(): w1 = [w1[:2], w1[2:]]]
    unnamed x50 -> x68, local copies, waits for them, and re-layouts: 8.84 us -> 10.4 us
  transfers between devices with their start and end apart: 40 -> 52, of which waited for: 13 -> 20; matrix products, arithmetic and copies ran while one was open for 7% -> 5% of each run, Pallas kernels for 7% -> 5%
where the time goes in v1:
time: 282 us; the launch traced here: 280 us
  starting transfers between devices  111 us (39%)
  waiting for transfers between devices  101 us (36%)
  Pallas kernels  33.4 us (12%)
  local copies, waits for them, and re-layouts  14.9 us (5%)
  blocking collectives  12.3 us (4%)
  other arithmetic  7.07 us (3%)
    ppermute x30, waiting for transfers between devices, shift(): return lax.ppermute(block, axis, [(i, (i + step) % 4) for i in range(4)])  66.6 us
    ppermute x30, starting transfers between devices, shift(): return lax.ppermute(block, axis, [(i, (i + step) % 4) for i in range(4)])  47.7 us
    ppermute x17, starting transfers between devices, swap_core(): return lax.ppermute(block, 'c', [(0, 1), (1, 0)])  38.5 us
    all_to_all x5, waiting for transfers between devices, exchange(): return lax.all_to_all(parts, axes, 0, 0, tiled=True)  29 us
    all_to_all x5, starting transfers between devices, exchange(): return lax.all_to_all(parts, axes, 0, 0, tiled=True)  24.7 us
    all_to_all x1, blocking collectives, exchange(): return lax.all_to_all(parts, axes, 0, 0, tiled=True)  12.3 us
    pallas_call x1, Pallas kernels, block_layer(): pl.pallas_call(block_kernel, out_shape=[sds(16, n, 1024), sds(n, 1024)],...  11.4 us
    unnamed x68, local copies, waits for them, and re-layouts  10.4 us
  transfers between devices with their start and end apart: 52, of which 20 were waited for; matrix products, arithmetic and copies ran while one was open for 5% of the time, Pallas kernels for 5%

profile of v1, /device:TPU:1, one launch (start us, length us, event | category | flops | bytes accessed | tf_op | source)
XLA Modules:
  0.0 280.3 jit_solution(8135167200854297727)
XLA Ops:
  1.9 3.3 %collective-permute-start.2 = (bf16[208,256]{1,0:T(8,128)(2,1)S(1)}, bf16[208,256]{1,0:T(8,128)(2,1)S(1)}, u32[]{:S(2)}, u32[]{:S(2)}) collective-permute-start(bf16[208,256]{1,0:T(8,128)(2,1)S(1)} %concatenate.33), channel_id=1, source_target_pairs={{0,24},{8,0},{16,8},{24,16},{1,25},{9,1},{17,9},{25,17},{2,26},{10... | collective-permute-start | bytes 319496 | tf_op jit(solution)/shard_map/ppermute | solution.py:28
  7.0 3.3 %shard_map.64 = (bf16[2,352,256]{2,1,0:T(8,128)(2,1)}, bf16[2,352,256]{2,1,0:T(8,128)(2,1)}, bf16[2,352,256]{2,1,0:T(8,128)(2,1)}, bf16[2,352,256]{2,1,0:T(8,128...) custom-call(s32[4]{0:T(128)} %pad_add_fusion.place_ref, ...), custom_call_target="tpu_custom_call" | custom-call | tf_op jit(solution)/shard_map/pallas_call | solution.py:115
  20.2 2.9 %collective-permute-start.4 = (bf16[4,192,256]{2,1,0:T(8,128)(2,1)S(1)}, bf16[4,192,256]{2,1,0:T(8,128)(2,1)S(1)}, u32[]{:S(2)}, u32[]{:S(2)}) collective-permute-start(bf16[4,192,256]{2,1,0:T(8,128)(2,1)S(1)} %slice.86.refs_0_), channel_id=1, source_target_pairs={{0,4},{2,6},{4,0},{6,2},{1,5},{3,7},{5,1},{7,3},{8,12},{10,14},{12... | collective-permute-start | bytes 1179656 | tf_op jit(solution)/shard_map/ppermute | solution.py:28
  23.1 5.4 %collective-permute-done.7.refs_6_ = bf16[2,352,256]{2,1,0:T(8,128)(2,1)S(1)} collective-permute-done((bf16[2,352,256]{2,1,0:T(8,128)(2,1)}, bf16[2,352,256]{2,1,0:T(8,128)(2,1)S(1)}, u32[]{:S(2)}, u32[]{:S(2)}) %collective-permute-start.7) | collective-permute-done | bytes 360480 | tf_op jit(solution)/shard_map/ppermute | solution.py:28
  28.5 2.7 collective-permute-start.5
  34.5 5.3 %collective-permute-done.5.refs_3_ = bf16[4,192,256]{2,1,0:T(8,128)(2,1)S(1)} collective-permute-done((bf16[4,192,256]{2,1,0:T(8,128)(2,1)S(1)}, bf16[4,192,256]{2,1,0:T(8,128)(2,1)S(1)}, u32[]{:S(2)}, u32[]{:S(2)}) %collective-permute-start.5) | collective-permute-done | bytes 393248 | tf_op jit(solution)/shard_map/ppermute | solution.py:28
  41.3 8.6 %shard_map.65 = (bf16[192,1408]{1,0:T(8,128)(2,1)}, bf16[96,1408]{1,0:T(8,128)(2,1)}, bf16[96,1408]{1,0:T(8,128)(2,1)}, bf16[96,1408]{1,0:T(8,128)(2,1)}, bf16[9...) custom-call(s32[4]{0:T(128)} %pad_add_fusion.place_ref, ...), custom_call_target="tpu_custom_call" | custom-call | tf_op jit(solution)/shard_map/pallas_call | solution.py:168
  52.8 3.3 %shard_map.68 = bf16[4,3,352,256]{3,2,1,0:T(8,128)(2,1)} custom-call(bf16[2,256,1408]{2,1,0:T(8,128)(2,1)} %gate_ref.3, bf16[2,256,1408]{2,1,0:T(8,128)(2,1)} %up_ref.3, bf16[2,1408,256]{2,1,0:T(8,128)(2,1)} %down_ref.3), custom_call_target="tpu_custom_call" | custom-call | tf_op jit(solution)/shard_map/pallas_call | solution.py:84
  56.1 4.6 %all-to-all-start.2 = ((bf16[4,3,352,256]{3,2,1,0:T(8,128)(2,1)}), bf16[4,3,352,256]{3,2,1,0:T(8,128)(2,1)S(1)}, u32[]{:S(2)}, u32[]{:S(2)}) async-start(bf16[4,3,352,256]{3,2,1,0:T(8,128)(2,1)} %shard_map.68), calls=%async_computation.2 | async-start | bytes 4325376 | tf_op jit(solution)/shard_map/all_to_all | solution.py:20
  60.7 2.7 collective-permute-start.13
  66.1 27.7 %collective-permute-done.17 = bf16[96,1408]{1,0:T(8,128)(2,1)S(1)} collective-permute-done((bf16[96,1408]{1,0:T(8,128)(2,1)}, bf16[96,1408]{1,0:T(8,128)(2,1)S(1)}, u32[]{:S(2)}, u32[]{:S(2)}) %collective-permute-start.17) | collective-permute-done | bytes 270368 | tf_op jit(solution)/shard_map/ppermute | solution.py:28
  97.2 3.1 %collective-permute-start.24 = (bf16[352,256]{1,0:T(8,128)(2,1)}, bf16[352,256]{1,0:T(8,128)(2,1)}, u32[]{:S(2)}, u32[]{:S(2)}) collective-permute-start(bf16[352,256]{1,0:T(8,128)(2,1)} %get-tuple-element.37), channel_id=1, source_target_pairs={{0,24},{8,0},{16,8},{24,16},{1,25},{9,1},{17,9},{25,17},{2,26},{10... | collective-permute-start | bytes 540680 | tf_op jit(solution)/shard_map/ppermute | solution.py:28
  103.3 6.1 %collective-permute-start.25 = (bf16[352,256]{1,0:T(8,128)(2,1)S(1)}, bf16[352,256]{1,0:T(8,128)(2,1)S(1)}, u32[]{:S(2)}, u32[]{:S(2)}) collective-permute-start(bf16[352,256]{1,0:T(8,128)(2,1)S(1)} %copy-done.20), channel_id=1, source_target_pairs={{0,1},{1,0},{2,3},{3,2},{4,5},{5,4},{6,7},{7,6},{8,9},{9,8},{10,11... | collective-permute-start | bytes 540680 | tf_op jit(solution)/shard_map/ppermute | solution.py:36
  121.7 4.3 %collective-permute-done.20.refs_2_ = bf16[192,704]{1,0:T(8,128)(2,1)} collective-permute-done((bf16[192,704]{1,0:T(8,128)(2,1)S(1)}, bf16[192,704]{1,0:T(8,128)(2,1)}, u32[]{:S(2)}, u32[]{:S(2)}) %collective-permute-start.20) | collective-permute-done | bytes 270368 | tf_op jit(solution)/shard_map/ppermute | solution.py:28
  128.7 5.1 %shard_map.66 = bf16[768,1024]{1,0:T(8,128)(2,1)} custom-call(s32[4]{0:T(128)} %pad_add_fusion.place_ref, bf16[192,704]{1,0:T(8,128)(2,1)} %copy-done.6, bf16[192,704]{1,0:T(8,128)(2,1)} %collective-permute-done.19.refs_1_, bf16[192,704]{1,0:T(8,128)(2,1)} %collective-permute-done.20.refs_2_, bf16[192,704]{1,0:T(8,128)(2,1)} %collective-permute-done.21.refs_3_, ...), custom_call_target="tpu_custom_call" | custom-call | tf_op jit(solution)/shard_map/pallas_call | solution.py:203
  133.8 5.3 %all-to-all-start = ((bf16[16,48,1024]{2,1,0:T(8,128)(2,1)}), bf16[16,48,1024]{2,1,0:T(8,128)(2,1)S(1)}, u32[]{:S(2)}, u32[]{:S(2)}) async-start(bf16[16,48,1024]{2,1,0:T(8,128)(2,1)} %bitcast.40), calls=%async_computation | async-start | bytes 3145728 | tf_op jit(solution)/shard_map/all_to_all | solution.py:20
  146.6 2.7 collective-permute-start.29
  155.6 3.3 %collective-permute-done.31 = f32[2,1024]{1,0:T(2,128)S(1)} collective-permute-done((f32[2,1024]{1,0:T(2,128)S(1)}, f32[2,1024]{1,0:T(2,128)S(1)}, u32[]{:S(2)}, u32[]{:S(2)}) %collective-permute-start.31) | collective-permute-done | bytes 8224 | tf_op jit(solution)/shard_map/ppermute | solution.py:28
  158.8 4.5 %collective-permute-start.38 = (bf16[2,3,352,256]{3,2,1,0:T(8,128)(2,1)}, bf16[2,3,352,256]{3,2,1,0:T(8,128)(2,1)}, u32[]{:S(2)}, u32[]{:S(2)}) collective-permute-start(bf16[2,3,352,256]{3,2,1,0:T(8,128)(2,1)} %get-tuple-element.44.refs_0_), channel_id=1, source_target_pairs={{0,1},{1,0},{2,3},{3,2},{4,5},{5,4},{6,7},{7,6},{8,9},{9,8},{10,11... | collective-permute-start | bytes 3244040 | tf_op jit(solution)/shard_map/ppermute | solution.py:36
  165.7 2.7 collective-permute-start.37
  168.4 8.8 %collective-permute-start.40 = (bf16[2,3,352,256]{3,2,1,0:T(8,128)(2,1)}, bf16[2,3,352,256]{3,2,1,0:T(8,128)(2,1)}, u32[]{:S(2)}, u32[]{:S(2)}) collective-permute-start(bf16[2,3,352,256]{3,2,1,0:T(8,128)(2,1)} %collective-permute-done.32.refs_2_), channel_id=1, source_target_pairs={{0,1},{1,0},{2,3},{3,2},{4,5},{5,4},{6,7},{7,6},{8,9},{9,8},{10,11... | collective-permute-start | bytes 3244040 | tf_op jit(solution)/shard_map/ppermute | solution.py:36
  177.2 5.4 %all-to-all-done.branch = bf16[16,48,1024]{2,1,0:T(8,128)(2,1)S(1)} async-done(((bf16[16,48,1024]{2,1,0:T(8,128)(2,1)}), bf16[16,48,1024]{2,1,0:T(8,128)(2,1)S(1)}, u32[]{:S(2)}, u32[]{:S(2)}) %all-to-all-start) | async-done | bytes 1572896 | tf_op jit(solution)/shard_map/all_to_all | solution.py:20
  184.4 6.0 %all-to-all-start.1 = ((bf16[16,48,1152]{2,1,0:T(8,128)(2,1)}), bf16[16,48,1152]{2,1,0:T(8,128)(2,1)S(1)}, u32[]{:S(2)}, u32[]{:S(2)}) async-start(bf16[16,48,1152]{2,1,0:T(8,128)(2,1)} %shard_map.67), calls=%async_computation.1 | async-start | bytes 3538944 | tf_op jit(solution)/shard_map/all_to_all | solution.py:20
  190.4 4.8 %collective-permute-start.43 = (bf16[2,3,352,256]{3,2,1,0:T(8,128)(2,1)}, bf16[2,3,352,256]{3,2,1,0:T(8,128)(2,1)}, u32[]{:S(2)}, u32[]{:S(2)}) collective-permute-start(bf16[2,3,352,256]{3,2,1,0:T(8,128)(2,1)} %collective-permute-done.35.refs_5_), channel_id=1, source_target_pairs={{0,1},{1,0},{2,3},{3,2},{4,5},{5,4},{6,7},{7,6},{8,9},{9,8},{10,11... | collective-permute-start | bytes 3244040 | tf_op jit(solution)/shard_map/ppermute | solution.py:36
  195.3 10.4 %collective-permute-done.36.refs_6_ = bf16[2,3,352,256]{3,2,1,0:T(8,128)(2,1)} collective-permute-done((bf16[2,3,352,256]{3,2,1,0:T(8,128)(2,1)}, bf16[2,3,352,256]{3,2,1,0:T(8,128)(2,1)}, u32[]{:S(2)}, u32[]{:S(2)}) %collective-permute-start.36) | collective-permute-done | bytes 1081376 | tf_op jit(solution)/shard_map/ppermute | solution.py:28
  214.8 11.4 %shard_map.69 = (bf16[16,48,1024]{2,1,0:T(8,128)(2,1)}, bf16[48,1024]{1,0:T(8,128)(2,1)S(1)}) custom-call(s32[4]{0:T(128)S(1)} %copy-done.4, bf16[16,48,1152]{2,1,0:T(8,128)(2,1)S(1)} %all-to-all-done.1.rows_ref, f32[2,4096]{1,0:T(2,128)S(1)} %bitcast.39, bf16[2,3,352,256]{3,2,1,0:T(8,128)(2,1)} %get-tuple-element.44.refs_0_, ...), custom_call_target="tpu_custom_call" | custom-call | tf_op jit(solution)/shard_map/pallas_call | solution.py:305
  226.2 5.0 %all-to-all-start.3 = ((bf16[16,48,1024]{2,1,0:T(8,128)(2,1)}), bf16[16,48,1024]{2,1,0:T(8,128)(2,1)S(1)}, u32[]{:S(2)}, u32[]{:S(2)}) async-start(bf16[16,48,1024]{2,1,0:T(8,128)(2,1)} %get-tuple-element.40), calls=%async_computation.3 | async-start | bytes 3145728 | tf_op jit(solution)/shard_map/all_to_all | solution.py:20
  232.1 18.7 %all-to-all-done.3 = bf16[16,48,1024]{2,1,0:T(8,128)(2,1)S(1)} async-done(((bf16[16,48,1024]{2,1,0:T(8,128)(2,1)}), bf16[16,48,1024]{2,1,0:T(8,128)(2,1)S(1)}, u32[]{:S(2)}, u32[]{:S(2)}) %all-to-all-start.3) | async-done | bytes 1572896 | tf_op jit(solution)/shard_map/all_to_all | solution.py:20
  251.9 3.8 %all-to-all-start.4 = ((f32[4,2,48]{2,1,0:T(2,128)}), f32[4,2,48]{2,1,0:T(2,128)S(1)}, u32[]{:S(2)}, u32[]{:S(2)}) async-start(f32[4,2,48]{2,1,0:T(2,128)} %broadcast_in_dim.9), calls=%async_computation.4 | async-start | bytes 8192 | tf_op jit(solution)/shard_map/all_to_all | solution.py:20
  255.7 4.1 %all-to-all-done.4 = f32[4,2,48]{2,1,0:T(2,128)S(1)} async-done(((f32[4,2,48]{2,1,0:T(2,128)}), f32[4,2,48]{2,1,0:T(2,128)S(1)}, u32[]{:S(2)}, u32[]{:S(2)}) %all-to-all-start.4) | async-done | bytes 1568 | tf_op jit(solution)/shard_map/all_to_all | solution.py:20
  260.1 12.3 %all_to_all.30 = bf16[16,48,256]{2,1,0:T(8,128)(2,1)S(1)} all-to-all(bf16[16,48,256]{2,1,0:T(8,128)(2,1)S(1)} %bitcast.43), channel_id=1, replica_groups=mesh['z'=4,'x'=4,'y'=4,'c'=2] {'x','y'}, dimensions={0} | all-to-all | bytes 786432 | tf_op jit(solution)/shard_map/all_to_all | solution.py:20
  272.4 5.4 %collective-permute-start.46 = (bf16[768,256]{1,0:T(8,128)(2,1)S(1)}, bf16[768,256]{1,0:T(8,128)(2,1)S(1)}, u32[]{:S(2)}, u32[]{:S(2)}) collective-permute-start(bf16[768,256]{1,0:T(8,128)(2,1)S(1)} %bitcast.41), channel_id=1, source_target_pairs={{0,1},{1,0},{2,3},{3,2},{4,5},{5,4},{6,7},{7,6},{8,9},{9,8},{10,11... | collective-permute-start | bytes 1179656 | tf_op jit(solution)/shard_map/ppermute | solution.py:36
  (183 shorter events, 76.8 us)
Async XLA Ops:
  1.9 11.7 %collective-permute-start.2 = (bf16[208,256]{1,0:T(8,128)(2,1)S(1)}, bf16[208,256]{1,0:T(8,128)(2,1)S(1)}, u32[]{:S(2)}, u32[]{:S(2)}) collective-permute-start(bf16[208,256]{1,0:T(8,128)(2,1)S(1)} %concatenate.33), channel_id=1, source_target_pairs={{0,24},{8,0},{16,8},{24,16},{1,25},{9,1},{17,9},{25,17},{2,26},{10... | collective-permute-start | bytes 319496 | tf_op jit(solution)/shard_map/ppermute | solution.py:28
  11.9 16.7 %collective-permute-start.7 = (bf16[2,352,256]{2,1,0:T(8,128)(2,1)}, bf16[2,352,256]{2,1,0:T(8,128)(2,1)S(1)}, u32[]{:S(2)}, u32[]{:S(2)}) collective-permute-start(bf16[2,352,256]{2,1,0:T(8,128)(2,1)} %get-tuple-element.25), channel_id=1, source_target_pairs={{0,16},{8,24},{16,0},{24,8},{1,17},{9,25},{17,1},{25,9},{2,18},{10... | collective-permute-start | bytes 1081352 | tf_op jit(solution)/shard_map/ppermute | solution.py:28
  13.7 20.3 %collective-permute-start.3 = (bf16[4,192,256]{2,1,0:T(8,128)(2,1)S(1)}, bf16[4,192,256]{2,1,0:T(8,128)(2,1)S(1)}, u32[]{:S(2)}, u32[]{:S(2)}) collective-permute-start(bf16[4,192,256]{2,1,0:T(8,128)(2,1)S(1)} %slice.86.refs_0_), channel_id=1, source_target_pairs={{0,2},{2,4},{4,6},{6,0},{1,3},{3,5},{5,7},{7,1},{8,10},{10,12},{12... | collective-permute-start | bytes 1179656 | tf_op jit(solution)/shard_map/ppermute | solution.py:28
  15.1 16.2 %collective-permute-start.8 = (bf16[2,352,256]{2,1,0:T(8,128)(2,1)S(1)}, bf16[2,352,256]{2,1,0:T(8,128)(2,1)S(1)}, u32[]{:S(2)}, u32[]{:S(2)}) collective-permute-start(bf16[2,352,256]{2,1,0:T(8,128)(2,1)S(1)} %copy-done.29), channel_id=1, source_target_pairs={{0,24},{8,0},{16,8},{24,16},{1,25},{9,1},{17,9},{25,17},{2,26},{10... | collective-permute-start | bytes 1081352 | tf_op jit(solution)/shard_map/ppermute | solution.py:28
  15.9 18.1 %collective-permute-start.9 = (bf16[2,352,256]{2,1,0:T(8,128)(2,1)S(1)}, bf16[2,352,256]{2,1,0:T(8,128)(2,1)S(1)}, u32[]{:S(2)}, u32[]{:S(2)}) collective-permute-start(bf16[2,352,256]{2,1,0:T(8,128)(2,1)S(1)} %copy-done.12), channel_id=1, source_target_pairs={{0,1},{1,0},{2,3},{3,2},{4,5},{5,4},{6,7},{7,6},{8,9},{9,8},{10,11... | collective-permute-start | bytes 1081352 | tf_op jit(solution)/shard_map/ppermute | solution.py:36
  20.2 14.2 %collective-permute-start.4 = (bf16[4,192,256]{2,1,0:T(8,128)(2,1)S(1)}, bf16[4,192,256]{2,1,0:T(8,128)(2,1)S(1)}, u32[]{:S(2)}, u32[]{:S(2)}) collective-permute-start(bf16[4,192,256]{2,1,0:T(8,128)(2,1)S(1)} %slice.86.refs_0_), channel_id=1, source_target_pairs={{0,4},{2,6},{4,0},{6,2},{1,5},{3,7},{5,1},{7,3},{8,12},{10,14},{12... | collective-permute-start | bytes 1179656 | tf_op jit(solution)/shard_map/ppermute | solution.py:28
  28.5 11.3 %collective-permute-start.5 = (bf16[4,192,256]{2,1,0:T(8,128)(2,1)S(1)}, bf16[4,192,256]{2,1,0:T(8,128)(2,1)S(1)}, u32[]{:S(2)}, u32[]{:S(2)}) collective-permute-start(bf16[4,192,256]{2,1,0:T(8,128)(2,1)S(1)} %slice.86.refs_0_), channel_id=1, source_target_pairs={{0,6},{2,0},{4,2},{6,4},{1,7},{3,1},{5,3},{7,5},{8,14},{10,8},{12,... | collective-permute-start | bytes 1179656 | tf_op jit(solution)/shard_map/ppermute | solution.py:28
  49.9 14.1 %collective-permute-start.14 = (bf16[96,1408]{1,0:T(8,128)(2,1)}, bf16[96,1408]{1,0:T(8,128)(2,1)}, u32[]{:S(2)}, u32[]{:S(2)}) collective-permute-start(bf16[96,1408]{1,0:T(8,128)(2,1)} %get-tuple-element.30), channel_id=1, source_target_pairs={{0,32},{32,64},{64,96},{96,0},{1,33},{33,65},{65,97},{97,1},{2,34}... | collective-permute-start | bytes 811016 | tf_op jit(solution)/shard_map/ppermute | solution.py:28
  51.6 43.3 %collective-permute-start.22 = (bf16[352,256]{1,0:T(8,128)(2,1)}, bf16[352,256]{1,0:T(8,128)(2,1)}, u32[]{:S(2)}, u32[]{:S(2)}) collective-permute-start(bf16[352,256]{1,0:T(8,128)(2,1)} %get-tuple-element.35), channel_id=1, source_target_pairs={{0,8},{8,16},{16,24},{24,0},{1,9},{9,17},{17,25},{25,1},{2,10},{10... | collective-permute-start | bytes 540680 | tf_op jit(solution)/shard_map/ppermute | solution.py:28
  51.6 45.5 %collective-permute-start.23 = (bf16[352,256]{1,0:T(8,128)(2,1)}, bf16[352,256]{1,0:T(8,128)(2,1)}, u32[]{:S(2)}, u32[]{:S(2)}) collective-permute-start(bf16[352,256]{1,0:T(8,128)(2,1)} %get-tuple-element.36), channel_id=1, source_target_pairs={{0,16},{8,24},{16,0},{24,8},{1,17},{9,25},{17,1},{25,9},{2,18},{10... | collective-permute-start | bytes 540680 | tf_op jit(solution)/shard_map/ppermute | solution.py:28
  56.1 59.2 %all-to-all-start.2 = ((bf16[4,3,352,256]{3,2,1,0:T(8,128)(2,1)}), bf16[4,3,352,256]{3,2,1,0:T(8,128)(2,1)S(1)}, u32[]{:S(2)}, u32[]{:S(2)}) async-start(bf16[4,3,352,256]{3,2,1,0:T(8,128)(2,1)} %shard_map.68), calls=%async_computation.2 | async-start | bytes 4325376 | tf_op jit(solution)/shard_map/all_to_all | solution.py:20
  60.7 48.6 %collective-permute-start.13 = (bf16[96,1408]{1,0:T(8,128)(2,1)}, bf16[96,1408]{1,0:T(8,128)(2,1)S(1)}, u32[]{:S(2)}, u32[]{:S(2)}) collective-permute-start(bf16[96,1408]{1,0:T(8,128)(2,1)} %get-tuple-element.28), channel_id=1, source_target_pairs={{0,96},{32,0},{64,32},{96,64},{1,97},{33,1},{65,33},{97,65},{2,98}... | collective-permute-start | bytes 811016 | tf_op jit(solution)/shard_map/ppermute | solution.py:28
  63.5 30.2 %collective-permute-start.17 = (bf16[96,1408]{1,0:T(8,128)(2,1)}, bf16[96,1408]{1,0:T(8,128)(2,1)S(1)}, u32[]{:S(2)}, u32[]{:S(2)}) collective-permute-start(bf16[96,1408]{1,0:T(8,128)(2,1)} %get-tuple-element.33), channel_id=1, source_target_pairs={{0,96},{32,0},{64,32},{96,64},{1,97},{33,1},{65,33},{97,65},{2,98}... | collective-permute-start | bytes 811016 | tf_op jit(solution)/shard_map/ppermute | solution.py:28
  64.1 45.4 %collective-permute-start.16 = (bf16[96,1408]{1,0:T(8,128)(2,1)}, bf16[96,1408]{1,0:T(8,128)(2,1)S(1)}, u32[]{:S(2)}, u32[]{:S(2)}) collective-permute-start(bf16[96,1408]{1,0:T(8,128)(2,1)} %get-tuple-element.31), channel_id=1, source_target_pairs={{0,32},{32,64},{64,96},{96,0},{1,33},{33,65},{65,97},{97,1},{2,34}... | collective-permute-start | bytes 811016 | tf_op jit(solution)/shard_map/ppermute | solution.py:28
  93.7 16.2 %collective-permute-start.15 = (bf16[96,1408]{1,0:T(8,128)(2,1)S(1)}, bf16[96,1408]{1,0:T(8,128)(2,1)S(1)}, u32[]{:S(2)}, u32[]{:S(2)}) collective-permute-start(bf16[96,1408]{1,0:T(8,128)(2,1)S(1)} %add_convert_fusion.1), channel_id=1, source_target_pairs={{0,32},{32,64},{64,96},{96,0},{1,33},{33,65},{65,97},{97,1},{2,34}... | collective-permute-start | bytes 811016 | tf_op jit(solution)/shard_map/ppermute | solution.py:28
  94.9 15.0 %collective-permute-start.18 = (bf16[96,1408]{1,0:T(8,128)(2,1)S(1)}, bf16[96,1408]{1,0:T(8,128)(2,1)S(1)}, u32[]{:S(2)}, u32[]{:S(2)}) collective-permute-start(bf16[96,1408]{1,0:T(8,128)(2,1)S(1)} %add_convert_fusion), channel_id=1, source_target_pairs={{0,96},{32,0},{64,32},{96,64},{1,97},{33,1},{65,33},{97,65},{2,98}... | collective-permute-start | bytes 811016 | tf_op jit(solution)/shard_map/ppermute | solution.py:28
  110.6 15.4 %collective-permute-start.20 = (bf16[192,704]{1,0:T(8,128)(2,1)S(1)}, bf16[192,704]{1,0:T(8,128)(2,1)}, u32[]{:S(2)}, u32[]{:S(2)}) collective-permute-start(bf16[192,704]{1,0:T(8,128)(2,1)S(1)} %fusion.2.refs_0_), channel_id=1, source_target_pairs={{0,64},{32,96},{64,0},{96,32},{1,65},{33,97},{65,1},{97,33},{2,66}... | collective-permute-start | bytes 811016 | tf_op jit(solution)/shard_map/ppermute | solution.py:28
  113.3 15.4 %collective-permute-start.21 = (bf16[192,704]{1,0:T(8,128)(2,1)S(1)}, bf16[192,704]{1,0:T(8,128)(2,1)}, u32[]{:S(2)}, u32[]{:S(2)}) collective-permute-start(bf16[192,704]{1,0:T(8,128)(2,1)S(1)} %fusion.2.refs_0_), channel_id=1, source_target_pairs={{0,96},{32,0},{64,32},{96,64},{1,97},{33,1},{65,33},{97,65},{2,98}... | collective-permute-start | bytes 811016 | tf_op jit(solution)/shard_map/ppermute | solution.py:28
  116.8 46.6 %collective-permute-start.32 = (bf16[2,3,352,256]{3,2,1,0:T(8,128)(2,1)}, bf16[2,3,352,256]{3,2,1,0:T(8,128)(2,1)}, u32[]{:S(2)}, u32[]{:S(2)}) collective-permute-start(bf16[2,3,352,256]{3,2,1,0:T(8,128)(2,1)} %get-tuple-element.44.refs_0_), channel_id=1, source_target_pairs={{0,8},{8,16},{16,24},{24,0},{1,9},{9,17},{17,25},{25,1},{2,10},{10... | collective-permute-start | bytes 3244040 | tf_op jit(solution)/shard_map/ppermute | solution.py:28
  118.0 50.4 %collective-permute-start.34 = (bf16[2,3,352,256]{3,2,1,0:T(8,128)(2,1)}, bf16[2,3,352,256]{3,2,1,0:T(8,128)(2,1)S(1)}, u32[]{:S(2)}, u32[]{:S(2)}) collective-permute-start(bf16[2,3,352,256]{3,2,1,0:T(8,128)(2,1)} %get-tuple-element.44.refs_0_), channel_id=1, source_target_pairs={{0,24},{8,0},{16,8},{24,16},{1,25},{9,1},{17,9},{25,17},{2,26},{10... | collective-permute-start | bytes 3244040 | tf_op jit(solution)/shard_map/ppermute | solution.py:28
  120.2 45.5 %collective-permute-start.33 = (bf16[2,3,352,256]{3,2,1,0:T(8,128)(2,1)}, bf16[2,3,352,256]{3,2,1,0:T(8,128)(2,1)}, u32[]{:S(2)}, u32[]{:S(2)}) collective-permute-start(bf16[2,3,352,256]{3,2,1,0:T(8,128)(2,1)} %get-tuple-element.43.refs_1_), channel_id=1, source_target_pairs={{0,8},{8,16},{16,24},{24,0},{1,9},{9,17},{17,25},{25,1},{2,10},{10... | collective-permute-start | bytes 3244040 | tf_op jit(solution)/shard_map/ppermute | solution.py:28
  126.0 39.7 %collective-permute-start.35 = (bf16[2,3,352,256]{3,2,1,0:T(8,128)(2,1)}, bf16[2,3,352,256]{3,2,1,0:T(8,128)(2,1)}, u32[]{:S(2)}, u32[]{:S(2)}) collective-permute-start(bf16[2,3,352,256]{3,2,1,0:T(8,128)(2,1)} %get-tuple-element.43.refs_1_), channel_id=1, source_target_pairs={{0,24},{8,0},{16,8},{24,16},{1,25},{9,1},{17,9},{25,17},{2,26},{10... | collective-permute-start | bytes 3244040 | tf_op jit(solution)/shard_map/ppermute | solution.py:28
  133.8 48.8 %all-to-all-start = ((bf16[16,48,1024]{2,1,0:T(8,128)(2,1)}), bf16[16,48,1024]{2,1,0:T(8,128)(2,1)S(1)}, u32[]{:S(2)}, u32[]{:S(2)}) async-start(bf16[16,48,1024]{2,1,0:T(8,128)(2,1)} %bitcast.40), calls=%async_computation | async-start | bytes 3145728 | tf_op jit(solution)/shard_map/all_to_all | solution.py:20
  158.8 31.6 %collective-permute-start.38 = (bf16[2,3,352,256]{3,2,1,0:T(8,128)(2,1)}, bf16[2,3,352,256]{3,2,1,0:T(8,128)(2,1)}, u32[]{:S(2)}, u32[]{:S(2)}) collective-permute-start(bf16[2,3,352,256]{3,2,1,0:T(8,128)(2,1)} %get-tuple-element.44.refs_0_), channel_id=1, source_target_pairs={{0,1},{1,0},{2,3},{3,2},{4,5},{5,4},{6,7},{7,6},{8,9},{9,8},{10,11... | collective-permute-start | bytes 3244040 | tf_op jit(solution)/shard_map/ppermute | solution.py:36
  163.4 31.8 %collective-permute-start.39 = (bf16[2,3,352,256]{3,2,1,0:T(8,128)(2,1)}, bf16[2,3,352,256]{3,2,1,0:T(8,128)(2,1)}, u32[]{:S(2)}, u32[]{:S(2)}) collective-permute-start(bf16[2,3,352,256]{3,2,1,0:T(8,128)(2,1)} %get-tuple-element.43.refs_1_), channel_id=1, source_target_pairs={{0,1},{1,0},{2,3},{3,2},{4,5},{5,4},{6,7},{7,6},{8,9},{9,8},{10,11... | collective-permute-start | bytes 3244040 | tf_op jit(solution)/shard_map/ppermute | solution.py:36
  165.7 40.0 %collective-permute-start.36 = (bf16[2,3,352,256]{3,2,1,0:T(8,128)(2,1)}, bf16[2,3,352,256]{3,2,1,0:T(8,128)(2,1)}, u32[]{:S(2)}, u32[]{:S(2)}) collective-permute-start(bf16[2,3,352,256]{3,2,1,0:T(8,128)(2,1)} %collective-permute-done.32.refs_2_), channel_id=1, source_target_pairs={{0,8},{8,16},{16,24},{24,0},{1,9},{9,17},{17,25},{25,1},{2,10},{10... | collective-permute-start | bytes 3244040 | tf_op jit(solution)/shard_map/ppermute | solution.py:28
  165.7 42.1 %collective-permute-start.37 = (bf16[2,3,352,256]{3,2,1,0:T(8,128)(2,1)}, bf16[2,3,352,256]{3,2,1,0:T(8,128)(2,1)}, u32[]{:S(2)}, u32[]{:S(2)}) collective-permute-start(bf16[2,3,352,256]{3,2,1,0:T(8,128)(2,1)} %collective-permute-done.35.refs_5_), channel_id=1, source_target_pairs={{0,24},{8,0},{16,8},{24,16},{1,25},{9,1},{17,9},{25,17},{2,26},{10... | collective-permute-start | bytes 3244040 | tf_op jit(solution)/shard_map/ppermute | solution.py:28
  168.4 39.4 %collective-permute-start.40 = (bf16[2,3,352,256]{3,2,1,0:T(8,128)(2,1)}, bf16[2,3,352,256]{3,2,1,0:T(8,128)(2,1)}, u32[]{:S(2)}, u32[]{:S(2)}) collective-permute-start(bf16[2,3,352,256]{3,2,1,0:T(8,128)(2,1)} %collective-permute-done.32.refs_2_), channel_id=1, source_target_pairs={{0,1},{1,0},{2,3},{3,2},{4,5},{5,4},{6,7},{7,6},{8,9},{9,8},{10,11... | collective-permute-start | bytes 3244040 | tf_op jit(solution)/shard_map/ppermute | solution.py:36
  184.4 26.8 %all-to-all-start.1 = ((bf16[16,48,1152]{2,1,0:T(8,128)(2,1)}), bf16[16,48,1152]{2,1,0:T(8,128)(2,1)S(1)}, u32[]{:S(2)}, u32[]{:S(2)}) async-start(bf16[16,48,1152]{2,1,0:T(8,128)(2,1)} %shard_map.67), calls=%async_computation.1 | async-start | bytes 3538944 | tf_op jit(solution)/shard_map/all_to_all | solution.py:20
  190.4 20.1 %collective-permute-start.43 = (bf16[2,3,352,256]{3,2,1,0:T(8,128)(2,1)}, bf16[2,3,352,256]{3,2,1,0:T(8,128)(2,1)}, u32[]{:S(2)}, u32[]{:S(2)}) collective-permute-start(bf16[2,3,352,256]{3,2,1,0:T(8,128)(2,1)} %collective-permute-done.35.refs_5_), channel_id=1, source_target_pairs={{0,1},{1,0},{2,3},{3,2},{4,5},{5,4},{6,7},{7,6},{8,9},{9,8},{10,11... | collective-permute-start | bytes 3244040 | tf_op jit(solution)/shard_map/ppermute | solution.py:36
  195.2 13.4 %collective-permute-start.41 = (bf16[2,3,352,256]{3,2,1,0:T(8,128)(2,1)}, bf16[2,3,352,256]{3,2,1,0:T(8,128)(2,1)}, u32[]{:S(2)}, u32[]{:S(2)}) collective-permute-start(bf16[2,3,352,256]{3,2,1,0:T(8,128)(2,1)} %collective-permute-done.33.refs_3_), channel_id=1, source_target_pairs={{0,1},{1,0},{2,3},{3,2},{4,5},{5,4},{6,7},{7,6},{8,9},{9,8},{10,11... | collective-permute-start | bytes 3244040 | tf_op jit(solution)/shard_map/ppermute | solution.py:36
  226.2 24.6 %all-to-all-start.3 = ((bf16[16,48,1024]{2,1,0:T(8,128)(2,1)}), bf16[16,48,1024]{2,1,0:T(8,128)(2,1)S(1)}, u32[]{:S(2)}, u32[]{:S(2)}) async-start(bf16[16,48,1024]{2,1,0:T(8,128)(2,1)} %get-tuple-element.40), calls=%async_computation.3 | async-start | bytes 3145728 | tf_op jit(solution)/shard_map/all_to_all | solution.py:20
  (50 other events, 598.3 us)

commit v2 on v1

--- a/solution.py
+++ b/solution.py
@@ -20,10 +20,6 @@
     return lax.all_to_all(parts, axes, 0, 0, tiled=True)
 
 
-def share(block, axes, peers):
-    return exchange(jnp.broadcast_to(block[None], (peers, *block.shape)), axes)
-
-
 def shift(block, axis, step):
     return lax.ppermute(block, axis, [(i, (i + step) % 4) for i in range(4)])
 
@@ -68,40 +64,45 @@
     return started
 
 
-def turn_kernel(gate_ref, up_ref, down_ref, out):
-    rows = out.shape[2]
+def turn_pair(gate_ref, up_ref, turned):
     for g, ref in enumerate((gate_ref, up_ref)):
-        turned = ref[0].T
-        for p in range(4):
-            out[p, g] = turned[p * rows : p * rows + rows]
-    for p in range(4):
-        out[p, 2] = down_ref[0, p * rows : p * rows + rows]
-
-
-def turn(layer, gate, up, down):
+        turned[g] = ref[0].T
+
+
+def turn_kernel(place_ref, gate_ref, up_ref, down_ref, *rest):
+    outs, turned = rest[:-1], rest[-1]
+    own = place_ref[0]
+    rows = gate_ref.shape[2] // 4
+    turn_pair(gate_ref, up_ref, turned)
+    for k in range(4):
+        at = pl.ds(pl.multiple_of(lax.rem(own + k, 4) * rows, 16), rows)
+        outs[k][0:2] = turned[:, at, :]
+        outs[k][2] = down_ref[0, at, :]
+
+
+def turn(place, layer, gate, up, down):
     rows = gate.shape[2] // 4
     pick = lambda i: (layer, 0, 0)
     return pl.pallas_call(
         turn_kernel,
-        out_shape=sds(4, 3, rows, 256),
+        out_shape=[sds(3, rows, 256)] * 4,
         in_specs=[
+            SMEM,
             pl.BlockSpec((1, *gate.shape[1:]), pick),
             pl.BlockSpec((1, *up.shape[1:]), pick),
             pl.BlockSpec((1, *down.shape[1:]), pick),
         ],
-        out_specs=VMEM,
+        out_specs=[VMEM] * 4,
         grid=(1,),
-    )(gate, up, down)
+        scratch_shapes=[pltpu.VMEM((2, gate.shape[2], 256), BF16)],
+    )(place, gate, up, down)
 
 
 def pack_kernel(place_ref, gate_ref, up_ref, down_ref, *rest):
     outs, turned = rest[:-1], rest[-1]
     own = place_ref[1]
-    cols = gate_ref.shape[2]
-    for g, ref in enumerate((gate_ref, up_ref)):
-        for at in range(0, cols, 128):
-            turned[g, at : at + 128, :] = ref[0, :, at : at + 128].T
-    rows = cols // 4
+    rows = gate_ref.shape[2] // 4
+    turn_pair(gate_ref, up_ref, turned)
     for k in range(4):
         at = pl.ds(pl.multiple_of(lax.rem(own + k, 4) * rows, 16), rows)
         outs[k][0:2] = turned[:, at, :]
@@ -177,6 +178,7 @@
             pltpu.SemaphoreType.DMA((32,)),
             pltpu.SemaphoreType.DMA((7,)),
         ],
+        compiler_params=pltpu.CompilerParams(vmem_limit_bytes=56 << 20),
     )(place, *rows, *mine, *theirs)
 
 
@@ -203,13 +205,14 @@
     return pl.pallas_call(
         down_kernel,
         out_shape=sds(4 * n, 1024),
-        in_specs=[SMEM] + [ANY] * 12,
+        in_specs=[SMEM] + [VMEM] * 4 + [ANY] * 8,
         out_specs=VMEM,
         scratch_shapes=[
             pltpu.VMEM((4, n, cols), BF16),
             pltpu.VMEM((cols, 1024), BF16),
             pltpu.SemaphoreType.DMA((12,)),
         ],
+        compiler_params=pltpu.CompilerParams(vmem_limit_bytes=24 << 20),
     )(place, *hidden, *mine, *theirs)
 
 
@@ -250,10 +253,10 @@
 
 
 def block_kernel(place_ref, rows_ref, affine_ref, *refs):
-    pieces, out, own_out = refs[:16], refs[16], refs[17]
-    stream, tails, weights, row_sems, sems = refs[18:]
+    pieces, out, own_out = refs[:32], refs[32], refs[33]
+    stream, tails, weights, hidden, row_sems, sems = refs[34:]
     z, x, y = place_ref[0], place_ref[1], place_ref[2]
-    n, rows = rows_ref.shape[1], pieces[0].shape[2]
+    n, rows = rows_ref.shape[1], pieces[0].shape[1]
     copies = []
     for i in range(16):
         at = slice(i % 4 * n, i % 4 * n + n)
@@ -263,10 +266,9 @@
 
     def load(g):
         for i, piece in enumerate(pieces):
-            at, step, first = i // 8 * rows, (0, 1, 3, 2)[i % 8 // 2], i % 2 * 2
-            for q in range(2):
-                lanes = pl.ds(pl.multiple_of((first + q) * 1024 + behind(x, step) * 256, 256), 256)
-                pltpu.make_async_copy(piece.at[q, g], weights.at[g, at : at + rows, lanes], sems.at[g]).start()
+            at = i // 16 * rows
+            lanes = pl.ds(pl.multiple_of(behind(z, i % 4) * 1024 + behind(x, i // 4 % 4) * 256, 256), 256)
+            pltpu.make_async_copy(piece.at[g], weights.at[g, at : at + rows, lanes], sems.at[g]).start()
 
     def loaded(g):
         pltpu.make_async_copy(weights.at[g], weights.at[g], sems.at[g]).wait()
@@ -282,10 +284,16 @@
     mean = sum(means) / 4
     square = sum(squares) + sum((m - mean) * (m - mean) for m in means) * 1024
     scale = lax.rsqrt(square / WIDTH + EPSILON)
-    for q in range(4):
-        at = slice(q * 1024, q * 1024 + 1024)
-        value = (stream[:, at].astype(F32) + (means[q] - mean)) * scale
+
+    def normalise(q, carry):
+        at = pl.ds(pl.multiple_of(q * 1024, 1024), 1024)
+        tail = tails[q].astype(F32)
+        offset = tail[:, 0:1] + tail[:, 1:2] + tail[:, 2:3] - mean
+        value = (stream[:, at].astype(F32) + offset) * scale
         stream[:, at] = (value * affine_ref[0:1, at] + affine_ref[1:2, at]).astype(BF16)
+        return carry
+
+    lax.fori_loop(0, 4, normalise, 0)
     own_out[...] = stream[pl.ds(pl.multiple_of(y * n, 16), n), pl.ds(pl.multiple_of(z * 1024, 1024), 1024)]
     loaded(0)
     load(1)
@@ -293,28 +301,34 @@
     gate = dot_nt(stream[...], weights[0])
     gate = gate * jax.nn.sigmoid(gate)
     loaded(1)
-    hidden = (gate * dot_nt(stream[...], weights[1])).astype(BF16)
+    hidden[...] = (gate * dot_nt(stream[...], weights[1])).astype(BF16)
     loaded(2)
-    for q in range(4):
-        part = jnp.dot(hidden, weights[2, :, q * 1024 : q * 1024 + 1024], preferred_element_type=F32)
-        out[4 * q : 4 * q + 4] = part.astype(BF16).reshape(4, n, 1024)
+
+    def step(q, carry):
+        lanes = pl.ds(pl.multiple_of(q * 1024, 1024), 1024)
+        part = jnp.dot(hidden[...], weights[2, :, lanes], preferred_element_type=F32)
+        out[pl.ds(4 * q, 4)] = part.astype(BF16).reshape(4, n, 1024)
+        return carry
+
+    lax.fori_loop(0, 4, step, 0)
 
 
 def block_layer(place, rows, affine, pieces):
-    n, half = rows.shape[1], pieces[0].shape[2]
+    n, half = rows.shape[1], pieces[0].shape[1]
     return pl.pallas_call(
         block_kernel,
         out_shape=[sds(16, n, 1024), sds(n, 1024)],
-        in_specs=[SMEM, VMEM, VMEM] + [ANY] * 16,
+        in_specs=[SMEM, VMEM, VMEM] + [ANY] * 32,
         out_specs=[VMEM] * 2,
         scratch_shapes=[
             pltpu.VMEM((4 * n, 4096), BF16),
             pltpu.VMEM((4, 4 * n, 128), BF16),
             pltpu.VMEM((3, 2 * half, 4096), BF16),
+            pltpu.VMEM((4 * n, 2 * half), BF16),
             pltpu.SemaphoreType.DMA((32,)),
             pltpu.SemaphoreType.DMA((3,)),
         ],
-        compiler_params=pltpu.CompilerParams(vmem_limit_bytes=40 << 20),
+        compiler_params=pltpu.CompilerParams(vmem_limit_bytes=58 << 20),
     )(place, rows, affine, *pieces)
 
 
@@ -361,16 +375,16 @@
     gu0_core = [swap_core(w) for w in gu0]
     down0_core = [swap_core(w) for w in down0]
 
-    w1 = turn(1, gate_weight, up_weight, down_weight)
-    w1 = exchange(w1, "z")
-    w1 = [w1[:2], w1[2:]]
+    w1 = turn(place, 1, gate_weight, up_weight, down_weight)
+    w1 = exchange4(w1, "z")
     near, far = [], []
-    for h in range(2):
-        near.append(shift(w1[h], "x", 1))
-        far.append(shift(w1[h], "x", 3))
-    across = [shift(near[0], "x", 1)]
-    across.append(shift(far[1], "x", 3))
-    w1 = [*w1, *near, *far, *across]
+    for k in range(4):
+        near.append(shift(w1[k], "x", 1))
+        far.append(shift(w1[k], "x", 3))
+    across = []
+    for k in range(4):
+        across.append(shift(near[k], "x", 1) if k < 2 else shift(far[k], "x", 3))
+    w1 = [*w1, *near, *across, *far]
     w1_core = []
     for w in w1:
         w1_core.append(swap_core(w))
@@ -391,7 +405,7 @@
     )
     hidden = (jax.nn.silu(sums[:, :cols]) * sums[:, cols:]).astype(BF16)
     hidden = share4(hidden, "z")
-    partial = down(place, hidden, down0, down0_core)
+    partial = down(place, [in_vmem(piece) for piece in hidden], down0, down0_core)
     branch = exchange(partial.reshape(16, block, 1024), ("x", "y"))
     affine = in_order(mine[:, quarter : quarter + 12].astype(F32), x)
     affine = (affine[:, :4] + affine[:, 4:8]) + affine[:, 8:]
@@ -404,7 +418,8 @@
     parts, own = block_layer(place, stream, spread, w1 + w1_core)
     branch = exchange(parts, ("z", "y")).astype(F32).sum(axis=0)
     mixed = RESIDUAL * own.astype(F32) + branch
-    stats = share(row_stats(mixed), "z", 4).sum(axis=0)
+    stats = share4(row_stats(mixed), "z")
+    stats = (stats[0] + stats[2]) + (stats[1] + stats[3])
     out = normed(mixed, stats[0], stats[1], affine[1], affine[3])
     parts = jnp.broadcast_to(out.reshape(block, 4, 1, 256).transpose(1, 2, 0, 3), (4, 4, block, 256))
     ours = exchange(parts.reshape(16, block, 256), ("x", "y")).reshape(half, 256)

time: 282 us -> 310 us (1.099)
  starting transfers between devices: 111 us -> 140 us
  waiting for transfers between devices: 101 us -> 115 us
  local copies, waits for them, and re-layouts: 14.9 us -> 3.96 us
    ppermute x17 -> x25, starting transfers between devices: 38.5 us -> 65.4 us  [swap_core(): return lax.ppermute(block, 'c', [(0, 1), (1, 0)])]
    ppermute x30 -> x42, waiting for transfers between devices: 66.6 us -> 87.7 us  [shift(): return lax.ppermute(block, axis, [(i, (i + step) % 4) for i in range(4)])]
    unnamed x68 -> x74, local copies, waits for them, and re-layouts: 10.4 us -> 3.6 us
    all_to_all x5 -> x3, waiting for transfers between devices: 29 us -> 23.9 us  [exchange(): return lax.all_to_all(parts, axes, 0, 0, tiled=True)]
    all_to_all x5 -> x3, starting transfers between devices: 24.7 us -> 28.1 us  [exchange(): return lax.all_to_all(parts, axes, 0, 0, tiled=True)]
    ppermute x30 -> x42, starting transfers between devices: 47.7 us -> 46.4 us  [shift(): return lax.ppermute(block, axis, [(i, (i + step) % 4) for i in range(4)])]
  transfers between devices with their start and end apart: 52 -> 70, of which waited for: 20 -> 23; matrix products, arithmetic and copies ran while one was open for 5% -> 1% of each run, Pallas kernels for 5% -> 4%
where the time goes in v2:
time: 310 us; the launch traced here: 309 us
  starting transfers between devices  140 us (45%)
  waiting for transfers between devices  115 us (37%)
  Pallas kernels  33.1 us (11%)
  blocking collectives  10.7 us (3%)
  other arithmetic  5.82 us (2%)
  local copies, waits for them, and re-layouts  3.96 us (1%)
    ppermute x42, waiting for transfers between devices, shift(): return lax.ppermute(block, axis, [(i, (i + step) % 4) for i in range(4)])  87.7 us
    ppermute x25, starting transfers between devices, swap_core(): return lax.ppermute(block, 'c', [(0, 1), (1, 0)])  65.4 us
    ppermute x42, starting transfers between devices, shift(): return lax.ppermute(block, axis, [(i, (i + step) % 4) for i in range(4)])  46.4 us
    all_to_all x3, starting transfers between devices, exchange(): return lax.all_to_all(parts, axes, 0, 0, tiled=True)  28.1 us
    all_to_all x3, waiting for transfers between devices, exchange(): return lax.all_to_all(parts, axes, 0, 0, tiled=True)  23.9 us
    pallas_call x1, Pallas kernels, block_layer(): pl.pallas_call(block_kernel, out_shape=[sds(16, n, 1024), sds(n, 1024)],...  12.3 us
    all_to_all x1, blocking collectives, exchange(): return lax.all_to_all(parts, axes, 0, 0, tiled=True)  10.7 us
    pallas_call x1, Pallas kernels, gate_up(): pl.pallas_call(gate_up_kernel, out_shape=[sds(n, 4 * half)] + [sds(n // 2...  8.58 us
  transfers between devices with their start and end apart: 70, of which 23 were waited for; matrix products, arithmetic and copies ran while one was open for 1% of the time, Pallas kernels for 4%

profile of v2, /device:TPU:1, one launch (start us, length us, event | category | flops | bytes accessed | tf_op | source)
XLA Modules:
  0.0 309.2 jit_solution(9849453072540572993)
XLA Ops:
  1.2 3.3 %collective-permute-start.2 = (bf16[208,256]{1,0:T(8,128)(2,1)S(1)}, bf16[208,256]{1,0:T(8,128)(2,1)S(1)}, u32[]{:S(2)}, u32[]{:S(2)}) collective-permute-start(bf16[208,256]{1,0:T(8,128)(2,1)S(1)} %concatenate.33), channel_id=1, source_target_pairs={{0,24},{8,0},{16,8},{24,16},{1,25},{9,1},{17,9},{25,17},{2,26},{10... | collective-permute-start | bytes 319496 | tf_op jit(solution)/shard_map/ppermute | solution.py:24
  6.4 3.3 %shard_map.64 = (bf16[2,352,256]{2,1,0:T(8,128)(2,1)}, bf16[2,352,256]{2,1,0:T(8,128)(2,1)}, bf16[2,352,256]{2,1,0:T(8,128)(2,1)}, bf16[2,352,256]{2,1,0:T(8,128...) custom-call(s32[4]{0:T(128)} %pad_add_fusion.place_ref, ...), custom_call_target="tpu_custom_call" | custom-call | tf_op jit(solution)/shard_map/pallas_call | solution.py:116
  22.5 5.4 %collective-permute-done.7.refs_6_ = bf16[2,352,256]{2,1,0:T(8,128)(2,1)S(1)} collective-permute-done((bf16[2,352,256]{2,1,0:T(8,128)(2,1)}, bf16[2,352,256]{2,1,0:T(8,128)(2,1)S(1)}, u32[]{:S(2)}, u32[]{:S(2)}) %collective-permute-start.7) | collective-permute-done | bytes 360480 | tf_op jit(solution)/shard_map/ppermute | solution.py:24
  31.9 3.5 %collective-permute-done.5.refs_3_ = bf16[4,192,256]{2,1,0:T(8,128)(2,1)S(1)} collective-permute-done((bf16[4,192,256]{2,1,0:T(8,128)(2,1)S(1)}, bf16[4,192,256]{2,1,0:T(8,128)(2,1)S(1)}, u32[]{:S(2)}, u32[]{:S(2)}) %collective-permute-start.5) | collective-permute-done | bytes 393248 | tf_op jit(solution)/shard_map/ppermute | solution.py:24
  40.0 8.6 %shard_map.65 = (bf16[192,1408]{1,0:T(8,128)(2,1)}, bf16[96,1408]{1,0:T(8,128)(2,1)}, bf16[96,1408]{1,0:T(8,128)(2,1)}, bf16[96,1408]{1,0:T(8,128)(2,1)}, bf16[9...) custom-call(s32[4]{0:T(128)} %pad_add_fusion.place_ref, ...), custom_call_target="tpu_custom_call" | custom-call | tf_op jit(solution)/shard_map/pallas_call | solution.py:169
  57.6 4.1 %collective-permute-done.17 = bf16[96,1408]{1,0:T(8,128)(2,1)S(1)} collective-permute-done((bf16[96,1408]{1,0:T(8,128)(2,1)}, bf16[96,1408]{1,0:T(8,128)(2,1)S(1)}, u32[]{:S(2)}, u32[]{:S(2)}) %collective-permute-start.17) | collective-permute-done | bytes 270368 | tf_op jit(solution)/shard_map/ppermute | solution.py:24
  62.7 3.4 %collective-permute-start.18 = (bf16[96,1408]{1,0:T(8,128)(2,1)S(1)}, bf16[96,1408]{1,0:T(8,128)(2,1)S(1)}, u32[]{:S(2)}, u32[]{:S(2)}) collective-permute-start(bf16[96,1408]{1,0:T(8,128)(2,1)S(1)} %add_convert_fusion), channel_id=1, source_target_pairs={{0,96},{32,0},{64,32},{96,64},{1,97},{33,1},{65,33},{97,65},{2,98}... | collective-permute-start | bytes 811016 | tf_op jit(solution)/shard_map/ppermute | solution.py:24
  66.2 4.1 %collective-permute-done.31 = f32[2,1024]{1,0:T(2,128)S(1)} collective-permute-done((f32[2,1024]{1,0:T(2,128)S(1)}, f32[2,1024]{1,0:T(2,128)S(1)}, u32[]{:S(2)}, u32[]{:S(2)}) %collective-permute-start.31) | collective-permute-done | bytes 8224 | tf_op jit(solution)/shard_map/ppermute | solution.py:24
  70.3 4.0 %collective-permute-done.30 = f32[2,1024]{1,0:T(2,128)S(1)} collective-permute-done((f32[2,1024]{1,0:T(2,128)S(1)}, f32[2,1024]{1,0:T(2,128)S(1)}, u32[]{:S(2)}, u32[]{:S(2)}) %collective-permute-start.30) | collective-permute-done | bytes 8224 | tf_op jit(solution)/shard_map/ppermute | solution.py:24
  77.8 3.5 %shard_map.68 = (bf16[3,352,256]{2,1,0:T(8,128)(2,1)}, bf16[3,352,256]{2,1,0:T(8,128)(2,1)}, bf16[3,352,256]{2,1,0:T(8,128)(2,1)}, bf16[3,352,256]{2,1,0:T(8,128)(2,1)}) custom-call(s32[4]{0:T(128)} %pad_add_fusion.place_ref, bf16[2,256,1408]{2,1,0:T(8,128)(2,1)} %gate_ref.3, bf16[2,256,1408]{2,1,0:T(8,128)(2,1)} %up_ref.3, bf16[2,1408,256]{2,1,0:T(8,128)(2,1)} %down_ref.3), custom_call_target="tpu_custom_call" | custom-call | tf_op jit(solution)/shard_map/pallas_call | solution.py:86
  84.7 9.2 %collective-permute-start.25 = (bf16[352,256]{1,0:T(8,128)(2,1)S(1)}, bf16[352,256]{1,0:T(8,128)(2,1)S(1)}, u32[]{:S(2)}, u32[]{:S(2)}) collective-permute-start(bf16[352,256]{1,0:T(8,128)(2,1)S(1)} %copy-done.1), channel_id=1, source_target_pairs={{0,1},{1,0},{2,3},{3,2},{4,5},{5,4},{6,7},{7,6},{8,9},{9,8},{10,11... | collective-permute-start | bytes 540680 | tf_op jit(solution)/shard_map/ppermute | solution.py:32
  94.4 3.7 %collective-permute-start.27 = (bf16[352,256]{1,0:T(8,128)(2,1)S(1)}, bf16[352,256]{1,0:T(8,128)(2,1)S(1)}, u32[]{:S(2)}, u32[]{:S(2)}) collective-permute-start(bf16[352,256]{1,0:T(8,128)(2,1)S(1)} %collective-permute-done.23.refs_6_), channel_id=1, source_target_pairs={{0,1},{1,0},{2,3},{3,2},{4,5},{5,4},{6,7},{7,6},{8,9},{9,8},{10,11... | collective-permute-start | bytes 540680 | tf_op jit(solution)/shard_map/ppermute | solution.py:32
  101.8 3.4 %collective-permute-start.33 = (bf16[3,352,256]{2,1,0:T(8,128)(2,1)}, bf16[3,352,256]{2,1,0:T(8,128)(2,1)}, u32[]{:S(2)}, u32[]{:S(2)}) collective-permute-start(bf16[3,352,256]{2,1,0:T(8,128)(2,1)} %get-tuple-element.45), channel_id=1, source_target_pairs={{0,64},{32,96},{64,0},{96,32},{1,65},{33,97},{65,1},{97,33},{2,66}... | collective-permute-start | bytes 1622024 | tf_op jit(solution)/shard_map/ppermute | solution.py:24
  105.3 4.1 %collective-permute-done.32.refs_1_ = bf16[3,352,256]{2,1,0:T(8,128)(2,1)S(1)} collective-permute-done((bf16[3,352,256]{2,1,0:T(8,128)(2,1)S(1)}, bf16[3,352,256]{2,1,0:T(8,128)(2,1)S(1)}, u32[]{:S(2)}, u32[]{:S(2)}) %collective-permute-start.32) | collective-permute-done | bytes 540704 | tf_op jit(solution)/shard_map/ppermute | solution.py:24
  109.4 7.5 %collective-permute-start.47 = (bf16[3,352,256]{2,1,0:T(8,128)(2,1)S(1)}, bf16[3,352,256]{2,1,0:T(8,128)(2,1)}, u32[]{:S(2)}, u32[]{:S(2)}) collective-permute-start(bf16[3,352,256]{2,1,0:T(8,128)(2,1)S(1)} %copy-done.5), channel_id=1, source_target_pairs={{0,1},{1,0},{2,3},{3,2},{4,5},{5,4},{6,7},{7,6},{8,9},{9,8},{10,11... | collective-permute-start | bytes 1622024 | tf_op jit(solution)/shard_map/ppermute | solution.py:32
  117.7 4.2 %collective-permute-done.19.refs_1_ = bf16[192,704]{1,0:T(8,128)(2,1)S(1)} collective-permute-done((bf16[192,704]{1,0:T(8,128)(2,1)S(1)}, bf16[192,704]{1,0:T(8,128)(2,1)S(1)}, u32[]{:S(2)}, u32[]{:S(2)}) %collective-permute-start.19) | collective-permute-done | bytes 270368 | tf_op jit(solution)/shard_map/ppermute | solution.py:24
  122.7 3.7 %shard_map.66 = bf16[768,1024]{1,0:T(8,128)(2,1)} custom-call(s32[4]{0:T(128)S(1)} %copy-done.3, bf16[192,704]{1,0:T(8,128)(2,1)S(1)} %fusion.2.refs_0_, bf16[192,704]{1,0:T(8,128)(2,1)S(1)} %collective-permute-done.19.refs_1_, bf16[192,704]{1,0:T(8,128)(2,1)S(1)} %collective-permute-done.20.refs_2_, bf16[192,704]{1,0:T(8,128)(2,1)S(1)} %collective-permute-done.21.refs_3_, ...), custom_call_target="tpu_custom_call" | custom-call | tf_op jit(solution)/shard_map/pallas_call | solution.py:205
  126.4 16.5 %all-to-all-start = ((bf16[16,48,1024]{2,1,0:T(8,128)(2,1)}), bf16[16,48,1024]{2,1,0:T(8,128)(2,1)S(1)}, u32[]{:S(2)}, u32[]{:S(2)}) async-start(bf16[16,48,1024]{2,1,0:T(8,128)(2,1)} %bitcast.8), calls=%async_computation | async-start | bytes 3145728 | tf_op jit(solution)/shard_map/all_to_all | solution.py:20
  142.9 4.2 %collective-permute-start.48 = (bf16[3,352,256]{2,1,0:T(8,128)(2,1)}, bf16[3,352,256]{2,1,0:T(8,128)(2,1)S(1)}, u32[]{:S(2)}, u32[]{:S(2)}) collective-permute-start(bf16[3,352,256]{2,1,0:T(8,128)(2,1)} %copy-done.6), channel_id=1, source_target_pairs={{0,1},{1,0},{2,3},{3,2},{4,5},{5,4},{6,7},{7,6},{8,9},{9,8},{10,11... | collective-permute-start | bytes 1622024 | tf_op jit(solution)/shard_map/ppermute | solution.py:32
  153.3 16.6 %collective-permute-done.46.refs_13_ = bf16[3,352,256]{2,1,0:T(8,128)(2,1)S(1)} collective-permute-done((bf16[3,352,256]{2,1,0:T(8,128)(2,1)}, bf16[3,352,256]{2,1,0:T(8,128)(2,1)S(1)}, u32[]{:S(2)}, u32[]{:S(2)}) %collective-permute-start.46) | collective-permute-done | bytes 540704 | tf_op jit(solution)/shard_map/ppermute | solution.py:24
  169.9 9.2 %collective-permute-start.50 = (bf16[3,352,256]{2,1,0:T(8,128)(2,1)}, bf16[3,352,256]{2,1,0:T(8,128)(2,1)}, u32[]{:S(2)}, u32[]{:S(2)}) collective-permute-start(bf16[3,352,256]{2,1,0:T(8,128)(2,1)} %collective-permute-done.34.refs_3_), channel_id=1, source_target_pairs={{0,1},{1,0},{2,3},{3,2},{4,5},{5,4},{6,7},{7,6},{8,9},{9,8},{10,11... | collective-permute-start | bytes 1622024 | tf_op jit(solution)/shard_map/ppermute | solution.py:32
  181.6 8.6 %collective-permute-start.59 = (bf16[3,352,256]{2,1,0:T(8,128)(2,1)}, bf16[3,352,256]{2,1,0:T(8,128)(2,1)}, u32[]{:S(2)}, u32[]{:S(2)}) collective-permute-start(bf16[3,352,256]{2,1,0:T(8,128)(2,1)} %collective-permute-done.45.refs_12_), channel_id=1, source_target_pairs={{0,1},{1,0},{2,3},{3,2},{4,5},{5,4},{6,7},{7,6},{8,9},{9,8},{10,11... | collective-permute-start | bytes 1622024 | tf_op jit(solution)/shard_map/ppermute | solution.py:32
  192.0 4.6 %all-to-all-start.1 = ((bf16[16,48,1152]{2,1,0:T(8,128)(2,1)}), bf16[16,48,1152]{2,1,0:T(8,128)(2,1)S(1)}, u32[]{:S(2)}, u32[]{:S(2)}) async-start(bf16[16,48,1152]{2,1,0:T(8,128)(2,1)} %shard_map.67), calls=%async_computation.1 | async-start | bytes 3538944 | tf_op jit(solution)/shard_map/all_to_all | solution.py:20
  200.0 12.1 %collective-permute-done.39.refs_8_ = bf16[3,352,256]{2,1,0:T(8,128)(2,1)} collective-permute-done((bf16[3,352,256]{2,1,0:T(8,128)(2,1)}, bf16[3,352,256]{2,1,0:T(8,128)(2,1)}, u32[]{:S(2)}, u32[]{:S(2)}) %collective-permute-start.39) | collective-permute-done | bytes 540704 | tf_op jit(solution)/shard_map/ppermute | solution.py:24
  215.5 8.2 %collective-permute-done.40.refs_9_ = bf16[3,352,256]{2,1,0:T(8,128)(2,1)} collective-permute-done((bf16[3,352,256]{2,1,0:T(8,128)(2,1)}, bf16[3,352,256]{2,1,0:T(8,128)(2,1)}, u32[]{:S(2)}, u32[]{:S(2)}) %collective-permute-start.40) | collective-permute-done | bytes 540704 | tf_op jit(solution)/shard_map/ppermute | solution.py:24
  227.7 9.2 %collective-permute-done.44.refs_11_ = bf16[3,352,256]{2,1,0:T(8,128)(2,1)} collective-permute-done((bf16[3,352,256]{2,1,0:T(8,128)(2,1)}, bf16[3,352,256]{2,1,0:T(8,128)(2,1)}, u32[]{:S(2)}, u32[]{:S(2)}) %collective-permute-start.44) | collective-permute-done | bytes 540704 | tf_op jit(solution)/shard_map/ppermute | solution.py:24
  240.6 12.3 %shard_map.69 = (bf16[16,48,1024]{2,1,0:T(8,128)(2,1)}, bf16[48,1024]{1,0:T(8,128)(2,1)}) custom-call(s32[4]{0:T(128)} %pad_add_fusion.place_ref, bf16[16,48,1152]{2,1,0:T(8,128)(2,1)S(1)} %all-to-all-done.1.rows_ref, f32[2,4096]{1,0:T(2,128)} %bitcast.51, bf16[3,352,256]{2,1,0:T(8,128)(2,1)} %get-tuple-element.43.refs_0_, bf16[3,352,256]{2,1,0:T(8,128)(2,1)} %copy-done.6, ...), custom_call_target="tpu_custom_call" | custom-call | tf_op jit(solution)/shard_map/pallas_call | solution.py:318
  252.9 7.1 %all-to-all-start.2 = ((bf16[16,48,1024]{2,1,0:T(8,128)(2,1)}), bf16[16,48,1024]{2,1,0:T(8,128)(2,1)S(1)}, u32[]{:S(2)}, u32[]{:S(2)}) async-start(bf16[16,48,1024]{2,1,0:T(8,128)(2,1)} %get-tuple-element.48), calls=%async_computation.2 | async-start | bytes 3145728 | tf_op jit(solution)/shard_map/all_to_all | solution.py:20
  260.0 23.9 %all-to-all-done.2 = bf16[16,48,1024]{2,1,0:T(8,128)(2,1)S(1)} async-done(((bf16[16,48,1024]{2,1,0:T(8,128)(2,1)}), bf16[16,48,1024]{2,1,0:T(8,128)(2,1)S(1)}, u32[]{:S(2)}, u32[]{:S(2)}) %all-to-all-start.2) | async-done | bytes 1572896 | tf_op jit(solution)/shard_map/all_to_all | solution.py:20
  288.1 3.0 collective-permute-done.63
  291.4 10.7 %all_to_all.20 = bf16[16,48,256]{2,1,0:T(8,128)(2,1)S(1)} all-to-all(bf16[16,48,256]{2,1,0:T(8,128)(2,1)S(1)} %bitcast.41), channel_id=1, replica_groups=mesh['z'=4,'x'=4,'y'=4,'c'=2] {'x','y'}, dimensions={0} | all-to-all | bytes 786432 | tf_op jit(solution)/shard_map/all_to_all | solution.py:20
  302.0 4.6 %collective-permute-start.66 = (bf16[768,256]{1,0:T(8,128)(2,1)S(1)}, bf16[768,256]{1,0:T(8,128)(2,1)S(1)}, u32[]{:S(2)}, u32[]{:S(2)}) collective-permute-start(bf16[768,256]{1,0:T(8,128)(2,1)S(1)} %bitcast.39), channel_id=1, source_target_pairs={{0,1},{1,0},{2,3},{3,2},{4,5},{5,4},{6,7},{7,6},{8,9},{9,8},{10,11... | collective-permute-start | bytes 1179656 | tf_op jit(solution)/shard_map/ppermute | solution.py:32
  (223 shorter events, 79.0 us)
Async XLA Ops:
  11.2 16.7 %collective-permute-start.7 = (bf16[2,352,256]{2,1,0:T(8,128)(2,1)}, bf16[2,352,256]{2,1,0:T(8,128)(2,1)S(1)}, u32[]{:S(2)}, u32[]{:S(2)}) collective-permute-start(bf16[2,352,256]{2,1,0:T(8,128)(2,1)} %get-tuple-element.29), channel_id=1, source_target_pairs={{0,16},{8,24},{16,0},{24,8},{1,17},{9,25},{17,1},{25,9},{2,18},{10... | collective-permute-start | bytes 1081352 | tf_op jit(solution)/shard_map/ppermute | solution.py:24
  13.0 16.2 %collective-permute-start.8 = (bf16[2,352,256]{2,1,0:T(8,128)(2,1)}, bf16[2,352,256]{2,1,0:T(8,128)(2,1)S(1)}, u32[]{:S(2)}, u32[]{:S(2)}) collective-permute-start(bf16[2,352,256]{2,1,0:T(8,128)(2,1)} %get-tuple-element.30), channel_id=1, source_target_pairs={{0,24},{8,0},{16,8},{24,16},{1,25},{9,1},{17,9},{25,17},{2,26},{10... | collective-permute-start | bytes 1081352 | tf_op jit(solution)/shard_map/ppermute | solution.py:24
  13.7 18.1 %collective-permute-start.9 = (bf16[2,352,256]{2,1,0:T(8,128)(2,1)}, bf16[2,352,256]{2,1,0:T(8,128)(2,1)S(1)}, u32[]{:S(2)}, u32[]{:S(2)}) collective-permute-start(bf16[2,352,256]{2,1,0:T(8,128)(2,1)} %get-tuple-element.27.refs_4_), channel_id=1, source_target_pairs={{0,1},{1,0},{2,3},{3,2},{4,5},{5,4},{6,7},{7,6},{8,9},{9,8},{10,11... | collective-permute-start | bytes 1081352 | tf_op jit(solution)/shard_map/ppermute | solution.py:32
  15.9 19.6 %collective-permute-start.5 = (bf16[4,192,256]{2,1,0:T(8,128)(2,1)S(1)}, bf16[4,192,256]{2,1,0:T(8,128)(2,1)S(1)}, u32[]{:S(2)}, u32[]{:S(2)}) collective-permute-start(bf16[4,192,256]{2,1,0:T(8,128)(2,1)S(1)} %slice.78.refs_0_), channel_id=1, source_target_pairs={{0,6},{2,0},{4,2},{6,4},{1,7},{3,1},{5,3},{7,5},{8,14},{10,8},{12,... | collective-permute-start | bytes 1179656 | tf_op jit(solution)/shard_map/ppermute | solution.py:24
  19.6 16.9 %collective-permute-start.4 = (bf16[4,192,256]{2,1,0:T(8,128)(2,1)S(1)}, bf16[4,192,256]{2,1,0:T(8,128)(2,1)S(1)}, u32[]{:S(2)}, u32[]{:S(2)}) collective-permute-start(bf16[4,192,256]{2,1,0:T(8,128)(2,1)S(1)} %slice.78.refs_0_), channel_id=1, source_target_pairs={{0,4},{2,6},{4,0},{6,2},{1,5},{3,7},{5,1},{7,3},{8,12},{10,14},{12... | collective-permute-start | bytes 1179656 | tf_op jit(solution)/shard_map/ppermute | solution.py:24
  50.3 33.7 %collective-permute-start.13 = (bf16[96,1408]{1,0:T(8,128)(2,1)}, bf16[96,1408]{1,0:T(8,128)(2,1)S(1)}, u32[]{:S(2)}, u32[]{:S(2)}) collective-permute-start(bf16[96,1408]{1,0:T(8,128)(2,1)} %get-tuple-element.32), channel_id=1, source_target_pairs={{0,96},{32,0},{64,32},{96,64},{1,97},{33,1},{65,33},{97,65},{2,98}... | collective-permute-start | bytes 811016 | tf_op jit(solution)/shard_map/ppermute | solution.py:24
  52.5 32.2 %collective-permute-start.16 = (bf16[96,1408]{1,0:T(8,128)(2,1)}, bf16[96,1408]{1,0:T(8,128)(2,1)S(1)}, u32[]{:S(2)}, u32[]{:S(2)}) collective-permute-start(bf16[96,1408]{1,0:T(8,128)(2,1)} %get-tuple-element.35), channel_id=1, source_target_pairs={{0,32},{32,64},{64,96},{96,0},{1,33},{33,65},{65,97},{97,1},{2,34}... | collective-permute-start | bytes 811016 | tf_op jit(solution)/shard_map/ppermute | solution.py:24
  57.5 36.4 %collective-permute-start.15 = (bf16[96,1408]{1,0:T(8,128)(2,1)S(1)}, bf16[96,1408]{1,0:T(8,128)(2,1)S(1)}, u32[]{:S(2)}, u32[]{:S(2)}) collective-permute-start(bf16[96,1408]{1,0:T(8,128)(2,1)S(1)} %add_convert_fusion.1), channel_id=1, source_target_pairs={{0,32},{32,64},{64,96},{96,0},{1,33},{33,65},{65,97},{97,1},{2,34}... | collective-permute-start | bytes 811016 | tf_op jit(solution)/shard_map/ppermute | solution.py:24
  62.7 31.3 %collective-permute-start.18 = (bf16[96,1408]{1,0:T(8,128)(2,1)S(1)}, bf16[96,1408]{1,0:T(8,128)(2,1)S(1)}, u32[]{:S(2)}, u32[]{:S(2)}) collective-permute-start(bf16[96,1408]{1,0:T(8,128)(2,1)S(1)} %add_convert_fusion), channel_id=1, source_target_pairs={{0,96},{32,0},{64,32},{96,64},{1,97},{33,1},{65,33},{97,65},{2,98}... | collective-permute-start | bytes 811016 | tf_op jit(solution)/shard_map/ppermute | solution.py:24
  99.5 17.3 %collective-permute-start.20 = (bf16[192,704]{1,0:T(8,128)(2,1)S(1)}, bf16[192,704]{1,0:T(8,128)(2,1)S(1)}, u32[]{:S(2)}, u32[]{:S(2)}) collective-permute-start(bf16[192,704]{1,0:T(8,128)(2,1)S(1)} %fusion.2.refs_0_), channel_id=1, source_target_pairs={{0,64},{32,96},{64,0},{96,32},{1,65},{33,97},{65,1},{97,33},{2,66}... | collective-permute-start | bytes 811016 | tf_op jit(solution)/shard_map/ppermute | solution.py:24
  99.9 22.1 %collective-permute-start.19 = (bf16[192,704]{1,0:T(8,128)(2,1)S(1)}, bf16[192,704]{1,0:T(8,128)(2,1)S(1)}, u32[]{:S(2)}, u32[]{:S(2)}) collective-permute-start(bf16[192,704]{1,0:T(8,128)(2,1)S(1)} %fusion.2.refs_0_), channel_id=1, source_target_pairs={{0,32},{32,64},{64,96},{96,0},{1,33},{33,65},{65,97},{97,1},{2,34}... | collective-permute-start | bytes 811016 | tf_op jit(solution)/shard_map/ppermute | solution.py:24
  101.8 41.0 %collective-permute-start.33 = (bf16[3,352,256]{2,1,0:T(8,128)(2,1)}, bf16[3,352,256]{2,1,0:T(8,128)(2,1)}, u32[]{:S(2)}, u32[]{:S(2)}) collective-permute-start(bf16[3,352,256]{2,1,0:T(8,128)(2,1)} %get-tuple-element.45), channel_id=1, source_target_pairs={{0,64},{32,96},{64,0},{96,32},{1,65},{33,97},{65,1},{97,33},{2,66}... | collective-permute-start | bytes 1622024 | tf_op jit(solution)/shard_map/ppermute | solution.py:24
  109.3 37.7 %collective-permute-start.34 = (bf16[3,352,256]{2,1,0:T(8,128)(2,1)}, bf16[3,352,256]{2,1,0:T(8,128)(2,1)}, u32[]{:S(2)}, u32[]{:S(2)}) collective-permute-start(bf16[3,352,256]{2,1,0:T(8,128)(2,1)} %get-tuple-element.46), channel_id=1, source_target_pairs={{0,96},{32,0},{64,32},{96,64},{1,97},{33,1},{65,33},{97,65},{2,98}... | collective-permute-start | bytes 1622024 | tf_op jit(solution)/shard_map/ppermute | solution.py:24
  109.4 40.6 %collective-permute-start.47 = (bf16[3,352,256]{2,1,0:T(8,128)(2,1)S(1)}, bf16[3,352,256]{2,1,0:T(8,128)(2,1)}, u32[]{:S(2)}, u32[]{:S(2)}) collective-permute-start(bf16[3,352,256]{2,1,0:T(8,128)(2,1)S(1)} %copy-done.5), channel_id=1, source_target_pairs={{0,1},{1,0},{2,3},{3,2},{4,5},{5,4},{6,7},{7,6},{8,9},{9,8},{10,11... | collective-permute-start | bytes 1622024 | tf_op jit(solution)/shard_map/ppermute | solution.py:32
  116.8 33.1 %collective-permute-start.45 = (bf16[3,352,256]{2,1,0:T(8,128)(2,1)S(1)}, bf16[3,352,256]{2,1,0:T(8,128)(2,1)}, u32[]{:S(2)}, u32[]{:S(2)}) collective-permute-start(bf16[3,352,256]{2,1,0:T(8,128)(2,1)S(1)} %copy-done.5), channel_id=1, source_target_pairs={{0,24},{8,0},{16,8},{24,16},{1,25},{9,1},{17,9},{25,17},{2,26},{10... | collective-permute-start | bytes 1622024 | tf_op jit(solution)/shard_map/ppermute | solution.py:24
  121.9 28.4 %collective-permute-start.35 = (bf16[3,352,256]{2,1,0:T(8,128)(2,1)S(1)}, bf16[3,352,256]{2,1,0:T(8,128)(2,1)}, u32[]{:S(2)}, u32[]{:S(2)}) collective-permute-start(bf16[3,352,256]{2,1,0:T(8,128)(2,1)S(1)} %copy-done.5), channel_id=1, source_target_pairs={{0,8},{8,16},{16,24},{24,0},{1,9},{9,17},{17,25},{25,1},{2,10},{10... | collective-permute-start | bytes 1622024 | tf_op jit(solution)/shard_map/ppermute | solution.py:24
  126.4 63.8 %all-to-all-start = ((bf16[16,48,1024]{2,1,0:T(8,128)(2,1)}), bf16[16,48,1024]{2,1,0:T(8,128)(2,1)S(1)}, u32[]{:S(2)}, u32[]{:S(2)}) async-start(bf16[16,48,1024]{2,1,0:T(8,128)(2,1)} %bitcast.8), calls=%async_computation | async-start | bytes 3145728 | tf_op jit(solution)/shard_map/all_to_all | solution.py:20
  147.1 22.9 %collective-permute-start.46 = (bf16[3,352,256]{2,1,0:T(8,128)(2,1)}, bf16[3,352,256]{2,1,0:T(8,128)(2,1)S(1)}, u32[]{:S(2)}, u32[]{:S(2)}) collective-permute-start(bf16[3,352,256]{2,1,0:T(8,128)(2,1)} %copy-done.6), channel_id=1, source_target_pairs={{0,24},{8,0},{16,8},{24,16},{1,25},{9,1},{17,9},{25,17},{2,26},{10... | collective-permute-start | bytes 1622024 | tf_op jit(solution)/shard_map/ppermute | solution.py:24
  149.9 29.2 %collective-permute-start.36 = (bf16[3,352,256]{2,1,0:T(8,128)(2,1)}, bf16[3,352,256]{2,1,0:T(8,128)(2,1)S(1)}, u32[]{:S(2)}, u32[]{:S(2)}) collective-permute-start(bf16[3,352,256]{2,1,0:T(8,128)(2,1)} %copy-done.6), channel_id=1, source_target_pairs={{0,8},{8,16},{16,24},{24,0},{1,9},{9,17},{17,25},{25,1},{2,10},{10... | collective-permute-start | bytes 1622024 | tf_op jit(solution)/shard_map/ppermute | solution.py:24
  149.9 29.8 %collective-permute-start.49 = (bf16[3,352,256]{2,1,0:T(8,128)(2,1)}, bf16[3,352,256]{2,1,0:T(8,128)(2,1)S(1)}, u32[]{:S(2)}, u32[]{:S(2)}) collective-permute-start(bf16[3,352,256]{2,1,0:T(8,128)(2,1)} %collective-permute-done.33.refs_2_), channel_id=1, source_target_pairs={{0,1},{1,0},{2,3},{3,2},{4,5},{5,4},{6,7},{7,6},{8,9},{9,8},{10,11... | collective-permute-start | bytes 1622024 | tf_op jit(solution)/shard_map/ppermute | solution.py:32
  150.4 31.2 %collective-permute-start.41 = (bf16[3,352,256]{2,1,0:T(8,128)(2,1)}, bf16[3,352,256]{2,1,0:T(8,128)(2,1)S(1)}, u32[]{:S(2)}, u32[]{:S(2)}) collective-permute-start(bf16[3,352,256]{2,1,0:T(8,128)(2,1)} %collective-permute-done.33.refs_2_), channel_id=1, source_target_pairs={{0,24},{8,0},{16,8},{24,16},{1,25},{9,1},{17,9},{25,17},{2,26},{10... | collective-permute-start | bytes 1622024 | tf_op jit(solution)/shard_map/ppermute | solution.py:24
  153.3 43.3 %collective-permute-start.37 = (bf16[3,352,256]{2,1,0:T(8,128)(2,1)}, bf16[3,352,256]{2,1,0:T(8,128)(2,1)}, u32[]{:S(2)}, u32[]{:S(2)}) collective-permute-start(bf16[3,352,256]{2,1,0:T(8,128)(2,1)} %collective-permute-done.33.refs_2_), channel_id=1, source_target_pairs={{0,8},{8,16},{16,24},{24,0},{1,9},{9,17},{17,25},{25,1},{2,10},{10... | collective-permute-start | bytes 1622024 | tf_op jit(solution)/shard_map/ppermute | solution.py:24
  169.9 27.1 %collective-permute-start.50 = (bf16[3,352,256]{2,1,0:T(8,128)(2,1)}, bf16[3,352,256]{2,1,0:T(8,128)(2,1)}, u32[]{:S(2)}, u32[]{:S(2)}) collective-permute-start(bf16[3,352,256]{2,1,0:T(8,128)(2,1)} %collective-permute-done.34.refs_3_), channel_id=1, source_target_pairs={{0,1},{1,0},{2,3},{3,2},{4,5},{5,4},{6,7},{7,6},{8,9},{9,8},{10,11... | collective-permute-start | bytes 1622024 | tf_op jit(solution)/shard_map/ppermute | solution.py:32
  179.1 17.9 %collective-permute-start.43 = (bf16[3,352,256]{2,1,0:T(8,128)(2,1)}, bf16[3,352,256]{2,1,0:T(8,128)(2,1)}, u32[]{:S(2)}, u32[]{:S(2)}) collective-permute-start(bf16[3,352,256]{2,1,0:T(8,128)(2,1)} %collective-permute-done.34.refs_3_), channel_id=1, source_target_pairs={{0,24},{8,0},{16,8},{24,16},{1,25},{9,1},{17,9},{25,17},{2,26},{10... | collective-permute-start | bytes 1622024 | tf_op jit(solution)/shard_map/ppermute | solution.py:24
  179.7 18.3 %collective-permute-start.38 = (bf16[3,352,256]{2,1,0:T(8,128)(2,1)}, bf16[3,352,256]{2,1,0:T(8,128)(2,1)}, u32[]{:S(2)}, u32[]{:S(2)}) collective-permute-start(bf16[3,352,256]{2,1,0:T(8,128)(2,1)} %collective-permute-done.34.refs_3_), channel_id=1, source_target_pairs={{0,8},{8,16},{16,24},{24,0},{1,9},{9,17},{17,25},{25,1},{2,10},{10... | collective-permute-start | bytes 1622024 | tf_op jit(solution)/shard_map/ppermute | solution.py:24
  181.6 17.4 %collective-permute-start.59 = (bf16[3,352,256]{2,1,0:T(8,128)(2,1)}, bf16[3,352,256]{2,1,0:T(8,128)(2,1)}, u32[]{:S(2)}, u32[]{:S(2)}) collective-permute-start(bf16[3,352,256]{2,1,0:T(8,128)(2,1)} %collective-permute-done.45.refs_12_), channel_id=1, source_target_pairs={{0,1},{1,0},{2,3},{3,2},{4,5},{5,4},{6,7},{7,6},{8,9},{9,8},{10,11... | collective-permute-start | bytes 1622024 | tf_op jit(solution)/shard_map/ppermute | solution.py:32
  192.0 48.6 %all-to-all-start.1 = ((bf16[16,48,1152]{2,1,0:T(8,128)(2,1)}), bf16[16,48,1152]{2,1,0:T(8,128)(2,1)S(1)}, u32[]{:S(2)}, u32[]{:S(2)}) async-start(bf16[16,48,1152]{2,1,0:T(8,128)(2,1)} %shard_map.67), calls=%async_computation.1 | async-start | bytes 3538944 | tf_op jit(solution)/shard_map/all_to_all | solution.py:20
  198.0 16.0 %collective-permute-start.52 = (bf16[3,352,256]{2,1,0:T(8,128)(2,1)}, bf16[3,352,256]{2,1,0:T(8,128)(2,1)S(1)}, u32[]{:S(2)}, u32[]{:S(2)}) collective-permute-start(bf16[3,352,256]{2,1,0:T(8,128)(2,1)} %copy-done.10), channel_id=1, source_target_pairs={{0,1},{1,0},{2,3},{3,2},{4,5},{5,4},{6,7},{7,6},{8,9},{9,8},{10,11... | collective-permute-start | bytes 1622024 | tf_op jit(solution)/shard_map/ppermute | solution.py:32
  199.0 24.7 %collective-permute-start.40 = (bf16[3,352,256]{2,1,0:T(8,128)(2,1)}, bf16[3,352,256]{2,1,0:T(8,128)(2,1)}, u32[]{:S(2)}, u32[]{:S(2)}) collective-permute-start(bf16[3,352,256]{2,1,0:T(8,128)(2,1)} %copy-done.10), channel_id=1, source_target_pairs={{0,8},{8,16},{16,24},{24,0},{1,9},{9,17},{17,25},{25,1},{2,10},{10... | collective-permute-start | bytes 1622024 | tf_op jit(solution)/shard_map/ppermute | solution.py:24
  199.3 24.4 %collective-permute-start.61 = (bf16[3,352,256]{2,1,0:T(8,128)(2,1)}, bf16[3,352,256]{2,1,0:T(8,128)(2,1)}, u32[]{:S(2)}, u32[]{:S(2)}) collective-permute-start(bf16[3,352,256]{2,1,0:T(8,128)(2,1)} %copy-done.12), channel_id=1, source_target_pairs={{0,1},{1,0},{2,3},{3,2},{4,5},{5,4},{6,7},{7,6},{8,9},{9,8},{10,11... | collective-permute-start | bytes 1622024 | tf_op jit(solution)/shard_map/ppermute | solution.py:32
  223.7 15.8 %collective-permute-start.54 = (bf16[3,352,256]{2,1,0:T(8,128)(2,1)}, bf16[3,352,256]{2,1,0:T(8,128)(2,1)}, u32[]{:S(2)}, u32[]{:S(2)}) collective-permute-start(bf16[3,352,256]{2,1,0:T(8,128)(2,1)} %collective-permute-done.38.refs_7_), channel_id=1, source_target_pairs={{0,1},{1,0},{2,3},{3,2},{4,5},{5,4},{6,7},{7,6},{8,9},{9,8},{10,11... | collective-permute-start | bytes 1622024 | tf_op jit(solution)/shard_map/ppermute | solution.py:32
  252.9 31.0 %all-to-all-start.2 = ((bf16[16,48,1024]{2,1,0:T(8,128)(2,1)}), bf16[16,48,1024]{2,1,0:T(8,128)(2,1)S(1)}, u32[]{:S(2)}, u32[]{:S(2)}) async-start(bf16[16,48,1024]{2,1,0:T(8,128)(2,1)} %get-tuple-element.48), calls=%async_computation.2 | async-start | bytes 3145728 | tf_op jit(solution)/shard_map/all_to_all | solution.py:20
  (71 other events, 703.8 us)

commit v3 on v2

--- a/solution.py
+++ b/solution.py
@@ -18,6 +18,10 @@
 
 def exchange(parts, axes):
     return lax.all_to_all(parts, axes, 0, 0, tiled=True)
+
+
+def share(block, axes, peers):
+    return exchange(jnp.broadcast_to(block[None], (peers, *block.shape)), axes)
 
 
 def shift(block, axis, step):
@@ -135,10 +139,15 @@
     n, half = rows[0].shape[1], mine[0].shape[1]
     block = own_out.shape[0]
     lanes = [pl.ds(pl.multiple_of(behind(x, m) * 256, 256), 256) for m in range(4)]
+
+    def slot(b):
+        ahead = lax.rem(b + 4 - z, 4)
+        return jnp.where(ahead == 0, 3, jnp.where(ahead == 1, 1, jnp.where(ahead == 2, 0, 2)))
+
     copies = []
     for j in range(4):
         for m in range(4):
-            copies.append((rows[j].at[m], stream.at[behind(y, j), :, lanes[m]]))
+            copies.append((rows[j].at[m], stream.at[slot(behind(y, j)), :, lanes[m]]))
     for g in range(2):
         for m in range(4):
             for s, piece in enumerate((mine[m], theirs[m])):
@@ -147,20 +156,27 @@
     started = run_copies(copies, sems)
     for copy in started[:24]:
         copy.wait()
-    own_out[...] = stream[x, pl.ds(pl.multiple_of(y * block, 16), block), :]
-    whole = stream[...].reshape(4 * n, 1024)
-    for g in range(2):
-        at = slice(2 * g * half, 2 * g * half + 2 * half)
-        if g == 1:
-            for copy in started[24:]:
-                copy.wait()
-        partial[:, :, at] = dot_nt(whole, weights[at]).astype(BF16).reshape(4, n, 2 * half)
-    copies = [(partial.at[z], outs[0])]
-    for k in range(1, 4):
-        for h in range(2):
-            src = partial.at[lax.rem(z + k, 4), h * n // 2 : h * n // 2 + n // 2]
-            copies.append((src, outs[2 * k - 1 + h]))
-    for copy in run_copies(copies, out_sems):
+    own_out[...] = stream[slot(x), pl.ds(pl.multiple_of(y * block, 16), block), :]
+    sent = []
+    for part in range(2):
+        picked = stream[2 * part : 2 * part + 2].reshape(2 * n, 1024)
+        for g in range(2):
+            at = slice(2 * g * half, 2 * g * half + 2 * half)
+            if part == 0 and g == 1:
+                for copy in started[24:]:
+                    copy.wait()
+            partial[2 * part : 2 * part + 2, :, at] = dot_nt(picked, weights[at]).astype(BF16).reshape(2, n, 2 * half)
+        for s in (2 * part, 2 * part + 1):
+            k = (2, 1, 3, 0)[s]
+            if k == 0:
+                copies = [(partial.at[s], outs[0])]
+            else:
+                copies = [(partial.at[s, h * n // 2 : h * n // 2 + n // 2], outs[2 * k - 1 + h]) for h in range(2)]
+            for src, dst in copies:
+                copy = pltpu.make_async_copy(src, dst, out_sems.at[len(sent)])
+                copy.start()
+                sent.append(copy)
+    for copy in sent:
         copy.wait()
 
 
@@ -223,7 +239,7 @@
     return high, middle, (rest - middle.astype(F32)).astype(BF16)
 
 
-def norm_kernel(branch, own, out, message, sems):
+def norm_kernel(branch, own, out, message):
     mixed = RESIDUAL * own[...].astype(F32)
     for i in range(branch.shape[0]):
         mixed += branch[i].astype(F32)
@@ -236,8 +252,9 @@
     for i, part in enumerate(parts_of(mean) + parts_of((mixed * mixed).sum(axis=1, keepdims=True))):
         tail = jnp.where(lane == i, part.astype(F32), tail)
     message[:, cols:] = tail.astype(BF16)
-    for copy in run_copies([(message, out.at[i]) for i in range(out.shape[0])], sems):
-        copy.wait()
+    whole = message[...]
+    for i in range(out.shape[0]):
+        out[i] = whole
 
 
 def norm_message(branch, own):
@@ -246,8 +263,8 @@
         norm_kernel,
         out_shape=sds(16, n, cols + 128),
         in_specs=[VMEM] * 2,
-        out_specs=ANY,
-        scratch_shapes=[pltpu.VMEM((n, cols + 128), BF16), pltpu.SemaphoreType.DMA((16,))],
+        out_specs=VMEM,
+        scratch_shapes=[pltpu.VMEM((n, cols + 128), BF16)],
         compiler_params=pltpu.CompilerParams(vmem_limit_bytes=16 << 20),
     )(branch, own)
 
@@ -274,6 +291,7 @@
         pltpu.make_async_copy(weights.at[g], weights.at[g], sems.at[g]).wait()
 
     load(0)
+    load(1)
     for copy in row_copies:
         copy.wait()
     means, squares = [], []
@@ -295,9 +313,8 @@
 
     lax.fori_loop(0, 4, normalise, 0)
     own_out[...] = stream[pl.ds(pl.multiple_of(y * n, 16), n), pl.ds(pl.multiple_of(z * 1024, 1024), 1024)]
+    load(2)
     loaded(0)
-    load(1)
-    load(2)
     gate = dot_nt(stream[...], weights[0])
     gate = gate * jax.nn.sigmoid(gate)
     loaded(1)
@@ -418,13 +435,13 @@
     parts, own = block_layer(place, stream, spread, w1 + w1_core)
     branch = exchange(parts, ("z", "y")).astype(F32).sum(axis=0)
     mixed = RESIDUAL * own.astype(F32) + branch
-    stats = share4(row_stats(mixed), "z")
-    stats = (stats[0] + stats[2]) + (stats[1] + stats[3])
+    stats = share(row_stats(mixed), "z", 4).sum(axis=0)
     out = normed(mixed, stats[0], stats[1], affine[1], affine[3])
     parts = jnp.broadcast_to(out.reshape(block, 4, 1, 256).transpose(1, 2, 0, 3), (4, 4, block, 256))
     ours = exchange(parts.reshape(16, block, 256), ("x", "y")).reshape(half, 256)
     theirs = swap_core(ours)
-    return jnp.where(c == 0, jnp.concatenate((ours, theirs)), jnp.concatenate((theirs, ours)))
+    whole = lax.dynamic_update_slice_in_dim(jnp.zeros((2 * half, 256), BF16), ours, c * half, 0)
+    return lax.dynamic_update_slice_in_dim(whole, theirs, (1 - c) * half, 0)
 
 
 def solution(mesh):

time: 310 us -> 315 us (1.016)
  waiting for transfers between devices: 115 us -> 136 us
  starting transfers between devices: 140 us -> 120 us
  local copies, waits for them, and re-layouts: 3.96 us -> 8.09 us
    ppermute x25, starting transfers between devices: 65.4 us -> 39.4 us  [swap_core(): return lax.ppermute(block, 'c', [(0, 1), (1, 0)])]
    ppermute x42 -> x39, waiting for transfers between devices: 87.7 us -> 102 us  [shift(): return lax.ppermute(block, axis, [(i, (i + step) % 4) for i in range(4)])]
    ppermute x42 -> x39, starting transfers between devices: 46.4 us -> 54.1 us  [shift(): return lax.ppermute(block, axis, [(i, (i + step) % 4) for i in range(4)])]
    all_to_all x3 -> x4, waiting for transfers between devices: 23.9 us -> 28.1 us  [exchange(): return lax.all_to_all(parts, axes, 0, 0, tiled=True)]
    all_to_all x3 -> x4, starting transfers between devices: 28.1 us -> 26.8 us  [exchange(): return lax.all_to_all(parts, axes, 0, 0, tiled=True)]
  transfers between devices with their start and end apart: 70 -> 68, of which waited for: 23 -> 25; matrix products, arithmetic and copies ran while one was open for 1% -> 1% of each run, Pallas kernels for 4% -> 4%
where the time goes in v3:
time: 315 us; the launch traced here: 314 us
  waiting for transfers between devices  136 us (43%)
  starting transfers between devices  120 us (38%)
  Pallas kernels  31.9 us (10%)
  blocking collectives  13.3 us (4%)
  local copies, waits for them, and re-layouts  8.09 us (3%)
  other arithmetic  4.51 us (1%)
    ppermute x39, waiting for transfers between devices, shift(): return lax.ppermute(block, axis, [(i, (i + step) % 4) for i in range(4)])  102 us
    ppermute x39, starting transfers between devices, shift(): return lax.ppermute(block, axis, [(i, (i + step) % 4) for i in range(4)])  54.1 us
    ppermute x25, starting transfers between devices, swap_core(): return lax.ppermute(block, 'c', [(0, 1), (1, 0)])  39.4 us
    all_to_all x4, waiting for transfers between devices, exchange(): return lax.all_to_all(parts, axes, 0, 0, tiled=True)  28.1 us
    all_to_all x4, starting transfers between devices, exchange(): return lax.all_to_all(parts, axes, 0, 0, tiled=True)  26.8 us
    all_to_all x1, blocking collectives, exchange(): return lax.all_to_all(parts, axes, 0, 0, tiled=True)  13.3 us
    pallas_call x1, Pallas kernels, block_layer(): pl.pallas_call(block_kernel, out_shape=[sds(16, n, 1024), sds(n, 1024)],...  11.9 us
    pallas_call x1, Pallas kernels, gate_up(): pl.pallas_call(gate_up_kernel, out_shape=[sds(n, 4 * half)] + [sds(n // 2...  7.87 us
  transfers between devices with their start and end apart: 68, of which 25 were waited for; matrix products, arithmetic and copies ran while one was open for 1% of the time, Pallas kernels for 4%

profile of v3, /device:TPU:1, one launch (start us, length us, event | category | flops | bytes accessed | tf_op | source)
XLA Modules:
  0.0 314.4 jit_solution(3070035968005391764)
XLA Ops:
  8.2 3.3 %shard_map.64 = (bf16[2,352,256]{2,1,0:T(8,128)(2,1)}, bf16[2,352,256]{2,1,0:T(8,128)(2,1)}, bf16[2,352,256]{2,1,0:T(8,128)(2,1)}, bf16[2,352,256]{2,1,0:T(8,128...) custom-call(s32[4]{0:T(128)} %pad_add_fusion.place_ref, ...), custom_call_target="tpu_custom_call" | custom-call | tf_op jit(solution)/shard_map/pallas_call | solution.py:120
  17.9 4.7 %collective-permute-done.6.refs_5_ = bf16[2,352,256]{2,1,0:T(8,128)(2,1)S(1)} collective-permute-done((bf16[2,352,256]{2,1,0:T(8,128)(2,1)}, bf16[2,352,256]{2,1,0:T(8,128)(2,1)S(1)}, u32[]{:S(2)}, u32[]{:S(2)}) %collective-permute-start.6) | collective-permute-done | bytes 360480 | tf_op jit(solution)/shard_map/ppermute | solution.py:28
  22.6 2.9 collective-permute-start.4
  30.7 5.1 %collective-permute-start.10 = (bf16[2,352,256]{2,1,0:T(8,128)(2,1)S(1)}, bf16[2,352,256]{2,1,0:T(8,128)(2,1)S(1)}, u32[]{:S(2)}, u32[]{:S(2)}) collective-permute-start(bf16[2,352,256]{2,1,0:T(8,128)(2,1)S(1)} %collective-permute-done.6.refs_5_), channel_id=1, source_target_pairs={{0,1},{1,0},{2,3},{3,2},{4,5},{5,4},{6,7},{7,6},{8,9},{9,8},{10,11... | collective-permute-start | bytes 1081352 | tf_op jit(solution)/shard_map/ppermute | solution.py:36
  39.1 7.9 %shard_map.65 = (bf16[192,1408]{1,0:T(8,128)(2,1)}, bf16[96,1408]{1,0:T(8,128)(2,1)}, bf16[96,1408]{1,0:T(8,128)(2,1)}, bf16[96,1408]{1,0:T(8,128)(2,1)}, bf16[9...) custom-call(s32[4]{0:T(128)} %pad_add_fusion.place_ref, ...), custom_call_target="tpu_custom_call" | custom-call | tf_op jit(solution)/shard_map/pallas_call | solution.py:185
  47.0 3.8 %collective-permute-start.17 = (bf16[96,1408]{1,0:T(8,128)(2,1)}, bf16[96,1408]{1,0:T(8,128)(2,1)S(1)}, u32[]{:S(2)}, u32[]{:S(2)}) collective-permute-start(bf16[96,1408]{1,0:T(8,128)(2,1)} %get-tuple-element.37), channel_id=1, source_target_pairs={{0,96},{32,0},{64,32},{96,64},{1,97},{33,1},{65,33},{97,65},{2,98}... | collective-permute-start | bytes 811016 | tf_op jit(solution)/shard_map/ppermute | solution.py:28
  55.5 3.1 collective-permute-start.18
  64.1 5.3 %collective-permute-done.31 = f32[2,1024]{1,0:T(2,128)S(1)} collective-permute-done((f32[2,1024]{1,0:T(2,128)S(1)}, f32[2,1024]{1,0:T(2,128)S(1)}, u32[]{:S(2)}, u32[]{:S(2)}) %collective-permute-start.31) | collective-permute-done | bytes 8224 | tf_op jit(solution)/shard_map/ppermute | solution.py:28
  69.5 3.9 %collective-permute-done.30 = f32[2,1024]{1,0:T(2,128)S(1)} collective-permute-done((f32[2,1024]{1,0:T(2,128)S(1)}, f32[2,1024]{1,0:T(2,128)S(1)}, u32[]{:S(2)}, u32[]{:S(2)}) %collective-permute-start.30) | collective-permute-done | bytes 8224 | tf_op jit(solution)/shard_map/ppermute | solution.py:28
  73.5 3.2 %collective-permute-start.22 = (bf16[352,256]{1,0:T(8,128)(2,1)S(1)}, bf16[352,256]{1,0:T(8,128)(2,1)S(1)}, u32[]{:S(2)}, u32[]{:S(2)}) collective-permute-start(bf16[352,256]{1,0:T(8,128)(2,1)S(1)} %copy-done.37), channel_id=1, source_target_pairs={{0,8},{8,16},{16,24},{24,0},{1,9},{9,17},{17,25},{25,1},{2,10},{10... | collective-permute-start | bytes 540680 | tf_op jit(solution)/shard_map/ppermute | solution.py:28
  76.7 3.5 %shard_map.68 = (bf16[3,352,256]{2,1,0:T(8,128)(2,1)}, bf16[3,352,256]{2,1,0:T(8,128)(2,1)}, bf16[3,352,256]{2,1,0:T(8,128)(2,1)}, bf16[3,352,256]{2,1,0:T(8,128)(2,1)}) custom-call(s32[4]{0:T(128)} %pad_add_fusion.place_ref, bf16[2,256,1408]{2,1,0:T(8,128)(2,1)} %gate_ref.3, bf16[2,256,1408]{2,1,0:T(8,128)(2,1)} %up_ref.3, bf16[2,1408,256]{2,1,0:T(8,128)(2,1)} %down_ref.3), custom_call_target="tpu_custom_call" | custom-call | tf_op jit(solution)/shard_map/pallas_call | solution.py:90
  85.4 9.1 %collective-permute-start.25 = (bf16[352,256]{1,0:T(8,128)(2,1)S(1)}, bf16[352,256]{1,0:T(8,128)(2,1)S(1)}, u32[]{:S(2)}, u32[]{:S(2)}) collective-permute-start(bf16[352,256]{1,0:T(8,128)(2,1)S(1)} %copy-done.1), channel_id=1, source_target_pairs={{0,1},{1,0},{2,3},{3,2},{4,5},{5,4},{6,7},{7,6},{8,9},{9,8},{10,11... | collective-permute-start | bytes 540680 | tf_op jit(solution)/shard_map/ppermute | solution.py:36
  94.9 5.1 %collective-permute-start.27 = (bf16[352,256]{1,0:T(8,128)(2,1)S(1)}, bf16[352,256]{1,0:T(8,128)(2,1)S(1)}, u32[]{:S(2)}, u32[]{:S(2)}) collective-permute-start(bf16[352,256]{1,0:T(8,128)(2,1)S(1)} %collective-permute-done.23.refs_6_), channel_id=1, source_target_pairs={{0,1},{1,0},{2,3},{3,2},{4,5},{5,4},{6,7},{7,6},{8,9},{9,8},{10,11... | collective-permute-start | bytes 540680 | tf_op jit(solution)/shard_map/ppermute | solution.py:36
  100.3 2.9 collective-permute-start.20
  110.1 5.8 %collective-permute-done.19.refs_1_ = bf16[192,704]{1,0:T(8,128)(2,1)S(1)} collective-permute-done((bf16[192,704]{1,0:T(8,128)(2,1)S(1)}, bf16[192,704]{1,0:T(8,128)(2,1)S(1)}, u32[]{:S(2)}, u32[]{:S(2)}) %collective-permute-start.19) | collective-permute-done | bytes 270368 | tf_op jit(solution)/shard_map/ppermute | solution.py:28
  116.2 6.2 %collective-permute-done.20.refs_2_ = bf16[192,704]{1,0:T(8,128)(2,1)S(1)} collective-permute-done((bf16[192,704]{1,0:T(8,128)(2,1)S(1)}, bf16[192,704]{1,0:T(8,128)(2,1)S(1)}, u32[]{:S(2)}, u32[]{:S(2)}) %collective-permute-start.20) | collective-permute-done | bytes 270368 | tf_op jit(solution)/shard_map/ppermute | solution.py:28
  126.5 3.7 %shard_map.66 = bf16[768,1024]{1,0:T(8,128)(2,1)} custom-call(s32[4]{0:T(128)S(1)} %copy-done.3, bf16[192,704]{1,0:T(8,128)(2,1)S(1)} %fusion.2.refs_0_, bf16[192,704]{1,0:T(8,128)(2,1)S(1)} %collective-permute-done.19.refs_1_, bf16[192,704]{1,0:T(8,128)(2,1)S(1)} %collective-permute-done.20.refs_2_, bf16[192,704]{1,0:T(8,128)(2,1)S(1)} %collective-permute-done.21.refs_3_, ...), custom_call_target="tpu_custom_call" | custom-call | tf_op jit(solution)/shard_map/pallas_call | solution.py:221
  130.2 15.9 %all-to-all-start = ((bf16[16,48,1024]{2,1,0:T(8,128)(2,1)}), bf16[16,48,1024]{2,1,0:T(8,128)(2,1)S(1)}, u32[]{:S(2)}, u32[]{:S(2)}) async-start(bf16[16,48,1024]{2,1,0:T(8,128)(2,1)} %bitcast.8), calls=%async_computation | async-start | bytes 3145728 | tf_op jit(solution)/shard_map/all_to_all | solution.py:20
  151.8 26.3 %collective-permute-done.36.refs_5_ = bf16[3,352,256]{2,1,0:T(8,128)(2,1)S(1)} collective-permute-done((bf16[3,352,256]{2,1,0:T(8,128)(2,1)}, bf16[3,352,256]{2,1,0:T(8,128)(2,1)S(1)}, u32[]{:S(2)}, u32[]{:S(2)}) %collective-permute-start.36) | collective-permute-done | bytes 540704 | tf_op jit(solution)/shard_map/ppermute | solution.py:28
  179.5 9.2 %collective-permute-done.43.refs_15_ = bf16[3,352,256]{2,1,0:T(8,128)(2,1)S(1)} collective-permute-done((bf16[3,352,256]{2,1,0:T(8,128)(2,1)}, bf16[3,352,256]{2,1,0:T(8,128)(2,1)S(1)}, u32[]{:S(2)}, u32[]{:S(2)}) %collective-permute-start.43) | collective-permute-done | bytes 540704 | tf_op jit(solution)/shard_map/ppermute | solution.py:28
  194.5 3.8 %all-to-all-start.1 = ((bf16[16,48,1152]{2,1,0:T(8,128)(2,1)}), bf16[16,48,1152]{2,1,0:T(8,128)(2,1)S(1)}, u32[]{:S(2)}, u32[]{:S(2)}) async-start(bf16[16,48,1152]{2,1,0:T(8,128)(2,1)} %shard_map.67), calls=%async_computation.1 | async-start | bytes 3538944 | tf_op jit(solution)/shard_map/all_to_all | solution.py:20
  198.3 3.0 collective-permute-done.37.refs_6_
  203.3 9.7 %collective-permute-done.38.refs_7_ = bf16[3,352,256]{2,1,0:T(8,128)(2,1)} collective-permute-done((bf16[3,352,256]{2,1,0:T(8,128)(2,1)}, bf16[3,352,256]{2,1,0:T(8,128)(2,1)}, u32[]{:S(2)}, u32[]{:S(2)}) %collective-permute-start.38) | collective-permute-done | bytes 540704 | tf_op jit(solution)/shard_map/ppermute | solution.py:28
  217.9 11.1 %collective-permute-done.40.refs_9_ = bf16[3,352,256]{2,1,0:T(8,128)(2,1)} collective-permute-done((bf16[3,352,256]{2,1,0:T(8,128)(2,1)S(1)}, bf16[3,352,256]{2,1,0:T(8,128)(2,1)}, u32[]{:S(2)}, u32[]{:S(2)}) %collective-permute-start.40) | collective-permute-done | bytes 540704 | tf_op jit(solution)/shard_map/ppermute | solution.py:28
  230.6 9.1 %collective-permute-done.44.refs_11_ = bf16[3,352,256]{2,1,0:T(8,128)(2,1)} collective-permute-done((bf16[3,352,256]{2,1,0:T(8,128)(2,1)}, bf16[3,352,256]{2,1,0:T(8,128)(2,1)}, u32[]{:S(2)}, u32[]{:S(2)}) %collective-permute-start.44) | collective-permute-done | bytes 540704 | tf_op jit(solution)/shard_map/ppermute | solution.py:28
  247.0 11.9 %shard_map.69 = (bf16[16,48,1024]{2,1,0:T(8,128)(2,1)}, bf16[48,1024]{1,0:T(8,128)(2,1)}) custom-call(s32[4]{0:T(128)} %pad_add_fusion.place_ref, bf16[16,48,1152]{2,1,0:T(8,128)(2,1)S(1)} %all-to-all-done.1.rows_ref, f32[2,4096]{1,0:T(2,128)} %bitcast.51, bf16[3,352,256]{2,1,0:T(8,128)(2,1)} %get-tuple-element.43.refs_0_, bf16[3,352,256]{2,1,0:T(8,128)(2,1)} %copy-done.7, ...), custom_call_target="tpu_custom_call" | custom-call | tf_op jit(solution)/shard_map/pallas_call | solution.py:335
  258.9 3.8 %all-to-all-start.2 = ((bf16[16,48,1024]{2,1,0:T(8,128)(2,1)}), bf16[16,48,1024]{2,1,0:T(8,128)(2,1)S(1)}, u32[]{:S(2)}, u32[]{:S(2)}) async-start(bf16[16,48,1024]{2,1,0:T(8,128)(2,1)} %get-tuple-element.48), calls=%async_computation.2 | async-start | bytes 3145728 | tf_op jit(solution)/shard_map/all_to_all | solution.py:20
  262.8 24.0 %all-to-all-done.2 = bf16[16,48,1024]{2,1,0:T(8,128)(2,1)S(1)} async-done(((bf16[16,48,1024]{2,1,0:T(8,128)(2,1)}), bf16[16,48,1024]{2,1,0:T(8,128)(2,1)S(1)}, u32[]{:S(2)}, u32[]{:S(2)}) %all-to-all-start.2) | async-done | bytes 1572896 | tf_op jit(solution)/shard_map/all_to_all | solution.py:20
  287.8 3.2 %all-to-all-start.3 = ((f32[4,2,48]{2,1,0:T(2,128)}), f32[4,2,48]{2,1,0:T(2,128)S(1)}, u32[]{:S(2)}, u32[]{:S(2)}) async-start(f32[4,2,48]{2,1,0:T(2,128)} %broadcast_in_dim.23), calls=%async_computation.3 | async-start | bytes 8192 | tf_op jit(solution)/shard_map/all_to_all | solution.py:20
  291.1 4.1 %all-to-all-done.3 = f32[4,2,48]{2,1,0:T(2,128)S(1)} async-done(((f32[4,2,48]{2,1,0:T(2,128)}), f32[4,2,48]{2,1,0:T(2,128)S(1)}, u32[]{:S(2)}, u32[]{:S(2)}) %all-to-all-start.3) | async-done | bytes 1568 | tf_op jit(solution)/shard_map/all_to_all | solution.py:20
  295.4 13.3 %all_to_all.25 = bf16[16,48,256]{2,1,0:T(8,128)(2,1)S(1)} all-to-all(bf16[16,48,256]{2,1,0:T(8,128)(2,1)S(1)} %bitcast.41), channel_id=1, replica_groups=mesh['z'=4,'x'=4,'y'=4,'c'=2] {'x','y'}, dimensions={0} | all-to-all | bytes 786432 | tf_op jit(solution)/shard_map/all_to_all | solution.py:20
  308.7 3.6 %collective-permute-start.63 = (bf16[768,256]{1,0:T(8,128)(2,1)S(1)}, bf16[768,256]{1,0:T(8,128)(2,1)S(1)}, u32[]{:S(2)}, u32[]{:S(2)}) collective-permute-start(bf16[768,256]{1,0:T(8,128)(2,1)S(1)} %bitcast.39), channel_id=1, source_target_pairs={{0,1},{1,0},{2,3},{3,2},{4,5},{5,4},{6,7},{7,6},{8,9},{9,8},{10,11... | collective-permute-start | bytes 1179656 | tf_op jit(solution)/shard_map/ppermute | solution.py:36
  (232 shorter events, 82.3 us)
Async XLA Ops:
  11.8 16.1 %collective-permute-start.7 = (bf16[2,352,256]{2,1,0:T(8,128)(2,1)}, bf16[2,352,256]{2,1,0:T(8,128)(2,1)S(1)}, u32[]{:S(2)}, u32[]{:S(2)}) collective-permute-start(bf16[2,352,256]{2,1,0:T(8,128)(2,1)} %get-tuple-element.29), channel_id=1, source_target_pairs={{0,16},{8,24},{16,0},{24,8},{1,17},{9,25},{17,1},{25,9},{2,18},{10... | collective-permute-start | bytes 1081352 | tf_op jit(solution)/shard_map/ppermute | solution.py:28
  12.7 18.0 %collective-permute-start.8 = (bf16[2,352,256]{2,1,0:T(8,128)(2,1)}, bf16[2,352,256]{2,1,0:T(8,128)(2,1)S(1)}, u32[]{:S(2)}, u32[]{:S(2)}) collective-permute-start(bf16[2,352,256]{2,1,0:T(8,128)(2,1)} %get-tuple-element.30), channel_id=1, source_target_pairs={{0,24},{8,0},{16,8},{24,16},{1,25},{9,1},{17,9},{25,17},{2,26},{10... | collective-permute-start | bytes 1081352 | tf_op jit(solution)/shard_map/ppermute | solution.py:28
  14.3 21.4 %collective-permute-start.9 = (bf16[2,352,256]{2,1,0:T(8,128)(2,1)}, bf16[2,352,256]{2,1,0:T(8,128)(2,1)S(1)}, u32[]{:S(2)}, u32[]{:S(2)}) collective-permute-start(bf16[2,352,256]{2,1,0:T(8,128)(2,1)} %get-tuple-element.27.refs_4_), channel_id=1, source_target_pairs={{0,1},{1,0},{2,3},{3,2},{4,5},{5,4},{6,7},{7,6},{8,9},{9,8},{10,11... | collective-permute-start | bytes 1081352 | tf_op jit(solution)/shard_map/ppermute | solution.py:36
  16.5 19.3 %collective-permute-start.3 = (bf16[4,192,256]{2,1,0:T(8,128)(2,1)S(1)}, bf16[4,192,256]{2,1,0:T(8,128)(2,1)S(1)}, u32[]{:S(2)}, u32[]{:S(2)}) collective-permute-start(bf16[4,192,256]{2,1,0:T(8,128)(2,1)S(1)} %slice.78.refs_0_), channel_id=1, source_target_pairs={{0,2},{2,4},{4,6},{6,0},{1,3},{3,5},{5,7},{7,1},{8,10},{10,12},{12... | collective-permute-start | bytes 1179656 | tf_op jit(solution)/shard_map/ppermute | solution.py:28
  50.8 32.8 %collective-permute-start.13 = (bf16[96,1408]{1,0:T(8,128)(2,1)}, bf16[96,1408]{1,0:T(8,128)(2,1)S(1)}, u32[]{:S(2)}, u32[]{:S(2)}) collective-permute-start(bf16[96,1408]{1,0:T(8,128)(2,1)} %get-tuple-element.32), channel_id=1, source_target_pairs={{0,96},{32,0},{64,32},{96,64},{1,97},{33,1},{65,33},{97,65},{2,98}... | collective-permute-start | bytes 811016 | tf_op jit(solution)/shard_map/ppermute | solution.py:28
  53.5 31.9 %collective-permute-start.16 = (bf16[96,1408]{1,0:T(8,128)(2,1)}, bf16[96,1408]{1,0:T(8,128)(2,1)S(1)}, u32[]{:S(2)}, u32[]{:S(2)}) collective-permute-start(bf16[96,1408]{1,0:T(8,128)(2,1)} %get-tuple-element.35), channel_id=1, source_target_pairs={{0,32},{32,64},{64,96},{96,0},{1,33},{33,65},{65,97},{97,1},{2,34}... | collective-permute-start | bytes 811016 | tf_op jit(solution)/shard_map/ppermute | solution.py:28
  55.5 38.9 %collective-permute-start.18 = (bf16[96,1408]{1,0:T(8,128)(2,1)S(1)}, bf16[96,1408]{1,0:T(8,128)(2,1)S(1)}, u32[]{:S(2)}, u32[]{:S(2)}) collective-permute-start(bf16[96,1408]{1,0:T(8,128)(2,1)S(1)} %add_convert_fusion), channel_id=1, source_target_pairs={{0,96},{32,0},{64,32},{96,64},{1,97},{33,1},{65,33},{97,65},{2,98}... | collective-permute-start | bytes 811016 | tf_op jit(solution)/shard_map/ppermute | solution.py:28
  59.6 34.9 %collective-permute-start.15 = (bf16[96,1408]{1,0:T(8,128)(2,1)S(1)}, bf16[96,1408]{1,0:T(8,128)(2,1)S(1)}, u32[]{:S(2)}, u32[]{:S(2)}) collective-permute-start(bf16[96,1408]{1,0:T(8,128)(2,1)S(1)} %add_convert_fusion.1), channel_id=1, source_target_pairs={{0,32},{32,64},{64,96},{96,0},{1,33},{33,65},{65,97},{97,1},{2,34}... | collective-permute-start | bytes 811016 | tf_op jit(solution)/shard_map/ppermute | solution.py:28
  83.6 16.7 %collective-permute-start.24 = (bf16[352,256]{1,0:T(8,128)(2,1)S(1)}, bf16[352,256]{1,0:T(8,128)(2,1)S(1)}, u32[]{:S(2)}, u32[]{:S(2)}) collective-permute-start(bf16[352,256]{1,0:T(8,128)(2,1)S(1)} %copy-done.35), channel_id=1, source_target_pairs={{0,24},{8,0},{16,8},{24,16},{1,25},{9,1},{17,9},{25,17},{2,26},{10... | collective-permute-start | bytes 540680 | tf_op jit(solution)/shard_map/ppermute | solution.py:28
  100.3 22.1 %collective-permute-start.20 = (bf16[192,704]{1,0:T(8,128)(2,1)S(1)}, bf16[192,704]{1,0:T(8,128)(2,1)S(1)}, u32[]{:S(2)}, u32[]{:S(2)}) collective-permute-start(bf16[192,704]{1,0:T(8,128)(2,1)S(1)} %fusion.2.refs_0_), channel_id=1, source_target_pairs={{0,64},{32,96},{64,0},{96,32},{1,65},{33,97},{65,1},{97,33},{2,66}... | collective-permute-start | bytes 811016 | tf_op jit(solution)/shard_map/ppermute | solution.py:28
  103.2 21.6 %collective-permute-start.21 = (bf16[192,704]{1,0:T(8,128)(2,1)S(1)}, bf16[192,704]{1,0:T(8,128)(2,1)S(1)}, u32[]{:S(2)}, u32[]{:S(2)}) collective-permute-start(bf16[192,704]{1,0:T(8,128)(2,1)S(1)} %fusion.2.refs_0_), channel_id=1, source_target_pairs={{0,96},{32,0},{64,32},{96,64},{1,97},{33,1},{65,33},{97,65},{2,98}... | collective-permute-start | bytes 811016 | tf_op jit(solution)/shard_map/ppermute | solution.py:28
  105.2 40.9 %collective-permute-start.33 = (bf16[3,352,256]{2,1,0:T(8,128)(2,1)}, bf16[3,352,256]{2,1,0:T(8,128)(2,1)}, u32[]{:S(2)}, u32[]{:S(2)}) collective-permute-start(bf16[3,352,256]{2,1,0:T(8,128)(2,1)} %get-tuple-element.45), channel_id=1, source_target_pairs={{0,64},{32,96},{64,0},{96,32},{1,65},{33,97},{65,1},{97,33},{2,66}... | collective-permute-start | bytes 1622024 | tf_op jit(solution)/shard_map/ppermute | solution.py:28
  109.6 38.0 %collective-permute-start.34 = (bf16[3,352,256]{2,1,0:T(8,128)(2,1)}, bf16[3,352,256]{2,1,0:T(8,128)(2,1)}, u32[]{:S(2)}, u32[]{:S(2)}) collective-permute-start(bf16[3,352,256]{2,1,0:T(8,128)(2,1)} %get-tuple-element.46), channel_id=1, source_target_pairs={{0,96},{32,0},{64,32},{96,64},{1,97},{33,1},{65,33},{97,65},{2,98}... | collective-permute-start | bytes 1622024 | tf_op jit(solution)/shard_map/ppermute | solution.py:28
  115.9 33.0 %collective-permute-start.35 = (bf16[3,352,256]{2,1,0:T(8,128)(2,1)S(1)}, bf16[3,352,256]{2,1,0:T(8,128)(2,1)}, u32[]{:S(2)}, u32[]{:S(2)}) collective-permute-start(bf16[3,352,256]{2,1,0:T(8,128)(2,1)S(1)} %copy-done.6), channel_id=1, source_target_pairs={{0,8},{8,16},{16,24},{24,0},{1,9},{9,17},{17,25},{25,1},{2,10},{10... | collective-permute-start | bytes 1622024 | tf_op jit(solution)/shard_map/ppermute | solution.py:28
  122.4 27.8 %collective-permute-start.45 = (bf16[3,352,256]{2,1,0:T(8,128)(2,1)S(1)}, bf16[3,352,256]{2,1,0:T(8,128)(2,1)}, u32[]{:S(2)}, u32[]{:S(2)}) collective-permute-start(bf16[3,352,256]{2,1,0:T(8,128)(2,1)S(1)} %copy-done.6), channel_id=1, source_target_pairs={{0,24},{8,0},{16,8},{24,16},{1,25},{9,1},{17,9},{25,17},{2,26},{10... | collective-permute-start | bytes 1622024 | tf_op jit(solution)/shard_map/ppermute | solution.py:28
  124.8 25.5 %collective-permute-start.47 = (bf16[3,352,256]{2,1,0:T(8,128)(2,1)S(1)}, bf16[3,352,256]{2,1,0:T(8,128)(2,1)}, u32[]{:S(2)}, u32[]{:S(2)}) collective-permute-start(bf16[3,352,256]{2,1,0:T(8,128)(2,1)S(1)} %copy-done.6), channel_id=1, source_target_pairs={{0,1},{1,0},{2,3},{3,2},{4,5},{5,4},{6,7},{7,6},{8,9},{9,8},{10,11... | collective-permute-start | bytes 1622024 | tf_op jit(solution)/shard_map/ppermute | solution.py:36
  130.2 62.7 %all-to-all-start = ((bf16[16,48,1024]{2,1,0:T(8,128)(2,1)}), bf16[16,48,1024]{2,1,0:T(8,128)(2,1)S(1)}, u32[]{:S(2)}, u32[]{:S(2)}) async-start(bf16[16,48,1024]{2,1,0:T(8,128)(2,1)} %bitcast.8), calls=%async_computation | async-start | bytes 3145728 | tf_op jit(solution)/shard_map/all_to_all | solution.py:20
  146.1 32.0 %collective-permute-start.36 = (bf16[3,352,256]{2,1,0:T(8,128)(2,1)}, bf16[3,352,256]{2,1,0:T(8,128)(2,1)S(1)}, u32[]{:S(2)}, u32[]{:S(2)}) collective-permute-start(bf16[3,352,256]{2,1,0:T(8,128)(2,1)} %copy-done.7), channel_id=1, source_target_pairs={{0,8},{8,16},{16,24},{24,0},{1,9},{9,17},{17,25},{25,1},{2,10},{10... | collective-permute-start | bytes 1622024 | tf_op jit(solution)/shard_map/ppermute | solution.py:28
  147.6 30.5 %collective-permute-start.41 = (bf16[3,352,256]{2,1,0:T(8,128)(2,1)}, bf16[3,352,256]{2,1,0:T(8,128)(2,1)S(1)}, u32[]{:S(2)}, u32[]{:S(2)}) collective-permute-start(bf16[3,352,256]{2,1,0:T(8,128)(2,1)} %collective-permute-done.33.refs_2_), channel_id=1, source_target_pairs={{0,24},{8,0},{16,8},{24,16},{1,25},{9,1},{17,9},{25,17},{2,26},{10... | collective-permute-start | bytes 1622024 | tf_op jit(solution)/shard_map/ppermute | solution.py:28
  148.9 39.7 %collective-permute-start.43 = (bf16[3,352,256]{2,1,0:T(8,128)(2,1)}, bf16[3,352,256]{2,1,0:T(8,128)(2,1)S(1)}, u32[]{:S(2)}, u32[]{:S(2)}) collective-permute-start(bf16[3,352,256]{2,1,0:T(8,128)(2,1)} %collective-permute-done.34.refs_3_), channel_id=1, source_target_pairs={{0,24},{8,0},{16,8},{24,16},{1,25},{9,1},{17,9},{25,17},{2,26},{10... | collective-permute-start | bytes 1622024 | tf_op jit(solution)/shard_map/ppermute | solution.py:28
  150.2 40.3 %collective-permute-start.39 = (bf16[3,352,256]{2,1,0:T(8,128)(2,1)}, bf16[3,352,256]{2,1,0:T(8,128)(2,1)S(1)}, u32[]{:S(2)}, u32[]{:S(2)}) collective-permute-start(bf16[3,352,256]{2,1,0:T(8,128)(2,1)} %collective-permute-done.35.refs_4_), channel_id=1, source_target_pairs={{0,8},{8,16},{16,24},{24,0},{1,9},{9,17},{17,25},{25,1},{2,10},{10... | collective-permute-start | bytes 1622024 | tf_op jit(solution)/shard_map/ppermute | solution.py:28
  150.3 41.6 %collective-permute-start.51 = (bf16[3,352,256]{2,1,0:T(8,128)(2,1)}, bf16[3,352,256]{2,1,0:T(8,128)(2,1)S(1)}, u32[]{:S(2)}, u32[]{:S(2)}) collective-permute-start(bf16[3,352,256]{2,1,0:T(8,128)(2,1)} %collective-permute-done.35.refs_4_), channel_id=1, source_target_pairs={{0,1},{1,0},{2,3},{3,2},{4,5},{5,4},{6,7},{7,6},{8,9},{9,8},{10,11... | collective-permute-start | bytes 1622024 | tf_op jit(solution)/shard_map/ppermute | solution.py:36
  178.1 23.3 %collective-permute-start.37 = (bf16[3,352,256]{2,1,0:T(8,128)(2,1)}, bf16[3,352,256]{2,1,0:T(8,128)(2,1)}, u32[]{:S(2)}, u32[]{:S(2)}) collective-permute-start(bf16[3,352,256]{2,1,0:T(8,128)(2,1)} %collective-permute-done.33.refs_2_), channel_id=1, source_target_pairs={{0,8},{8,16},{16,24},{24,0},{1,9},{9,17},{17,25},{25,1},{2,10},{10... | collective-permute-start | bytes 1622024 | tf_op jit(solution)/shard_map/ppermute | solution.py:28
  178.1 34.8 %collective-permute-start.38 = (bf16[3,352,256]{2,1,0:T(8,128)(2,1)}, bf16[3,352,256]{2,1,0:T(8,128)(2,1)}, u32[]{:S(2)}, u32[]{:S(2)}) collective-permute-start(bf16[3,352,256]{2,1,0:T(8,128)(2,1)} %collective-permute-done.34.refs_3_), channel_id=1, source_target_pairs={{0,8},{8,16},{16,24},{24,0},{1,9},{9,17},{17,25},{25,1},{2,10},{10... | collective-permute-start | bytes 1622024 | tf_op jit(solution)/shard_map/ppermute | solution.py:28
  188.6 25.5 %collective-permute-start.46 = (bf16[3,352,256]{2,1,0:T(8,128)(2,1)}, bf16[3,352,256]{2,1,0:T(8,128)(2,1)}, u32[]{:S(2)}, u32[]{:S(2)}) collective-permute-start(bf16[3,352,256]{2,1,0:T(8,128)(2,1)} %copy-done.7), channel_id=1, source_target_pairs={{0,24},{8,0},{16,8},{24,16},{1,25},{9,1},{17,9},{25,17},{2,26},{10... | collective-permute-start | bytes 1622024 | tf_op jit(solution)/shard_map/ppermute | solution.py:28
  190.6 23.6 %collective-permute-start.59 = (bf16[3,352,256]{2,1,0:T(8,128)(2,1)}, bf16[3,352,256]{2,1,0:T(8,128)(2,1)}, u32[]{:S(2)}, u32[]{:S(2)}) collective-permute-start(bf16[3,352,256]{2,1,0:T(8,128)(2,1)} %collective-permute-done.45.refs_12_), channel_id=1, source_target_pairs={{0,1},{1,0},{2,3},{3,2},{4,5},{5,4},{6,7},{7,6},{8,9},{9,8},{10,11... | collective-permute-start | bytes 1622024 | tf_op jit(solution)/shard_map/ppermute | solution.py:36
  192.0 24.8 %collective-permute-start.48 = (bf16[3,352,256]{2,1,0:T(8,128)(2,1)}, bf16[3,352,256]{2,1,0:T(8,128)(2,1)}, u32[]{:S(2)}, u32[]{:S(2)}) collective-permute-start(bf16[3,352,256]{2,1,0:T(8,128)(2,1)} %copy-done.7), channel_id=1, source_target_pairs={{0,1},{1,0},{2,3},{3,2},{4,5},{5,4},{6,7},{7,6},{8,9},{9,8},{10,11... | collective-permute-start | bytes 1622024 | tf_op jit(solution)/shard_map/ppermute | solution.py:36
  194.5 52.5 %all-to-all-start.1 = ((bf16[16,48,1152]{2,1,0:T(8,128)(2,1)}), bf16[16,48,1152]{2,1,0:T(8,128)(2,1)S(1)}, u32[]{:S(2)}, u32[]{:S(2)}) async-start(bf16[16,48,1152]{2,1,0:T(8,128)(2,1)} %shard_map.67), calls=%async_computation.1 | async-start | bytes 3538944 | tf_op jit(solution)/shard_map/all_to_all | solution.py:20
  216.8 23.0 %collective-permute-start.44 = (bf16[3,352,256]{2,1,0:T(8,128)(2,1)}, bf16[3,352,256]{2,1,0:T(8,128)(2,1)}, u32[]{:S(2)}, u32[]{:S(2)}) collective-permute-start(bf16[3,352,256]{2,1,0:T(8,128)(2,1)} %copy-done.11), channel_id=1, source_target_pairs={{0,24},{8,0},{16,8},{24,16},{1,25},{9,1},{17,9},{25,17},{2,26},{10... | collective-permute-start | bytes 1622024 | tf_op jit(solution)/shard_map/ppermute | solution.py:28
  216.9 24.3 %collective-permute-start.55 = (bf16[3,352,256]{2,1,0:T(8,128)(2,1)}, bf16[3,352,256]{2,1,0:T(8,128)(2,1)S(1)}, u32[]{:S(2)}, u32[]{:S(2)}) collective-permute-start(bf16[3,352,256]{2,1,0:T(8,128)(2,1)} %copy-done.12), channel_id=1, source_target_pairs={{0,1},{1,0},{2,3},{3,2},{4,5},{5,4},{6,7},{7,6},{8,9},{9,8},{10,11... | collective-permute-start | bytes 1622024 | tf_op jit(solution)/shard_map/ppermute | solution.py:36
  217.8 23.5 %collective-permute-start.52 = (bf16[3,352,256]{2,1,0:T(8,128)(2,1)S(1)}, bf16[3,352,256]{2,1,0:T(8,128)(2,1)S(1)}, u32[]{:S(2)}, u32[]{:S(2)}) collective-permute-start(bf16[3,352,256]{2,1,0:T(8,128)(2,1)S(1)} %copy-done.9), channel_id=1, source_target_pairs={{0,1},{1,0},{2,3},{3,2},{4,5},{5,4},{6,7},{7,6},{8,9},{9,8},{10,11... | collective-permute-start | bytes 1622024 | tf_op jit(solution)/shard_map/ppermute | solution.py:36
  258.9 27.8 %all-to-all-start.2 = ((bf16[16,48,1024]{2,1,0:T(8,128)(2,1)}), bf16[16,48,1024]{2,1,0:T(8,128)(2,1)S(1)}, u32[]{:S(2)}, u32[]{:S(2)}) async-start(bf16[16,48,1024]{2,1,0:T(8,128)(2,1)} %get-tuple-element.48), calls=%async_computation.2 | async-start | bytes 3145728 | tf_op jit(solution)/shard_map/all_to_all | solution.py:20
  (74 other events, 688.0 us)
